TPU v7x, 256 devices: a whole 4x4x8 slice. The times are simulated.
256 devices in a mesh: ep: 16 (over y, x), tp: 16 (over z, core).
Axes of the slice: x: 4, y: 4, z: 8, core: 2. Of those that a mesh axis runs over, the one named last changes fastest.
Arguments:
- mix_tokens: bfloat16 [4096, 4096], P('ep'), may hold values from -6 to 6
- mix_gain: float32 [4096], replicated, may hold values from 0.1 to 1.9
- value_weight: bfloat16 [4096, 2048], P(None, 'tp'), may hold values from -0.09375 to 0.09375
- inner_weight: bfloat16 [4096, 2048], P(None, 'tp'), may hold values from -0.09375 to 0.09375
- outer_weight: bfloat16 [4096, 2048], P(None, 'tp'), may hold values from -0.09375 to 0.09375
- conv_taps: float32 [3, 2048], P(None, 'tp'), may hold values from -3 to 3
- mix_weight: bfloat16 [2048, 4096], P('tp'), may hold values from -0.125 to 0.125
- moe_tokens: bfloat16 [4096, 4096], P('ep'), may hold values from -6 to 6
- moe_gain: float32 [4096], replicated, may hold values from 0.1 to 1.9
- router_group: bfloat16 [4096, 4], replicated, may hold values from -0.09375 to 0.09375
- router_expert: bfloat16 [4096, 16], replicated, may hold values from -0.09375 to 0.09375
- expert_routes: int32 [4096, 2], P('ep'), may hold values from 0 to 15, as said below
- gate_weight: bfloat16 [16, 4096, 2048], P('ep', None, 'tp'), may hold values from -0.09375 to 0.09375
- up_weight: bfloat16 [16, 4096, 2048], P('ep', None, 'tp'), may hold values from -0.09375 to 0.09375
- down_weight: bfloat16 [16, 2048, 4096], P('ep', 'tp'), may hold values from -0.5 to 0.5
Outputs:
- mixer_out: bfloat16 [4096, 4096], P(('ep', 'tp'))
- expert_out: bfloat16 [4096, 4096], P(('ep', 'tp'))
Inputs may be any that keep to these rules, and one draw needn't show every extreme that they name: `expert_routes`: the two experts of a row are different and lie in one group of 4 consecutive expert numbers. In each aligned block of 16 rows no expert is named more than 4 times, and in every draw some experts are named exactly 4 times in every block.
All inputs are finite; a program needn't handle non-finite values.
Results may differ from a plain program's by a relative error of at most 0.0076.
Values may be sent and summed in bfloat16 or wider, within the bound.
No kernel may reach another device: no remote copies, remote signals or barrier semaphores. Data moves between devices by JAX's collectives and lax.ppermute only.
A program may use at most 128 MiB of HBM per device.

v0:
```python
import jax
import jax.numpy as jnp
from jax import lax
from jax.sharding import PartitionSpec as P

TAPS = 3
EXPERTS = 16
GROUPS = 4
TOPK = 2
MOE_SHARE = 16
EPG = 4
CAP = 4


def from_behind(value, axis, steps):
    count = lax.axis_size(axis)
    initial, last = (max(0, -steps), min(count, count - steps))
    return lax.ppermute(value, axis, [(source, source + steps) for source in range(initial, last)])


def rms_rows(inputs, gain_vec):
    values = inputs.astype(jnp.float32)
    inverse = lax.rsqrt(jnp.mean(values * values, axis=-1, keepdims=True) + 1e-06)
    return (values * inverse * gain_vec).astype(jnp.bfloat16)


def route_weights(normed, routes, router_group, router_expert):
    group_logit = jnp.dot(normed, router_group, preferred_element_type=jnp.float32)
    expert_logit = jnp.dot(normed, router_expert, preferred_element_type=jnp.float32)
    group_exp = jnp.exp(group_logit)
    group_id = routes[:, 0] // EPG
    group_pick = (group_id[:, None] == jnp.arange(GROUPS, dtype=jnp.int32)[None, :]).astype(
        jnp.float32
    )
    group_gate = jnp.sum(group_exp * group_pick, axis=1) / jnp.sum(group_exp, axis=1)
    expert_pick = (
        routes[:, :, None] == jnp.arange(EXPERTS, dtype=jnp.int32)[None, None, :]
    ).astype(jnp.float32)
    chosen = jnp.exp(jnp.sum(expert_logit[:, None, :] * expert_pick, axis=2))
    return group_gate[:, None] * chosen / jnp.sum(chosen, axis=1, keepdims=True)


def block_ranks(routes):
    blocks = routes.shape[0]
    entries = routes.reshape(blocks, MOE_SHARE * TOPK)
    one_hot = (entries[:, :, None] == jnp.arange(EXPERTS, dtype=jnp.int32)[None, None, :]).astype(
        jnp.int32
    )
    before = jnp.cumsum(one_hot, axis=1) - one_hot
    return jnp.sum(before * one_hot, axis=2).reshape(routes.shape)


def dispatch_rows(normed, routes):
    slot_ids = routes * CAP + block_ranks(routes)
    targets = jnp.arange(EXPERTS * CAP, dtype=jnp.int32)
    select = (slot_ids[:, None, :, :] == targets[None, :, None, None]).astype(jnp.int32)
    select = jnp.sum(select, axis=3).astype(jnp.bfloat16)
    placed = jnp.einsum("bcs,bsd->bcd", select, normed, preferred_element_type=jnp.float32)
    return placed.astype(jnp.bfloat16).reshape(normed.shape[0], EXPERTS, CAP, normed.shape[2])


def expert_hidden(arrived, gate_weight, up_weight):
    gate_proj = jnp.einsum(
        "besd,edf->besf", arrived, gate_weight, preferred_element_type=jnp.float32
    )
    up_proj = jnp.einsum("besd,edf->besf", arrived, up_weight, preferred_element_type=jnp.float32)
    return (jax.nn.silu(gate_proj) * up_proj).astype(jnp.bfloat16)


def mixer_half(
    mix_tokens, mix_gain, value_weight, inner_weight, outer_weight, conv_taps, mix_weight
):
    normed = rms_rows(mix_tokens, mix_gain)
    value_proj = jnp.dot(normed, value_weight, preferred_element_type=jnp.float32)
    inner_proj = jnp.dot(normed, inner_weight, preferred_element_type=jnp.float32)
    outer_proj = jnp.dot(normed, outer_weight, preferred_element_type=jnp.float32)
    gated_in = (inner_proj * value_proj).astype(jnp.bfloat16)
    earlier = from_behind(gated_in[gated_in.shape[0] - (TAPS - 1) :], "ep", 1)
    padded = jnp.concatenate([earlier, gated_in], axis=0).astype(jnp.float32)
    seq_rows = gated_in.shape[0]
    mixed_conv = conv_taps[0] * padded[0:seq_rows]
    for tap_index in range(1, TAPS):
        mixed_conv = mixed_conv + conv_taps[tap_index] * padded[tap_index : tap_index + seq_rows]
    conv_out = (outer_proj * mixed_conv).astype(jnp.bfloat16)
    summed = lax.psum_scatter(
        jnp.dot(conv_out, mix_weight, preferred_element_type=jnp.float32),
        "tp",
        scatter_dimension=0,
        tiled=True,
    )
    return summed.astype(jnp.bfloat16)


def local(
    mix_tokens,
    mix_gain,
    value_weight,
    inner_weight,
    outer_weight,
    conv_taps,
    mix_weight,
    moe_tokens,
    moe_gain,
    router_group,
    router_expert,
    expert_routes,
    gate_weight,
    up_weight,
    down_weight,
):
    mixer_out = mixer_half(
        mix_tokens, mix_gain, value_weight, inner_weight, outer_weight, conv_taps, mix_weight
    )
    tp_index = lax.axis_index("tp")
    model_width = moe_tokens.shape[1]
    own_routes = lax.dynamic_slice_in_dim(expert_routes, tp_index * MOE_SHARE, MOE_SHARE, 0)
    own_tokens = lax.dynamic_slice_in_dim(moe_tokens, tp_index * MOE_SHARE, MOE_SHARE, 0)
    own_normed = rms_rows(own_tokens, moe_gain)
    placed = dispatch_rows(own_normed[None], own_routes[None])[0]
    arrived = lax.all_to_all(placed, "ep", split_axis=0, concat_axis=1, tiled=True)
    hidden = expert_hidden(
        lax.all_gather(arrived[None], "tp", axis=0, tiled=True), gate_weight, up_weight
    )
    local_experts = hidden.shape[1]
    slot_count = hidden.shape[2]
    per_block = local_experts * slot_count
    partial_value = jnp.einsum(
        "besf,efd->besd", hidden, down_weight, preferred_element_type=jnp.float32
    )
    summed = lax.psum_scatter(
        partial_value.reshape(per_block * lax.axis_size("tp"), model_width),
        "tp",
        scatter_dimension=0,
        tiled=True,
    )
    results = summed.astype(jnp.bfloat16).reshape(
        local_experts, slot_count // CAP, CAP, model_width
    )
    returned = lax.all_to_all(results, "ep", split_axis=1, concat_axis=0, tiled=True).reshape(
        EXPERTS * CAP, model_width
    )
    weights = route_weights(own_normed, own_routes, router_group, router_expert)
    own_slots = own_routes * CAP + block_ranks(own_routes[None])[0]
    picked = jnp.take(returned, own_slots, axis=0).astype(jnp.float32)
    expert_out = jnp.sum(weights[:, :, None] * picked, axis=1).astype(jnp.bfloat16)
    return (mixer_out, expert_out)


def solution(mesh):
    return jax.shard_map(
        local,
        mesh=mesh,
        in_specs=(
            P("ep", None),
            P(),
            P(None, "tp"),
            P(None, "tp"),
            P(None, "tp"),
            P(None, "tp"),
            P("tp", None),
            P("ep", None),
            P(),
            P(),
            P(),
            P("ep", None),
            P("ep", None, "tp"),
            P("ep", None, "tp"),
            P("ep", "tp", None),
        ),
        out_specs=(P(("ep", "tp"), None), P(("ep", "tp"), None)),
        check_vma=False,
    )
```

profile of v0, /device:TPU:2, one launch (start us, length us, event | category | flops | bytes accessed | tf_op | source)
XLA Modules:
  0.0 281.7 jit_solution(8360812834643250856)
XLA Ops:
  7.2 0.0 copy-start
  7.2 0.0 all-gather.2.cloned.1.call-start
  7.2 0.8 constant_dynamic-slice_fusion
  8.1 0.1 copy.25
  8.1 0.1 eq.90
  8.2 0.1 fusion.48
  8.3 0.1 reduce_window_sum.12
  8.4 0.2 select_reduce_fusion
  8.6 0.1 squeeze_reshape.6
  8.6 0.1 copy.26
  8.7 0.8 compare_and_fusion
  9.5 0.1 convert_reduce_fusion
  9.6 1.0 fusion.37
  10.6 1.3 convolution_convert_fusion
  11.9 0.2 squeeze_reshape.7
  12.1 17.4 %all_to_all.8 = bf16[16,4,4096]{2,1,0:T(4,128)(2,1)S(1)} all-to-all(bf16[16,4,4096]{2,1,0:T(4,128)(2,1)S(1)} %squeeze_reshape.7), channel_id=1, replica_groups=mesh['ep'=16,'tp'=16] {'ep'}, dimensions={0} | all-to-all | bytes 1048576 | tf_op jit(solution)/shard_map/all_to_all | solution.py:120
  29.5 0.9 broadcast_in_dim.12
  30.5 0.0 all-gather.2.cloned.1.call-update
  30.5 0.0 copy-start.2
  30.5 0.0 reduce-scatter.5.cloned.1.call-start
  30.5 55.9 %all-gather.2.cloned.1.call-done = bf16[16,1,64,4096]{3,2,1,0:T(8,128)(2,1)} async-done(((bf16[1,1,64,4096]{3,2,1,0:T(8,128)(2,1)}), bf16[16,1,64,4096]{3,2,1,0:T(8,128)(2,1)}) %all-gather.2.cloned.1.call-update) | async-done | bytes 8388624 | tf_op jit(solution)/shard_map/all_gather | solution.py:122
  86.5 5.9 %fusion.7 = f32[16,1,64,128]{3,2,0,1:T(8,128)S(1)} fusion(bf16[16,1,64,4096]{3,2,1,0:T(8,128)(2,1)} %all-gather.2.cloned.1.call-done, bf16[1,4096,128]{2,1,0:T(8,128)(2,1)} %param.27), kind=kOutput, calls=%fused_computation.11 | convolution fusion | flops 1073741824 | bytes 9961472 | tf_op jit(solution)/shard_map/besd,edf->besf/dot_general | solution.py:63
  92.4 0.0 copy-done
  92.4 0.0 copy-done.2
  92.4 14.4 %fusion.23 = f32[16,64,4096]{2,1,0:T(8,128)} fusion(bf16[16,1,64,4096]{3,2,1,0:T(8,128)(2,1)} %all-gather.2.cloned.1.call-done, bf16[1,128,4096]{2,1,0:T(8,128)(2,1)S(1)} %copy-done, bf16[1,4096,128]{2,1,0:T(8,128)(2,1)S(1)} %copy-done.2, f32[16,1,64,128]{3,2,0,1:T(8,128)S(1)} %fusion.7), kind=kOutput, calls=%fused_computation.16 | convolution fusion | flops 2148270080 | bytes 27787264 | tf_op jit(solution)/shard_map/besf,efd->besd/dot_general | solution.py:127
  106.8 0.0 copy-start.1
  106.8 0.0 reduce-scatter.5.cloned.1.call-update
  106.8 0.0 reduce-scatter.3.cloned.1.call-start
  106.9 1.5 copy-done.1
  108.4 0.0 copy-start.6
  108.4 0.5 fusion.4
  108.9 0.0 copy-done.3
  108.9 0.0 copy-start.5
  108.9 2.1 fusion.57
  111.0 0.0 copy-done.6
  111.0 0.9 fusion.26
  111.9 3.4 %collective-permute-start = (bf16[2,128]{1,0:T(2,128)(2,1)S(1)}, bf16[2,128]{1,0:T(2,128)(2,1)S(1)}, u32[]{:S(2)}, u32[]{:S(2)}) collective-permute-start(bf16[2,128]{1,0:T(2,128)(2,1)S(1)} %slice.34), channel_id=1, source_target_pairs={{0,16},{16,32},{32,48},{48,64},{64,80},{80,96},{96,112},{112,128},... | collective-permute-start | bytes 1544 | tf_op jit(solution)/shard_map/ppermute | solution.py:18
  115.3 0.0 copy-done.5
  115.3 2.1 collective-permute-done
  117.4 5.0 %fusion.27 = f32[256,4096]{1,0:T(8,128)} fusion(bf16[128,4096]{1,0:T(8,128)(2,1)} %param.21, bf16[4096,128]{1,0:T(8,128)(2,1)} %param.19, f32[258,128]{1,0:T(8,128)S(1)} %maximum_convert_fusion, f32[128]{0:T(128)S(1)} %get-tuple-element.7, f32[128]{0:T(128)S(1)} %get-tuple-element.8, f32[128]{0:T(128)S(1)} %get-tuple-element.6, ...), kind=kOutput, calls=%fused_computation.21 | convolution fusion | flops 541294592 | bytes 8800768 | tf_op jit(solution)/shard_map/dot_general | solution.py:86
  122.4 0.0 copy-start.4
  122.4 0.0 copy-start.8
  122.4 0.0 reduce-scatter.3.cloned.1.call-update
  122.4 0.7 copy-done.4
  123.1 0.1 copy-done.8
  123.1 1.2 fusion.61
  124.3 0.0 copy-done.7
  124.3 1.1 fusion.53
  125.5 80.6 %reduce-scatter.5.cloned.1.call-done = f32[64,4096]{1,0:T(8,128)} async-done(((f32[1024,4096]{1,0:T(8,128)}), f32[64,4096]{1,0:T(8,128)}) %reduce-scatter.5.cloned.1.call-update) | async-done | bytes 1048592 | tf_op jit(solution)/shard_map/reduce_scatter | solution.py:130
  206.1 1.3 convert_element_type.92
  207.4 1.0 reshape.229
  208.4 7.3 %all-to-all-start.1 = ((bf16[1,16,4,4096]{3,2,0,1:T(4,128)(2,1)}), bf16[1,16,4,4096]{3,2,0,1:T(4,128)(2,1)S(1)}, u32[]{:S(2)}, u32[]{:S(2)}) async-start(bf16[1,16,4,4096]{3,2,0,1:T(4,128)(2,1)} %reshape.229), calls=%async_computation.3 | async-start | bytes 1048576 | tf_op jit(solution)/shard_map/all_to_all | solution.py:139
  215.6 0.2 select_reduce_fusion.1
  215.8 0.1 copy.28
  215.9 0.1 reshape.233
  216.0 0.1 copy.24
  216.1 0.1 copy.27
  216.2 54.8 %reduce-scatter.3.cloned.1.call-done = f32[16,4096]{1,0:T(8,128)} async-done(((f32[256,4096]{1,0:T(8,128)}), f32[16,4096]{1,0:T(8,128)}) %reduce-scatter.3.cloned.1.call-update) | async-done | bytes 262160 | tf_op jit(solution)/shard_map/reduce_scatter | solution.py:85
  271.0 1.6 convert_element_type.84
  272.7 0.0 all-to-all-done.1
  272.7 0.1 reshape.230
  272.8 0.7 gather_fusion
  273.5 0.2 reshape.232
  273.7 1.5 multiply_reduce_fusion
  (13 shorter events, 0.1 us)
Async XLA Ops:
  7.2 85.2 %copy-start = (bf16[1,128,4096]{2,1,0:T(8,128)(2,1)S(1)}, bf16[1,128,4096]{2,1,0:T(8,128)(2,1)}, u32[]{:S(2)}) copy-start(bf16[1,128,4096]{2,1,0:T(8,128)(2,1)} %param.29) | copy-start | bytes 3145732
  7.2 79.3 %all-gather.2.cloned.1.call-start = ((), (), s32[]{:S(2)}) async-start(), calls=%async_computation.5 | async-start | bytes 8912896 | tf_op jit(solution)/shard_map/all_gather | solution.py:122
  30.5 61.9 %copy-start.2 = (bf16[1,4096,128]{2,1,0:T(8,128)(2,1)S(1)}, bf16[1,4096,128]{2,1,0:T(8,128)(2,1)}, u32[]{:S(2)}) copy-start(bf16[1,4096,128]{2,1,0:T(8,128)(2,1)} %param.28) | copy-start | bytes 3145732
  30.5 175.6 %reduce-scatter.5.cloned.1.call-start = ((), (), s32[]{:S(2)}) async-start(), calls=%async_computation.6 | async-start | bytes 17825792 | tf_op jit(solution)/shard_map/reduce_scatter | solution.py:130
  106.8 1.6 copy-start.1
  106.8 2.1 copy-start.3
  106.8 164.2 %reduce-scatter.3.cloned.1.call-start = ((), (), s32[]{:S(2)}) async-start(), calls=%async_computation.4 | async-start | bytes 4456448 | tf_op jit(solution)/shard_map/reduce_scatter | solution.py:85
  108.4 2.6 copy-start.6
  108.9 6.4 %copy-start.5 = (f32[3,128]{1,0:T(4,128)S(1)}, f32[3,128]{1,0:T(4,128)}, u32[]{:S(2)}) copy-start(f32[3,128]{1,0:T(4,128)} %param.20) | copy-start | bytes 4612
  111.9 5.5 %collective-permute-start = (bf16[2,128]{1,0:T(2,128)(2,1)S(1)}, bf16[2,128]{1,0:T(2,128)(2,1)S(1)}, u32[]{:S(2)}, u32[]{:S(2)}) collective-permute-start(bf16[2,128]{1,0:T(2,128)(2,1)S(1)} %slice.34), channel_id=1, source_target_pairs={{0,16},{16,32},{32,48},{48,64},{64,80},{80,96},{96,112},{112,128},... | collective-permute-start | bytes 1544 | tf_op jit(solution)/shard_map/ppermute | solution.py:18
  122.4 0.7 copy-start.4
  122.4 0.8 copy-start.8
  122.4 1.9 copy-start.7
  208.4 64.3 %all-to-all-start.1 = ((bf16[1,16,4,4096]{3,2,0,1:T(4,128)(2,1)}), bf16[1,16,4,4096]{3,2,0,1:T(4,128)(2,1)S(1)}, u32[]{:S(2)}, u32[]{:S(2)}) async-start(bf16[1,16,4,4096]{3,2,0,1:T(4,128)(2,1)} %reshape.229), calls=%async_computation.3 | async-start | bytes 1048576 | tf_op jit(solution)/shard_map/all_to_all | solution.py:139
Sparse Core Ops, SparseCore 0:
  30.6 55.8 all-gather.1
  107.0 99.0 reduce-scatter.4
  208.6 62.3 reduce-scatter.2
where the time goes:
time: 282 us
  waiting for transfers between devices  193 us (68%)
  matrix products  31.8 us (11%)
  blocking collectives  17.4 us (6%)
  between operations  14 us (5%)
  starting transfers between devices  10.8 us (4%)
  other arithmetic  7.33 us (3%)
  local copies, waits for them, and re-layouts  6.92 us (2%)
    reduce_scatter x1, waiting for transfers between devices, local(): lax.psum_scatter(partial_value.reshape(per_block * lax.axis_size('tp'), m...  80.6 us
    all_gather x1, waiting for transfers between devices, local(): lax.all_gather(arrived[None], 'tp', axis=0, tiled=True)  55.9 us
    reduce_scatter x1, waiting for transfers between devices, mixer_half(): lax.psum_scatter(jnp.dot(conv_out, mix_weight, preferred_element_type=jnp...  54.8 us
    all_to_all x1, blocking collectives, local(): lax.all_to_all(placed, 'ep', split_axis=0, concat_axis=1, tiled=True)  17.4 us
    dot_general x1, matrix products, local(): jnp.einsum('besf,efd->besd', hidden, down_weight, preferred_element_type=...  14.4 us
    all_to_all x1, starting transfers between devices, local(): lax.all_to_all(results, 'ep', split_axis=1, concat_axis=0, tiled=True)  7.27 us
    dot_general x1, matrix products, expert_hidden(): jnp.einsum('besd,edf->besf', arrived, gate_weight, preferred_element_type...  5.93 us
  transfers between devices with their start and end apart: 5, of which 4 were waited for; matrix products, arithmetic and copies ran while one was open for 5% of the time, Pallas kernels for 0%

commit v1 on v0

v1 whole, which is shorter than its diff:
```python
import jax
import jax.numpy as jnp
from jax import lax
from jax.sharding import Mesh
from jax.sharding import PartitionSpec as P

TAPS = 3
EXPERTS = 16
GROUPS = 4
TOPK = 2
MOE_SHARE = 16
EPG = 4
CAP = 4

EP = ("y", "x")
TP = ("z", "core")
ALL = EP + TP


def rms_rows(inputs, gain_vec):
    values = inputs.astype(jnp.float32)
    inverse = lax.rsqrt(jnp.mean(values * values, axis=-1, keepdims=True) + 1e-06)
    return (values * inverse * gain_vec).astype(jnp.bfloat16)


def route_weights(normed, routes, router_group, router_expert):
    group_logit = jnp.dot(normed, router_group, preferred_element_type=jnp.float32)
    expert_logit = jnp.dot(normed, router_expert, preferred_element_type=jnp.float32)
    group_exp = jnp.exp(group_logit)
    group_id = routes[:, 0] // EPG
    group_pick = (group_id[:, None] == jnp.arange(GROUPS, dtype=jnp.int32)[None, :]).astype(
        jnp.float32
    )
    group_gate = jnp.sum(group_exp * group_pick, axis=1) / jnp.sum(group_exp, axis=1)
    expert_pick = (
        routes[:, :, None] == jnp.arange(EXPERTS, dtype=jnp.int32)[None, None, :]
    ).astype(jnp.float32)
    chosen = jnp.exp(jnp.sum(expert_logit[:, None, :] * expert_pick, axis=2))
    return group_gate[:, None] * chosen / jnp.sum(chosen, axis=1, keepdims=True)


def block_ranks(routes):
    blocks = routes.shape[0] // MOE_SHARE
    entries = routes.reshape(blocks, MOE_SHARE * TOPK)
    same = entries[:, :, None] == entries[:, None, :]
    place = jnp.arange(MOE_SHARE * TOPK, dtype=jnp.int32)
    earlier = place[None, :] < place[:, None]
    return jnp.sum((same & earlier[None]).astype(jnp.int32), axis=2).reshape(routes.shape)


def swap_cores(value):
    return lax.ppermute(value, "core", [(0, 1), (1, 0)])


def own_core_blocks(array, core):
    rows, width = array.shape
    blocks = rows // MOE_SHARE
    split = array.reshape(blocks // 2, 2, MOE_SHARE, width)
    return lax.dynamic_index_in_dim(split, core, 1, keepdims=False).reshape(rows // 2, width)


def both_cores(mine, theirs, axis):
    return jnp.concatenate([mine, theirs], axis=axis)


def mixer_partial(
    mix_tokens, mix_gain, value_weight, inner_weight, outer_weight, conv_taps, mix_weight2, core
):
    normed = rms_rows(mix_tokens, mix_gain)
    value_proj = jnp.dot(normed, value_weight, preferred_element_type=jnp.float32)
    inner_proj = jnp.dot(normed, inner_weight, preferred_element_type=jnp.float32)
    outer_proj = jnp.dot(normed, outer_weight, preferred_element_type=jnp.float32)
    gated_in = (inner_proj * value_proj).astype(jnp.bfloat16)
    count = lax.axis_size(EP)
    earlier = lax.ppermute(
        gated_in[gated_in.shape[0] - (TAPS - 1) :], EP, [(i, i + 1) for i in range(count - 1)]
    )
    padded = jnp.concatenate([earlier, gated_in], axis=0).astype(jnp.float32)
    seq_rows = gated_in.shape[0]
    mixed_conv = conv_taps[0] * padded[0:seq_rows]
    for tap_index in range(1, TAPS):
        mixed_conv = mixed_conv + conv_taps[tap_index] * padded[tap_index : tap_index + seq_rows]
    conv_out = (outer_proj * mixed_conv).astype(jnp.bfloat16)
    mine = own_core_blocks(conv_out, core)
    theirs = swap_cores(own_core_blocks(conv_out, 1 - core))
    channels = both_cores(mine, theirs, 1)
    return jnp.dot(channels, mix_weight2, preferred_element_type=jnp.float32).astype(jnp.bfloat16)


def local(
    mix_tokens,
    mix_gain,
    value_weight,
    inner_weight,
    outer_weight,
    conv_taps,
    mix_weight,
    moe_tokens,
    moe_gain,
    router_group,
    router_expert,
    expert_routes,
    gate_weight,
    up_weight,
    down_weight,
):
    z_index = lax.axis_index("z")
    core = lax.axis_index("core")
    zs = lax.axis_size("z")
    eps = lax.axis_size(EP)
    width = moe_tokens.shape[1]

    gate_up = jnp.concatenate([gate_weight[0], up_weight[0]], axis=1)
    gate_up2 = both_cores(gate_up, swap_cores(gate_up), 1)
    down2 = both_cores(down_weight[0], swap_cores(down_weight[0]), 0)
    mix_weight2 = both_cores(mix_weight, swap_cores(mix_weight), 0)

    half_routes = own_core_blocks(expert_routes, core)
    half_normed = rms_rows(own_core_blocks(moe_tokens, core), moe_gain)
    ranks = block_ranks(half_routes)
    block_id = jnp.arange(half_routes.shape[0], dtype=jnp.int32)[:, None] // MOE_SHARE
    slots = half_routes * (zs * CAP) + block_id * CAP + ranks
    targets = jnp.arange(EXPERTS * zs * CAP, dtype=jnp.int32)
    select = (slots[None, :, 0] == targets[:, None]) | (slots[None, :, 1] == targets[:, None])
    placed = jnp.dot(
        select.astype(jnp.bfloat16), half_normed, preferred_element_type=jnp.float32
    ).astype(jnp.bfloat16)
    arrived = lax.all_to_all(
        placed.reshape(EXPERTS, zs * CAP, width), EP, split_axis=0, concat_axis=0, tiled=True
    ).reshape(eps * zs * CAP, width)

    partial_mix = mixer_partial(
        mix_tokens, mix_gain, value_weight, inner_weight, outer_weight, conv_taps, mix_weight2, core
    )
    mixer_out = lax.psum_scatter(partial_mix, "z", scatter_dimension=0, tiled=True)
    arrived, partial_mix, gate_up2 = lax.optimization_barrier((arrived, partial_mix, gate_up2))

    both = jnp.dot(arrived, gate_up2, preferred_element_type=jnp.float32)
    units = gate_weight.shape[2]
    gate_proj = jnp.concatenate([both[:, 0:units], both[:, 2 * units : 3 * units]], axis=1)
    up_proj = jnp.concatenate([both[:, units : 2 * units], both[:, 3 * units :]], axis=1)
    hidden = (jax.nn.silu(gate_proj) * up_proj).astype(jnp.bfloat16)
    hidden = (
        hidden.reshape(eps, zs, CAP, 2 * units).transpose(1, 0, 2, 3).reshape(-1, 2 * units)
    )
    hidden, mixer_out, down2 = lax.optimization_barrier((hidden, mixer_out, down2))
    partial_value = jnp.dot(hidden, down2, preferred_element_type=jnp.float32).astype(jnp.bfloat16)
    results = lax.psum_scatter(partial_value, "z", scatter_dimension=0, tiled=True)
    returned = lax.all_to_all(
        results.reshape(eps, CAP, width), EP, split_axis=0, concat_axis=0, tiled=True
    ).reshape(EXPERTS * CAP, width)

    own_routes = lax.dynamic_slice_in_dim(half_routes, z_index * MOE_SHARE, MOE_SHARE, 0)
    own_normed = lax.dynamic_slice_in_dim(half_normed, z_index * MOE_SHARE, MOE_SHARE, 0)
    own_ranks = lax.dynamic_slice_in_dim(ranks, z_index * MOE_SHARE, MOE_SHARE, 0)
    weights = route_weights(own_normed, own_routes, router_group, router_expert)
    own_slots = own_routes * CAP + own_ranks
    picked = jnp.take(returned, own_slots, axis=0).astype(jnp.float32)
    expert_out = jnp.sum(weights[:, :, None] * picked, axis=1).astype(jnp.bfloat16)
    return (mixer_out, expert_out)


def solution(mesh):
    torus = Mesh(mesh.devices.reshape(4, 4, 8, 2), ALL)
    return jax.shard_map(
        local,
        mesh=torus,
        in_specs=(
            P(EP, None),
            P(),
            P(None, TP),
            P(None, TP),
            P(None, TP),
            P(None, TP),
            P(TP, None),
            P(EP, None),
            P(),
            P(),
            P(),
            P(EP, None),
            P(EP, None, TP),
            P(EP, None, TP),
            P(EP, TP, None),
        ),
        out_specs=(P(ALL, None), P(ALL, None)),
        check_vma=False,
    )
```

time: 282 us -> 219 us (0.78)
  waiting for transfers between devices: 193 us -> 141 us
  blocking collectives: 17.4 us -> 0 us
  matrix products: 31.8 us -> 20.7 us
  starting transfers between devices: 10.8 us -> 19.2 us
  other arithmetic: 7.33 us -> 14.1 us
    all_gather x1 -> x0, waiting for transfers between devices: 55.9 us -> none  [local(): lax.all_gather(arrived[None], 'tp', axis=0, tiled=True)]
    reduce_scatter x2, waiting for transfers between devices: 135 us -> 83.1 us  [the longest x1 51.2 us: local(): lax.psum_scatter(partial_value, 'z', scatter_dimension=0, tiled=True)]
    ppermute x1 -> x5, waiting for transfers between devices: 2.06 us -> 48.7 us  [the longest x1 47.5 us: mixer_partial(): lax.ppermute(gated_in[gated_in.shape[0] - (TAPS - 1):], EP, [(i, i + 1) f...]
    all_to_all x1 -> x0, blocking collectives: 17.4 us -> none  [local(): lax.all_to_all(placed, 'ep', split_axis=0, concat_axis=1, tiled=True)]
    dot_general x6 -> x7, matrix products: 29.5 us -> 18.6 us  [the longest x1 5.79 us: local(): both = jnp.dot(arrived, gate_up2, preferred_element_type=jnp.float32)]
    all_to_all x1 -> x2, waiting for transfers between devices: 0.01 us -> 9.57 us  [the longest x1 9.56 us: local(): lax.all_to_all(results.reshape(eps, CAP, width), EP, split_axis=0, concat...]
    all_to_all x1 -> x2, starting transfers between devices: 7.27 us -> 14.9 us  [the longest x1 7.61 us: local(): lax.all_to_all(placed.reshape(EXPERTS, zs * CAP, width), EP, split_axis=0...]
    concatenate x0 -> x4, other arithmetic: none -> 7.16 us  [the longest x2 5.33 us: both_cores(): return jnp.concatenate([mine, theirs], axis=axis)]
  transfers between devices with their start and end apart: 5 -> 9, of which waited for: 4 -> 5; matrix products, arithmetic and copies ran while one was open for 5% -> 11% of each run, Pallas kernels for 0% -> 0%
where the time goes in v1:
time: 219 us; the launch traced here: 218 us
  waiting for transfers between devices  141 us (64%)
  matrix products  20.7 us (9%)
  starting transfers between devices  19.2 us (9%)
  between operations  14.4 us (7%)
  other arithmetic  14.1 us (6%)
  local copies, waits for them, and re-layouts  7.95 us (4%)
    reduce_scatter x1, waiting for transfers between devices, local(): lax.psum_scatter(partial_value, 'z', scatter_dimension=0, tiled=True)  51.2 us
    ppermute x1, waiting for transfers between devices, mixer_partial(): lax.ppermute(gated_in[gated_in.shape[0] - (TAPS - 1):], EP, [(i, i + 1) f...  47.5 us
    reduce_scatter x1, waiting for transfers between devices, local(): lax.psum_scatter(partial_mix, 'z', scatter_dimension=0, tiled=True)  31.9 us
    all_to_all x1, waiting for transfers between devices, local(): lax.all_to_all(results.reshape(eps, CAP, width), EP, split_axis=0, concat...  9.56 us
    all_to_all x1, starting transfers between devices, local(): lax.all_to_all(placed.reshape(EXPERTS, zs * CAP, width), EP, split_axis=0...  7.61 us
    all_to_all x1, starting transfers between devices, local(): lax.all_to_all(results.reshape(eps, CAP, width), EP, split_axis=0, concat...  7.27 us
    dot_general x1, matrix products, local(): both = jnp.dot(arrived, gate_up2, preferred_element_type=jnp.float32)  5.79 us
    concatenate x2, other arithmetic, both_cores(): return jnp.concatenate([mine, theirs], axis=axis)  5.33 us
  transfers between devices with their start and end apart: 9, of which 5 were waited for; matrix products, arithmetic and copies ran while one was open for 11% of the time, Pallas kernels for 0%

profile of v1, /device:TPU:2, one launch (start us, length us, event | category | flops | bytes accessed | tf_op | source)
XLA Modules:
  0.0 217.9 jit_solution(4882746622447486149)
XLA Ops:
  7.2 0.0 copy-start
  7.2 1.5 dynamic-slice_convert_fusion
  8.7 1.5 multiply_reduce_fusion
  10.2 0.1 reshape.185
  10.4 0.5 broadcast.150
  10.9 0.7 fusion.36
  11.6 0.1 copy.51
  11.6 0.1 copy.38
  11.7 0.3 convert_reduce_fusion
  12.0 0.1 reshape.187
  12.1 0.1 copy.40
  12.2 0.1 reshape.186
  12.3 0.1 rsqrt.20
  12.4 0.3 fusion.7
  12.7 1.0 copy-done.1
  13.7 3.2 %convolution_convert_fusion = bf16[512,4096]{1,0:T(8,128)(2,1)} fusion(bf16[128,4096]{1,0:T(8,128)(2,1)S(1)} %fusion.7, s32[128]{0:T(128)S(1)} %get-tuple-element.29, s32[128]{0:T(128)S(1)} %get-tuple-element.28), kind=kOutput, calls=%fused_computation.1 | convolution fusion | flops 539164672 | bytes 5243904 | tf_op jit(solution)/shard_map/dot_general | solution.py:125
  16.9 7.6 %all-to-all-start = ((bf16[16,32,4096]{2,1,0:T(8,128)(2,1)}), bf16[16,32,4096]{2,1,0:T(8,128)(2,1)}, u32[]{:S(2)}, u32[]{:S(2)}) async-start(bf16[16,32,4096]{2,1,0:T(8,128)(2,1)} %bitcast.48), calls=%async_computation | async-start | bytes 8388608 | tf_op jit(solution)/shard_map/all_to_all | solution.py:128
  24.5 0.0 reduce-scatter.3.cloned.1.call-start
  24.6 0.0 copy-start.4
  24.6 0.1 collective-permute-start.2
  24.7 1.6 pad_maximum_fusion.1
  26.3 0.5 collective-permute-start.3
  26.8 0.0 collective-permute-start.4
  26.8 0.0 copy-done.4
  26.8 0.5 fusion
  27.3 0.0 copy-start.10
  27.4 0.8 fusion.32
  28.2 0.9 fusion.9
  29.1 3.4 %collective-permute-start = (bf16[2,128]{1,0:T(2,128)(2,1)S(1)}, bf16[2,128]{1,0:T(2,128)(2,1)S(1)}, u32[]{:S(2)}, u32[]{:S(2)}) collective-permute-start(bf16[2,128]{1,0:T(2,128)(2,1)S(1)} %slice.58), channel_id=1, source_target_pairs={{0,16},{16,32},{32,48},{48,64},{64,80},{80,96},{96,112},{112,128},... | collective-permute-start | bytes 1544 | tf_op jit(solution)/shard_map/ppermute | solution.py:75
  32.5 0.0 copy-start.12
  32.5 47.5 %collective-permute-done = bf16[2,128]{1,0:T(2,128)(2,1)S(1)} collective-permute-done((bf16[2,128]{1,0:T(2,128)(2,1)S(1)}, bf16[2,128]{1,0:T(2,128)(2,1)S(1)}, u32[]{:S(2)}, u32[]{:S(2)}) %collective-permute-start) | collective-permute-done | bytes 544 | tf_op jit(solution)/shard_map/ppermute | solution.py:75
  80.0 2.0 fusion.8
  82.1 0.1 collective-permute-start.1
  82.2 1.2 collective-permute-done.1
  83.4 2.7 %convolution_convert_fusion.2 = bf16[128,4096]{1,0:T(8,128)(2,1)} fusion(bf16[128,4096]{1,0:T(8,128)(2,1)} %collective-permute-done.2, bf16[128,4096]{1,0:T(8,128)(2,1)S(1)} %copy-done.12, bf16[128,128]{1,0:T(8,128)(2,1)S(1)} %collective-permute-done.1, bf16[128,128]{1,0:T(8,128)(2,1)S(1)} %bitcast.61), kind=kOutput, calls=%fused_computation.5 | convolution fusion | flops 273285120 | bytes 3211264 | tf_op jit(solution)/shard_map/dot_general | solution.py:87
  86.1 0.0 reduce-scatter.3.cloned.1.call-update
  86.1 0.2 reduce-scatter.5.cloned.1.call-start
  86.4 1.7 pad_maximum_fusion.2
  88.1 3.7 %pad_maximum_fusion = bf16[4096,512]{1,0:T(8,128)(2,1)} fusion(bf16[4096,256]{1,0:T(8,128)(2,1)} %collective-permute-done.3, bf16[4096,128]{1,0:T(8,128)(2,1)} %bitcast.49, bf16[4096,128]{1,0:T(8,128)(2,1)} %bitcast.51), kind=kLoop, calls=%fused_computation.9 | loop fusion | flops 12582912 | bytes 8388608 | tf_op jit(solution)/shard_map/concatenate | solution.py:63
  91.7 5.8 %fusion.38 = f32[512,512]{1,0:T(8,128)S(1)} fusion(bf16[512,4096]{1,0:T(8,128)(2,1)} %bitcast.6, bf16[4096,512]{1,0:T(8,128)(2,1)} %pad_maximum_fusion), kind=kOutput, calls=%fused_computation.92 | convolution fusion | flops 2147483648 | bytes 9437184 | tf_op jit(solution)/shard_map/dot_general | solution.py:138
  97.5 0.1 fusion.37
  97.6 0.2 pad_maximum_fusion.3
  97.8 1.0 fusion.14
  98.8 1.0 reshape.194
  99.8 31.9 %reduce-scatter.3.cloned.1.call-done = bf16[16,4096]{1,0:T(8,128)(2,1)} async-done(((bf16[128,4096]{1,0:T(8,128)(2,1)}), bf16[16,4096]{1,0:T(8,128)(2,1)}) %reduce-scatter.3.cloned.1.call-update) | async-done | bytes 131088 | tf_op jit(solution)/shard_map/reduce_scatter | solution.py:135
  131.7 3.2 %convolution_convert_fusion.1 = bf16[512,4096]{1,0:T(8,128)(2,1)} fusion(bf16[512,256]{1,0:T(8,128)(2,1)S(1)} %reshape.194, bf16[256,4096]{1,0:T(8,128)(2,1)S(1)} %pad_maximum_fusion.2), kind=kOutput, calls=%fused_computation.2 | convolution fusion | flops 1075838976 | bytes 6553600 | tf_op jit(solution)/shard_map/dot_general | solution.py:147
  134.9 0.0 reduce-scatter.5.cloned.1.call-update
  135.0 0.1 compare_and_fusion
  135.1 0.6 copy-done.7
  135.7 1.1 fusion.35
  136.8 1.1 fusion.19
  137.9 51.2 %reduce-scatter.5.cloned.1.call-done = bf16[64,4096]{1,0:T(8,128)(2,1)} async-done(((bf16[512,4096]{1,0:T(8,128)(2,1)}), bf16[64,4096]{1,0:T(8,128)(2,1)}) %reduce-scatter.5.cloned.1.call-update) | async-done | bytes 524304 | tf_op jit(solution)/shard_map/reduce_scatter | solution.py:148
  189.1 2.0 reshape.195
  191.1 7.3 %all-to-all-start.1 = ((bf16[16,4,4096]{2,1,0:T(4,128)(2,1)}), bf16[16,4,4096]{2,1,0:T(4,128)(2,1)S(1)}, u32[]{:S(2)}, u32[]{:S(2)}) async-start(bf16[16,4,4096]{2,1,0:T(4,128)(2,1)} %reshape.195), calls=%async_computation.3 | async-start | bytes 1048576 | tf_op jit(solution)/shard_map/all_to_all | solution.py:149
  198.4 0.2 select_reduce_fusion
  198.6 0.1 copy.48
  198.6 0.1 reshape.200
  198.8 0.1 copy.45
  198.9 0.1 copy.47
  199.0 9.6 %all-to-all-done.1 = bf16[16,4,4096]{2,1,0:T(4,128)(2,1)S(1)} async-done(((bf16[16,4,4096]{2,1,0:T(4,128)(2,1)}), bf16[16,4,4096]{2,1,0:T(4,128)(2,1)S(1)}, u32[]{:S(2)}, u32[]{:S(2)}) %all-to-all-start.1) | async-done | bytes 524320 | tf_op jit(solution)/shard_map/all_to_all | solution.py:149
  208.5 0.1 reshape.196
  208.7 0.7 gather_fusion
  209.4 0.2 reshape.199
  209.6 1.5 multiply_reduce_fusion.1
  (40 shorter events, 0.2 us)
Async XLA Ops:
  7.2 20.1 %copy-start = (bf16[4096,128]{1,0:T(8,128)(2,1)S(1)}, bf16[4096,128]{1,0:T(8,128)(2,1)}, u32[]{:S(2)}) copy-start(bf16[4096,128]{1,0:T(8,128)(2,1)} %param.18) | copy-start | bytes 3145732
  7.2 3.1 %copy-start.9 = (s32[256,2]{0,1:T(2,128)S(1)}, s32[256,2]{0,1:T(2,128)}, u32[]{:S(2)}) copy-start(s32[256,2]{0,1:T(2,128)} %param.26) | copy-start | bytes 6148
  7.2 5.2 %copy-start.8 = (f32[4096]{0:T(1024)S(1)}, f32[4096]{0:T(1024)}, u32[]{:S(2)}) copy-start(f32[4096]{0:T(1024)} %param.23) | copy-start | bytes 49156
  12.7 1.0 copy-start.1
  16.9 7.8 %copy-start.2 = (bf16[1,4096,128]{2,1,0:T(8,128)(2,1)S(1)}, bf16[1,4096,128]{2,1,0:T(8,128)(2,1)}, u32[]{:S(2)}) copy-start(bf16[1,4096,128]{2,1,0:T(8,128)(2,1)} %param.28) | copy-start | bytes 3145732
  16.9 7.8 %copy-start.3 = (bf16[1,4096,128]{2,1,0:T(8,128)(2,1)S(1)}, bf16[1,4096,128]{2,1,0:T(8,128)(2,1)}, u32[]{:S(2)}) copy-start(bf16[1,4096,128]{2,1,0:T(8,128)(2,1)} %param.27) | copy-start | bytes 3145732
  16.9 74.8 %all-to-all-start = ((bf16[16,32,4096]{2,1,0:T(8,128)(2,1)}), bf16[16,32,4096]{2,1,0:T(8,128)(2,1)}, u32[]{:S(2)}, u32[]{:S(2)}) async-start(bf16[16,32,4096]{2,1,0:T(8,128)(2,1)} %bitcast.48), calls=%async_computation | async-start | bytes 8388608 | tf_op jit(solution)/shard_map/all_to_all | solution.py:128
  24.5 2.8 %copy-start.13 = (f32[4096]{0:T(1024)S(1)}, f32[4096]{0:T(1024)}, u32[]{:S(2)}) copy-start(f32[4096]{0:T(1024)} %param.16) | copy-start | bytes 49156
  24.5 107.2 %reduce-scatter.3.cloned.1.call-start = ((), (), s32[]{:S(2)}) async-start(), calls=%async_computation.4 | async-start | bytes 1179648 | tf_op jit(solution)/shard_map/reduce_scatter | solution.py:135
  24.6 2.2 %copy-start.4 = (bf16[256,4096]{1,0:T(8,128)(2,1)S(1)}, bf16[256,4096]{1,0:T(8,128)(2,1)}, u32[]{:S(2)}) copy-start(bf16[256,4096]{1,0:T(8,128)(2,1)} %param.15) | copy-start | bytes 6291460
  24.6 58.8 %collective-permute-start.2 = (bf16[128,4096]{1,0:T(8,128)(2,1)}, bf16[128,4096]{1,0:T(8,128)(2,1)}, u32[]{:S(2)}, u32[]{:S(2)}) collective-permute-start(bf16[128,4096]{1,0:T(8,128)(2,1)} %param.21), channel_id=1, source_target_pairs={{0,1},{1,0},{2,3},{3,2},{4,5},{5,4},{6,7},{7,6},{8,9},{9,8},{10,11... | collective-permute-start | bytes 3145736 | tf_op jit(solution)/shard_map/ppermute | solution.py:52
  26.3 1.9 copy-start.11
  26.3 61.8 %collective-permute-start.3 = (bf16[4096,256]{1,0:T(8,128)(2,1)}, bf16[4096,256]{1,0:T(8,128)(2,1)}, u32[]{:S(2)}, u32[]{:S(2)}) collective-permute-start(bf16[4096,256]{1,0:T(8,128)(2,1)} %pad_maximum_fusion.1), channel_id=1, source_target_pairs={{0,1},{1,0},{2,3},{3,2},{4,5},{5,4},{6,7},{7,6},{8,9},{9,8},{10,11... | collective-permute-start | bytes 6291464 | tf_op jit(solution)/shard_map/ppermute | solution.py:52
  26.8 59.6 %collective-permute-start.4 = (bf16[128,4096]{1,0:T(8,128)(2,1)}, bf16[128,4096]{1,0:T(8,128)(2,1)}, u32[]{:S(2)}, u32[]{:S(2)}) collective-permute-start(bf16[128,4096]{1,0:T(8,128)(2,1)} %bitcast.20), channel_id=1, source_target_pairs={{0,1},{1,0},{2,3},{3,2},{4,5},{5,4},{6,7},{7,6},{8,9},{9,8},{10,11... | collective-permute-start | bytes 3145736 | tf_op jit(solution)/shard_map/ppermute | solution.py:52
  27.3 5.1 %copy-start.10 = (f32[3,128]{1,0:T(4,128)S(1)}, f32[3,128]{1,0:T(4,128)}, u32[]{:S(2)}) copy-start(f32[3,128]{1,0:T(4,128)} %param.20) | copy-start | bytes 4612
  27.3 52.7 %copy-start.5 = (bf16[256,4096]{1,0:T(8,128)(2,1)S(1)}, bf16[256,4096]{1,0:T(8,128)(2,1)}, u32[]{:S(2)}) copy-start(bf16[256,4096]{1,0:T(8,128)(2,1)} %param.15) | copy-start | bytes 6291460
  29.1 50.9 %collective-permute-start = (bf16[2,128]{1,0:T(2,128)(2,1)S(1)}, bf16[2,128]{1,0:T(2,128)(2,1)S(1)}, u32[]{:S(2)}, u32[]{:S(2)}) collective-permute-start(bf16[2,128]{1,0:T(2,128)(2,1)S(1)} %slice.58), channel_id=1, source_target_pairs={{0,16},{16,32},{32,48},{48,64},{64,80},{80,96},{96,112},{112,128},... | collective-permute-start | bytes 1544 | tf_op jit(solution)/shard_map/ppermute | solution.py:75
  32.5 50.9 %copy-start.12 = (bf16[128,4096]{1,0:T(8,128)(2,1)S(1)}, bf16[128,4096]{1,0:T(8,128)(2,1)}, u32[]{:S(2)}) copy-start(bf16[128,4096]{1,0:T(8,128)(2,1)} %param.21) | copy-start | bytes 3145732
  82.1 1.3 collective-permute-start.1
  86.1 103.0 %reduce-scatter.5.cloned.1.call-start = ((), (), s32[]{:S(2)}) async-start(), calls=%async_computation.5 | async-start | bytes 4718592 | tf_op jit(solution)/shard_map/reduce_scatter | solution.py:148
  99.8 37.0 %copy-start.6 = (bf16[4096,16]{0,1:T(8,128)(2,1)S(1)}, bf16[4096,16]{0,1:T(8,128)(2,1)}, u32[]{:S(2)}) copy-start(bf16[4096,16]{0,1:T(8,128)(2,1)} %param.25) | copy-start | bytes 393220
  134.9 0.8 copy-start.7
  191.1 17.4 %all-to-all-start.1 = ((bf16[16,4,4096]{2,1,0:T(4,128)(2,1)}), bf16[16,4,4096]{2,1,0:T(4,128)(2,1)S(1)}, u32[]{:S(2)}, u32[]{:S(2)}) async-start(bf16[16,4,4096]{2,1,0:T(4,128)(2,1)} %reshape.195), calls=%async_computation.3 | async-start | bytes 1048576 | tf_op jit(solution)/shard_map/all_to_all | solution.py:149
Sparse Core Ops, SparseCore 0:
  86.2 45.4 reduce-scatter.2
  135.1 53.9 reduce-scatter.4

commit v2 on v1

v2 whole, which is shorter than its diff:
```python
import jax
import jax.numpy as jnp
from jax import lax
from jax.sharding import Mesh
from jax.sharding import PartitionSpec as P

TAPS = 3
EXPERTS = 16
GROUPS = 4
TOPK = 2
MOE_SHARE = 16
EPG = 4
CAP = 4

EP = ("y", "x")
TP = ("z", "core")
ALL = EP + TP


def rms_rows(inputs, gain_vec):
    values = inputs.astype(jnp.float32)
    inverse = lax.rsqrt(jnp.mean(values * values, axis=-1, keepdims=True) + 1e-06)
    return (values * inverse * gain_vec).astype(jnp.bfloat16)


def route_weights(normed, routes, router_group, router_expert):
    group_logit = jnp.dot(normed, router_group, preferred_element_type=jnp.float32)
    expert_logit = jnp.dot(normed, router_expert, preferred_element_type=jnp.float32)
    group_exp = jnp.exp(group_logit)
    group_id = routes[:, 0] // EPG
    group_pick = (group_id[:, None] == jnp.arange(GROUPS, dtype=jnp.int32)[None, :]).astype(
        jnp.float32
    )
    group_gate = jnp.sum(group_exp * group_pick, axis=1) / jnp.sum(group_exp, axis=1)
    expert_pick = (
        routes[:, :, None] == jnp.arange(EXPERTS, dtype=jnp.int32)[None, None, :]
    ).astype(jnp.float32)
    chosen = jnp.exp(jnp.sum(expert_logit[:, None, :] * expert_pick, axis=2))
    return group_gate[:, None] * chosen / jnp.sum(chosen, axis=1, keepdims=True)


def block_ranks(routes):
    blocks = routes.shape[0] // MOE_SHARE
    entries = routes.reshape(blocks, MOE_SHARE * TOPK)
    same = entries[:, :, None] == entries[:, None, :]
    place = jnp.arange(MOE_SHARE * TOPK, dtype=jnp.int32)
    earlier = place[None, :] < place[:, None]
    return jnp.sum((same & earlier[None]).astype(jnp.int32), axis=2).reshape(routes.shape)


def swap_cores(value):
    return lax.ppermute(value, "core", [(0, 1), (1, 0)])


def own_core_blocks(array, core):
    rows, width = array.shape
    blocks = rows // MOE_SHARE
    split = array.reshape(blocks // 2, 2, MOE_SHARE, width)
    return lax.dynamic_index_in_dim(split, core, 1, keepdims=False).reshape(rows // 2, width)


def both_cores(mine, theirs, axis):
    return jnp.concatenate([mine, theirs], axis=axis)


def mixer_channels(
    mix_tokens, before, mix_gain, weights, taps, core
):
    rows, width = mix_tokens.shape
    reach = TAPS - 1
    padded = jnp.concatenate([before, mix_tokens], axis=0)
    windows = [
        lax.dynamic_slice_in_dim(padded, (2 * block + core) * MOE_SHARE, MOE_SHARE + reach, 0)
        for block in range(rows // (2 * MOE_SHARE))
    ]
    normed = rms_rows(jnp.concatenate(windows, axis=0), mix_gain)
    value_proj, inner_proj, outer_proj = [
        jnp.concatenate(
            [jnp.dot(normed, part, preferred_element_type=jnp.float32) for part in pair], axis=1
        )
        for pair in weights
    ]
    channels = value_proj.shape[1]
    gated_in = (inner_proj * value_proj).astype(jnp.bfloat16).astype(jnp.float32)
    gated_in = gated_in.reshape(-1, MOE_SHARE + reach, channels)
    outer_proj = outer_proj.reshape(-1, MOE_SHARE + reach, channels)[:, reach:]
    mixed_conv = taps[0] * gated_in[:, 0:MOE_SHARE]
    for tap_index in range(1, TAPS):
        mixed_conv = mixed_conv + taps[tap_index] * gated_in[:, tap_index : tap_index + MOE_SHARE]
    return (outer_proj * mixed_conv).astype(jnp.bfloat16)


def swap_rows(array):
    return array.transpose(1, 0, 2)


def local(
    mix_tokens,
    mix_gain,
    value_weight,
    inner_weight,
    outer_weight,
    conv_taps,
    mix_weight,
    moe_tokens,
    moe_gain,
    router_group,
    router_expert,
    expert_routes,
    gate_weight,
    up_weight,
    down_weight,
):
    z_index = lax.axis_index("z")
    core = lax.axis_index("core")
    zs = lax.axis_size("z")
    eps = lax.axis_size(EP)
    width = moe_tokens.shape[1]
    units2 = 2 * gate_weight.shape[2]

    before = lax.ppermute(
        mix_tokens[mix_tokens.shape[0] - (TAPS - 1) :], EP, [(i, i + 1) for i in range(eps - 1)]
    )
    gate, up, down = gate_weight[0], up_weight[0], down_weight[0]
    swapped = [
        swap_cores(array)
        for array in (value_weight, inner_weight, outer_weight, mix_weight, gate, up, down)
    ]
    taps2 = both_cores(conv_taps, swap_cores(conv_taps), 1)
    down_mix = jnp.concatenate([down, swapped[6], mix_weight, swapped[3]], axis=0)
    gate_up = jnp.concatenate([gate, swapped[4], up, swapped[5]], axis=1)

    half_routes = own_core_blocks(expert_routes, core)
    half_normed = rms_rows(own_core_blocks(moe_tokens, core), moe_gain)
    ranks = block_ranks(half_routes)
    block_id = jnp.arange(half_routes.shape[0], dtype=jnp.int32)[:, None] // MOE_SHARE

    def dispatch(first, count, normed):
        position = (half_routes * count + ranks - first) * zs + block_id
        inside = (ranks >= first) & (ranks < first + count)
        position = jnp.where(inside, position, -1)
        targets = jnp.arange(EXPERTS * count * zs, dtype=jnp.int32)[:, None]
        select = (position[None, :, 0] == targets) | (position[None, :, 1] == targets)
        placed = jnp.dot(
            select.astype(jnp.bfloat16), normed, preferred_element_type=jnp.float32
        ).astype(jnp.bfloat16)
        return placed.reshape(EXPERTS, count * zs, width)

    def exchange(array):
        return lax.all_to_all(array, EP, split_axis=0, concat_axis=0, tiled=True)

    def expert_units(rows):
        both = jnp.dot(rows.reshape(-1, width), gate_up, preferred_element_type=jnp.float32)
        hidden = (jax.nn.silu(both[:, :units2]) * both[:, units2:]).astype(jnp.bfloat16)
        return swap_rows(hidden.reshape(-1, zs, units2))

    late = CAP - 1
    placed_first = dispatch(0, 1, half_normed)
    placed_first, half_late = lax.optimization_barrier((placed_first, half_normed))
    arrived_first = exchange(placed_first)
    arrived_late = exchange(dispatch(1, late, half_late))

    channels = mixer_channels(
        mix_tokens,
        before,
        mix_gain,
        (
            (value_weight, swapped[0]),
            (inner_weight, swapped[1]),
            (outer_weight, swapped[2]),
        ),
        taps2,
        core,
    )
    arrived_first, channels = lax.optimization_barrier((arrived_first, channels))

    first_units = expert_units(arrived_first)
    joint = jnp.concatenate(
        [
            jnp.concatenate([first_units, jnp.zeros_like(channels)], axis=2),
            jnp.concatenate([jnp.zeros_like(first_units), channels], axis=2),
        ],
        axis=1,
    )
    partial_first = jnp.dot(
        joint.reshape(-1, 2 * units2), down_mix, preferred_element_type=jnp.float32
    ).astype(jnp.bfloat16)
    arrived_late, _ = lax.optimization_barrier((arrived_late, partial_first))
    summed_first = lax.psum_scatter(partial_first, "z", scatter_dimension=0, tiled=True)
    mixer_out = summed_first[eps:]

    late_units = expert_units(arrived_late)
    partial_late = jnp.dot(
        late_units.reshape(-1, units2), down_mix[:units2], preferred_element_type=jnp.float32
    ).astype(jnp.bfloat16)
    summed_late = lax.psum_scatter(partial_late, "z", scatter_dimension=0, tiled=True)

    own_routes = lax.dynamic_slice_in_dim(half_routes, z_index * MOE_SHARE, MOE_SHARE, 0)
    own_normed = lax.dynamic_slice_in_dim(half_normed, z_index * MOE_SHARE, MOE_SHARE, 0)
    own_ranks = lax.dynamic_slice_in_dim(ranks, z_index * MOE_SHARE, MOE_SHARE, 0)
    weights = route_weights(own_normed, own_routes, router_group, router_expert)

    def combine(summed, first, count):
        returned = exchange(summed.reshape(eps, count * width // 128, 128)).reshape(-1, width)
        position = own_routes * count + own_ranks - first
        inside = (own_ranks >= first) & (own_ranks < first + count)
        position = jnp.where(inside, position, -1)
        targets = jnp.arange(EXPERTS * count, dtype=jnp.int32)
        spread = jnp.sum(
            jnp.where(position[:, :, None] == targets, weights[:, :, None], 0.0), axis=1
        )
        return jnp.dot(
            spread,
            returned.astype(jnp.float32),
            precision=lax.Precision.HIGHEST,
            preferred_element_type=jnp.float32,
        )

    expert_out = combine(summed_first[:eps], 0, 1) + combine(summed_late, 1, late)
    return (mixer_out, expert_out.astype(jnp.bfloat16))


def solution(mesh):
    torus = Mesh(mesh.devices.reshape(4, 4, 8, 2), ALL)
    return jax.shard_map(
        local,
        mesh=torus,
        in_specs=(
            P(EP, None),
            P(),
            P(None, TP),
            P(None, TP),
            P(None, TP),
            P(None, TP),
            P(TP, None),
            P(EP, None),
            P(),
            P(),
            P(),
            P(EP, None),
            P(EP, None, TP),
            P(EP, None, TP),
            P(EP, TP, None),
        ),
        out_specs=(P(ALL, None), P(ALL, None)),
        check_vma=False,
    )
```

time: 219 us -> 206 us (0.941)
  waiting for transfers between devices: 141 us -> 81.9 us
  local copies, waits for them, and re-layouts: 7.95 us -> 29 us
  starting transfers between devices: 19.2 us -> 35.8 us
  matrix products: 20.7 us -> 32.8 us
  other arithmetic: 14.1 us -> 9.88 us
    ppermute x1, waiting for transfers between devices: 47.5 us -> 0.01 us  [local(): lax.ppermute(mix_tokens[mix_tokens.shape[0] - (TAPS - 1):], EP, [(i, i +...]
    reduce_scatter x2, waiting for transfers between devices: 83.1 us -> 38 us  [the longest x1 38 us: local(): lax.psum_scatter(partial_late, 'z', scatter_dimension=0, tiled=True)]
    all_to_all x2 -> x4, waiting for transfers between devices: 9.57 us -> 43.8 us  [exchange(): return lax.all_to_all(array, EP, split_axis=0, concat_axis=0, tiled=True)]
    concatenate x0 -> x6, local copies, waits for them, and re-layouts: none -> 20.3 us  [the longest x1 14.7 us: mixer_channels(): normed = rms_rows(jnp.concatenate(windows, axis=0), mix_gain)]
    all_to_all x2 -> x4, starting transfers between devices: 14.9 us -> 30.4 us  [exchange(): return lax.all_to_all(array, EP, split_axis=0, concat_axis=0, tiled=True)]
    dot_general x7 -> x14, matrix products: 18.6 us -> 32.4 us  [the longest x6 10.9 us: mixer_channels(): jnp.dot(normed, part, preferred_element_type=jnp.float32)]
    concatenate x4, other arithmetic: 7.16 us -> 2.36 us  [the longest x2 2.33 us: mixer_channels(): padded = jnp.concatenate([before, mix_tokens], axis=0)]
  transfers between devices with their start and end apart: 9 -> 15, of which waited for: 5 -> 3; matrix products, arithmetic and copies ran while one was open for 11% -> 34% of each run, Pallas kernels for 0% -> 0%
where the time goes in v2:
time: 206 us; the launch traced here: 204 us
  waiting for transfers between devices  81.9 us (40%)
  starting transfers between devices  35.8 us (17%)
  matrix products  32.8 us (16%)
  local copies, waits for them, and re-layouts  29 us (14%)
  between operations  14.5 us (7%)
  other arithmetic  9.88 us (5%)
    all_to_all x4, waiting for transfers between devices, exchange(): return lax.all_to_all(array, EP, split_axis=0, concat_axis=0, tiled=True)  43.8 us
    reduce_scatter x1, waiting for transfers between devices, local(): lax.psum_scatter(partial_late, 'z', scatter_dimension=0, tiled=True)  38 us
    all_to_all x4, starting transfers between devices, exchange(): return lax.all_to_all(array, EP, split_axis=0, concat_axis=0, tiled=True)  30.4 us
    concatenate x1, local copies, waits for them, and re-layouts, mixer_channels(): normed = rms_rows(jnp.concatenate(windows, axis=0), mix_gain)  14.7 us
    dot_general x6, matrix products, mixer_channels(): jnp.dot(normed, part, preferred_element_type=jnp.float32)  10.9 us
    dot_general x2, matrix products, expert_units(): jnp.dot(rows.reshape(-1, width), gate_up, preferred_element_type=jnp.floa...  8.26 us
    concatenate x4, local copies, waits for them, and re-layouts, mixer_channels(): jnp.concatenate([jnp.dot(normed, part, preferred_element_type=jnp.float32...  5.57 us
    dot_general x1, matrix products, local(): jnp.dot(joint.reshape(-1, 2 * units2), down_mix, preferred_element_type=j...  4.17 us
  transfers between devices with their start and end apart: 15, of which 3 were waited for; matrix products, arithmetic and copies ran while one was open for 34% of the time, Pallas kernels for 0%

profile of v2, /device:TPU:2, one launch (start us, length us, event | category | flops | bytes accessed | tf_op | source)
XLA Modules:
  0.0 203.8 jit_solution(18416854427685878756)
XLA Ops:
  7.2 0.1 collective-permute-start.2
  7.3 0.9 slice.61
  8.1 3.4 %collective-permute-start = (bf16[2,4096]{1,0:T(2,128)(2,1)S(1)}, bf16[2,4096]{1,0:T(2,128)(2,1)S(1)}, u32[]{:S(2)}, u32[]{:S(2)}) collective-permute-start(bf16[2,4096]{1,0:T(2,128)(2,1)S(1)} %slice.61), channel_id=1, source_target_pairs={{0,16},{16,32},{32,48},{48,64},{64,80},{80,96},{96,112},{112,128},... | collective-permute-start | bytes 49160 | tf_op jit(solution)/shard_map/ppermute | solution.py:121
  11.6 0.3 collective-permute-start.5
  11.9 0.3 collective-permute-start.6
  12.2 0.2 collective-permute-start.4
  12.4 0.8 reshape.197
  13.3 0.1 copy.36
  13.4 1.5 multiply_reduce_fusion
  14.9 1.5 dynamic-slice_convert_fusion
  16.5 0.3 convert_reduce_fusion
  16.8 0.1 reshape.198
  16.9 0.1 add_select_fusion
  17.1 0.5 copy-done.6
  17.6 0.2 slice_reduce_fusion.1
  17.8 0.3 fusion.16
  18.1 1.4 fusion
  19.5 7.2 %all-to-all-start = ((bf16[16,8,4096]{2,1,0:T(8,128)(2,1)}), bf16[16,8,4096]{2,1,0:T(8,128)(2,1)}, u32[]{:S(2)}, u32[]{:S(2)}) async-start(bf16[16,8,4096]{2,1,0:T(8,128)(2,1)} %fusion), calls=%async_computation | async-start | bytes 2097152 | tf_op jit(solution)/shard_map/all_to_all | solution.py:150
  26.7 2.6 %convolution_convert_fusion.1 = bf16[384,4096]{1,0:T(8,128)(2,1)} fusion(bf16[128,4096]{1,0:T(8,128)(2,1)S(1)} %fusion.16, s32[128]{0:T(128)S(1)} %get-tuple-element.13, s32[128]{0:T(128)S(1)} %get-tuple-element.12), kind=kOutput, calls=%fused_computation.9 | convolution fusion | flops 404373504 | bytes 4195328 | tf_op jit(solution)/shard_map/dot_general | solution.py:144
  29.4 0.6 fusion.65
  30.0 0.5 collective-permute-start.1
  30.5 0.9 fusion.31
  31.4 1.4 fusion.24
  32.8 14.7 %concatenate.47 = bf16[144,4096]{1,0:T(8,128)(2,1)S(1)} concatenate(bf16[18,4096]{1,0:T(8,128)(2,1)} %get-tuple-element.19, bf16[18,4096]{1,0:T(8,128)(2,1)} %get-tuple-element.20, bf16[18,4096]{1,0:T(8,128)(2,1)} %get-tuple-element.21, bf16[18,4096]{1,0:T(8,128)(2,1)} %get-tuple-element.22, bf16[18,4096]{1,0:T(8,128)(2,1)} %get-tuple-element.23, ...), dimensions={0} | concatenate | bytes 2359296 | tf_op jit(solution)/shard_map/concatenate | solution.py:76
  47.6 0.3 fusion.9
  47.9 0.4 fusion.11
  48.3 0.5 copy-done.3
  48.8 1.1 fusion.70
  49.9 0.9 concatenate.53
  50.8 1.1 fusion.68
  51.9 1.6 concatenate.50
  53.5 2.3 %fusion.66 = f32[144,128]{1,0:T(8,128)} fusion(bf16[144,4096]{1,0:T(8,128)(2,1)S(1)} %fusion.11, bf16[4096,128]{1,0:T(8,128)(2,1)} %param.19), kind=kOutput, calls=%fused_computation.142 | convolution fusion | flops 150994944 | bytes 2301952 | tf_op jit(solution)/shard_map/dot_general | solution.py:79
  55.8 2.3 %fusion.69 = f32[144,128]{1,0:T(8,128)} fusion(bf16[144,4096]{1,0:T(8,128)(2,1)S(1)} %fusion.11, bf16[4096,128]{1,0:T(8,128)(2,1)} %collective-permute-done.3), kind=kOutput, calls=%fused_computation.145 | convolution fusion | flops 150994944 | bytes 2301952 | tf_op jit(solution)/shard_map/dot_general | solution.py:79
  58.2 1.5 concatenate.51
  59.7 0.5 collective-permute-start.8
  60.2 2.3 %fusion.71 = f32[144,128]{1,0:T(8,128)} fusion(bf16[144,4096]{1,0:T(8,128)(2,1)S(1)} %fusion.11, bf16[4096,128]{1,0:T(8,128)(2,1)} %collective-permute-done.4), kind=kOutput, calls=%fused_computation.147 | convolution fusion | flops 150994944 | bytes 2301952 | tf_op jit(solution)/shard_map/dot_general | solution.py:79
  62.5 1.5 concatenate.54
  64.1 1.7 fusion.67
  65.8 1.0 fusion.47
  67.0 7.2 %all-to-all-start.2 = ((bf16[16,24,4096]{2,1,0:T(8,128)(2,1)}), bf16[16,24,4096]{2,1,0:T(8,128)(2,1)}, u32[]{:S(2)}, u32[]{:S(2)}) async-start(bf16[16,24,4096]{2,1,0:T(8,128)(2,1)} %bitcast.66), calls=%async_computation.3 | async-start | bytes 6291456 | tf_op jit(solution)/shard_map/all_to_all | solution.py:150
  74.3 3.3 %fusion.17 = f32[128,512]{1,0:T(8,128)S(1)} fusion(bf16[16,8,4096]{2,1,0:T(8,128)(2,1)} %all-to-all-done, bf16[4096,128]{1,0:T(8,128)(2,1)} %collective-permute-done.6, bf16[4096,128]{1,0:T(8,128)(2,1)} %bitcast.83, bf16[4096,128]{1,0:T(8,128)(2,1)} %collective-permute-done.5, bf16[4096,128]{1,0:T(8,128)(2,1)} %bitcast.86), kind=kOutput, calls=%fused_computation.36 | convolution fusion | flops 553648128 | bytes 5505024 | tf_op jit(solution)/shard_map/dot_general | solution.py:153
  77.7 4.2 %convolution_convert_fusion.2 = bf16[256,4096]{1,0:T(8,128)(2,1)} fusion(bf16[256,512]{1,0:T(8,128)(2,1)S(1)} %bitcast.76, bf16[128,4096]{1,0:T(8,128)(2,1)} %collective-permute-done.8, bf16[128,4096]{1,0:T(8,128)(2,1)S(1)} %copy-done.15, bf16[128,4096]{1,0:T(8,128)(2,1)} %collective-permute-done.7, bf16[128,4096]{1,0:T(8,128)(2,1)S(1)} %bitcast.70), kind=kOutput, calls=%fused_computation.10 | convolution fusion | flops 1091567616 | bytes 6553600 | tf_op jit(solution)/shard_map/dot_general | solution.py:185
  81.9 36.3 %all-to-all-done.2 = bf16[16,24,4096]{2,1,0:T(8,128)(2,1)} async-done(((bf16[16,24,4096]{2,1,0:T(8,128)(2,1)}), bf16[16,24,4096]{2,1,0:T(8,128)(2,1)}, u32[]{:S(2)}, u32[]{:S(2)}) %all-to-all-start.2) | async-done | bytes 3145760 | tf_op jit(solution)/shard_map/all_to_all | solution.py:150
  118.2 5.0 %fusion.19 = f32[384,512]{1,0:T(8,128)S(1)} fusion(bf16[384,4096]{1,0:T(8,128)(2,1)} %bitcast.16, bf16[4096,128]{1,0:T(8,128)(2,1)} %collective-permute-done.6, bf16[4096,128]{1,0:T(8,128)(2,1)} %bitcast.84, bf16[4096,128]{1,0:T(8,128)(2,1)} %collective-permute-done.5, bf16[4096,128]{1,0:T(8,128)(2,1)} %bitcast.87), kind=kOutput, calls=%fused_computation.39 | convolution fusion | flops 1627389952 | bytes 8126464 | tf_op jit(solution)/shard_map/dot_general | solution.py:153
  123.2 0.1 fusion.35
  123.4 3.9 %convolution_convert_fusion = bf16[384,4096]{1,0:T(8,128)(2,1)} fusion(bf16[384,256]{1,0:T(8,128)(2,1)S(1)} %bitcast.72, bf16[128,4096]{1,0:T(8,128)(2,1)} %collective-permute-done.7, bf16[128,4096]{1,0:T(8,128)(2,1)S(1)} %bitcast.71), kind=kOutput, calls=%fused_computation.8 | convolution fusion | flops 811073536 | bytes 5439488 | tf_op jit(solution)/shard_map/dot_general | solution.py:193
  127.3 0.7 add_select_fusion.3
  128.0 0.1 copy.40
  128.1 0.1 copy.39
  128.2 0.8 fusion.56
  129.0 0.2 fusion.64
  129.2 0.2 fusion.44
  129.4 0.2 select_reduce_fusion.2
  129.6 1.6 slice_bitcast_fusion
  131.3 0.7 copy.44
  131.9 8.6 %all-to-all-start.1 = ((bf16[16,32,128]{2,1,0:T(8,128)(2,1)}), bf16[16,32,128]{2,1,0:T(8,128)(2,1)S(1)}, u32[]{:S(2)}, u32[]{:S(2)}) async-start(bf16[16,32,128]{2,1,0:T(8,128)(2,1)} %bitcast.23), calls=%async_computation.2 | async-start | bytes 262144 | tf_op jit(solution)/shard_map/all_to_all | solution.py:150
  140.6 38.0 %reduce-scatter.5.cloned.1.call-done = bf16[48,4096]{1,0:T(8,128)(2,1)} async-done(((bf16[384,4096]{1,0:T(8,128)(2,1)}), bf16[48,4096]{1,0:T(8,128)(2,1)}) %reduce-scatter.5.cloned.1.call-update) | async-done | bytes 393232 | tf_op jit(solution)/shard_map/reduce_scatter | solution.py:196
  178.6 1.9 reshape.212
  180.5 7.3 %all-to-all-start.3 = ((bf16[16,96,128]{2,1,0:T(8,128)(2,1)}), bf16[16,96,128]{2,1,0:T(8,128)(2,1)S(1)}, u32[]{:S(2)}, u32[]{:S(2)}) async-start(bf16[16,96,128]{2,1,0:T(8,128)(2,1)} %reshape.212), calls=%async_computation.5 | async-start | bytes 786432 | tf_op jit(solution)/shard_map/all_to_all | solution.py:150
  187.9 0.1 copy.38
  188.1 0.3 fusion.36
  188.3 7.5 %all-to-all-done.3 = bf16[16,96,128]{2,1,0:T(8,128)(2,1)S(1)} async-done(((bf16[16,96,128]{2,1,0:T(8,128)(2,1)}), bf16[16,96,128]{2,1,0:T(8,128)(2,1)S(1)}, u32[]{:S(2)}, u32[]{:S(2)}) %all-to-all-start.3) | async-done | bytes 393248 | tf_op jit(solution)/shard_map/all_to_all | solution.py:150
  195.9 0.2 reshape.213
  196.1 0.9 fusion.1
  (70 shorter events, 0.9 us)
Async XLA Ops:
  7.2 122.1 %copy-start = (bf16[4096,16]{0,1:T(8,128)(2,1)S(1)}, bf16[4096,16]{0,1:T(8,128)(2,1)}, u32[]{:S(2)}) copy-start(bf16[4096,16]{0,1:T(8,128)(2,1)} %param.25) | copy-start | bytes 393220
  7.2 22.2 %collective-permute-start.2 = (f32[3,128]{1,0:T(4,128)}, f32[3,128]{1,0:T(4,128)S(1)}, u32[]{:S(2)}, u32[]{:S(2)}) collective-permute-start(f32[3,128]{1,0:T(4,128)} %param.20), channel_id=1, source_target_pairs={{0,1},{1,0},{2,3},{3,2},{4,5},{5,4},{6,7},{7,6},{8,9},{9,8},{10,11... | collective-permute-start | bytes 4616 | tf_op jit(solution)/shard_map/ppermute | solution.py:52
  8.1 21.9 %collective-permute-start = (bf16[2,4096]{1,0:T(2,128)(2,1)S(1)}, bf16[2,4096]{1,0:T(2,128)(2,1)S(1)}, u32[]{:S(2)}, u32[]{:S(2)}) collective-permute-start(bf16[2,4096]{1,0:T(2,128)(2,1)S(1)} %slice.61), channel_id=1, source_target_pairs={{0,16},{16,32},{32,48},{48,64},{64,80},{80,96},{96,112},{112,128},... | collective-permute-start | bytes 49160 | tf_op jit(solution)/shard_map/ppermute | solution.py:121
  11.6 62.7 %collective-permute-start.5 = (bf16[4096,128]{1,0:T(8,128)(2,1)}, bf16[4096,128]{1,0:T(8,128)(2,1)}, u32[]{:S(2)}, u32[]{:S(2)}) collective-permute-start(bf16[4096,128]{1,0:T(8,128)(2,1)} %bitcast.85), channel_id=1, source_target_pairs={{0,1},{1,0},{2,3},{3,2},{4,5},{5,4},{6,7},{7,6},{8,9},{9,8},{10,11... | collective-permute-start | bytes 3145736 | tf_op jit(solution)/shard_map/ppermute | solution.py:52
  11.9 62.4 %collective-permute-start.6 = (bf16[4096,128]{1,0:T(8,128)(2,1)}, bf16[4096,128]{1,0:T(8,128)(2,1)}, u32[]{:S(2)}, u32[]{:S(2)}) collective-permute-start(bf16[4096,128]{1,0:T(8,128)(2,1)} %bitcast.82), channel_id=1, source_target_pairs={{0,1},{1,0},{2,3},{3,2},{4,5},{5,4},{6,7},{7,6},{8,9},{9,8},{10,11... | collective-permute-start | bytes 3145736 | tf_op jit(solution)/shard_map/ppermute | solution.py:52
  12.2 47.5 %collective-permute-start.4 = (bf16[4096,128]{1,0:T(8,128)(2,1)}, bf16[4096,128]{1,0:T(8,128)(2,1)}, u32[]{:S(2)}, u32[]{:S(2)}) collective-permute-start(bf16[4096,128]{1,0:T(8,128)(2,1)} %param.17), channel_id=1, source_target_pairs={{0,1},{1,0},{2,3},{3,2},{4,5},{5,4},{6,7},{7,6},{8,9},{9,8},{10,11... | collective-permute-start | bytes 3145736 | tf_op jit(solution)/shard_map/ppermute | solution.py:52
  13.4 3.7 %copy-start.5 = (s32[8,1,16,2]{3,2,0,1:T(8,128)}, s32[8,1,16,2]{3,2,0,1:T(8,128)S(1)}, u32[]{:S(2)}) copy-start(s32[8,1,16,2]{3,2,0,1:T(8,128)S(1)} %copy.36) | copy-start | bytes 3076
  13.4 4.4 %copy-start.9 = (f32[4096]{0:T(1024)S(1)}, f32[4096]{0:T(1024)}, u32[]{:S(2)}) copy-start(f32[4096]{0:T(1024)} %param.23) | copy-start | bytes 49156
  16.9 0.6 copy-start.6
  18.1 8.6 %copy-start.14 = (f32[3,128]{1,0:T(4,128)S(1)}, f32[3,128]{1,0:T(4,128)}, u32[]{:S(2)}) copy-start(f32[3,128]{1,0:T(4,128)} %param.20) | copy-start | bytes 4612
  19.5 47.4 %all-to-all-start = ((bf16[16,8,4096]{2,1,0:T(8,128)(2,1)}), bf16[16,8,4096]{2,1,0:T(8,128)(2,1)}, u32[]{:S(2)}, u32[]{:S(2)}) async-start(bf16[16,8,4096]{2,1,0:T(8,128)(2,1)} %fusion), calls=%async_computation | async-start | bytes 2097152 | tf_op jit(solution)/shard_map/all_to_all | solution.py:150
  26.7 3.8 %copy-start.1 = (bf16[256,4096]{1,0:T(8,128)(2,1)S(1)}, bf16[256,4096]{1,0:T(8,128)(2,1)}, u32[]{:S(2)}) copy-start(bf16[256,4096]{1,0:T(8,128)(2,1)} %param.15) | copy-start | bytes 6291460
  29.4 26.4 %collective-permute-start.3 = (bf16[4096,128]{1,0:T(8,128)(2,1)}, bf16[4096,128]{1,0:T(8,128)(2,1)}, u32[]{:S(2)}, u32[]{:S(2)}) collective-permute-start(bf16[4096,128]{1,0:T(8,128)(2,1)} %param.18), channel_id=1, source_target_pairs={{0,1},{1,0},{2,3},{3,2},{4,5},{5,4},{6,7},{7,6},{8,9},{9,8},{10,11... | collective-permute-start | bytes 3145736 | tf_op jit(solution)/shard_map/ppermute | solution.py:52
  30.0 34.1 %collective-permute-start.1 = (bf16[4096,128]{1,0:T(8,128)(2,1)}, bf16[4096,128]{1,0:T(8,128)(2,1)}, u32[]{:S(2)}, u32[]{:S(2)}) collective-permute-start(bf16[4096,128]{1,0:T(8,128)(2,1)} %param.19), channel_id=1, source_target_pairs={{0,1},{1,0},{2,3},{3,2},{4,5},{5,4},{6,7},{7,6},{8,9},{9,8},{10,11... | collective-permute-start | bytes 3145736 | tf_op jit(solution)/shard_map/ppermute | solution.py:52
  32.8 15.1 %copy-start.10 = (f32[4096]{0:T(1024)S(1)}, f32[4096]{0:T(1024)}, u32[]{:S(2)}) copy-start(f32[4096]{0:T(1024)} %param.16) | copy-start | bytes 49156
  47.6 1.2 copy-start.3
  48.8 2.0 copy-start.2
  51.9 3.9 %copy-start.4 = (bf16[1,128,4096]{2,1,0:T(8,128)(2,1)S(1)}, bf16[1,128,4096]{2,1,0:T(8,128)(2,1)}, u32[]{:S(2)}) copy-start(bf16[1,128,4096]{2,1,0:T(8,128)(2,1)} %param.29) | copy-start | bytes 3145732
  55.8 21.8 %collective-permute-start.7 = (bf16[128,4096]{1,0:T(8,128)(2,1)S(1)}, bf16[128,4096]{1,0:T(8,128)(2,1)}, u32[]{:S(2)}, u32[]{:S(2)}) collective-permute-start(bf16[128,4096]{1,0:T(8,128)(2,1)S(1)} %bitcast.69), channel_id=1, source_target_pairs={{0,1},{1,0},{2,3},{3,2},{4,5},{5,4},{6,7},{7,6},{8,9},{9,8},{10,11... | collective-permute-start | bytes 3145736 | tf_op jit(solution)/shard_map/ppermute | solution.py:52
  59.7 18.0 %collective-permute-start.8 = (bf16[128,4096]{1,0:T(8,128)(2,1)}, bf16[128,4096]{1,0:T(8,128)(2,1)}, u32[]{:S(2)}, u32[]{:S(2)}) collective-permute-start(bf16[128,4096]{1,0:T(8,128)(2,1)} %param.21), channel_id=1, source_target_pairs={{0,1},{1,0},{2,3},{3,2},{4,5},{5,4},{6,7},{7,6},{8,9},{9,8},{10,11... | collective-permute-start | bytes 3145736 | tf_op jit(solution)/shard_map/ppermute | solution.py:52
  62.5 4.3 %copy-start.11 = (f32[1,256]{1,0:T(1,128)S(1)}, f32[1,256]{1,0:T(1,128)}, u32[]{:S(2)}) copy-start(f32[1,256]{1,0:T(1,128)} %get-tuple-element.33) | copy-start | bytes 3076
  62.5 4.4 %copy-start.12 = (f32[1,256]{1,0:T(1,128)S(1)}, f32[1,256]{1,0:T(1,128)}, u32[]{:S(2)}) copy-start(f32[1,256]{1,0:T(1,128)} %get-tuple-element.34) | copy-start | bytes 3076
  62.5 4.4 %copy-start.13 = (f32[1,256]{1,0:T(1,128)S(1)}, f32[1,256]{1,0:T(1,128)}, u32[]{:S(2)}) copy-start(f32[1,256]{1,0:T(1,128)} %get-tuple-element.35) | copy-start | bytes 3076
  64.1 1.7 copy-start.7
  67.0 51.3 %all-to-all-start.2 = ((bf16[16,24,4096]{2,1,0:T(8,128)(2,1)}), bf16[16,24,4096]{2,1,0:T(8,128)(2,1)}, u32[]{:S(2)}, u32[]{:S(2)}) async-start(bf16[16,24,4096]{2,1,0:T(8,128)(2,1)} %bitcast.66), calls=%async_computation.3 | async-start | bytes 6291456 | tf_op jit(solution)/shard_map/all_to_all | solution.py:150
  74.2 55.4 %reduce-scatter.3.cloned.1.call-start = ((), (), s32[]{:S(2)}) async-start(), calls=%async_computation.6 | async-start | bytes 2359296 | tf_op jit(solution)/shard_map/reduce_scatter | solution.py:189
  74.2 3.5 %copy-start.15 = (bf16[128,4096]{1,0:T(8,128)(2,1)S(1)}, bf16[128,4096]{1,0:T(8,128)(2,1)}, u32[]{:S(2)}) copy-start(bf16[128,4096]{1,0:T(8,128)(2,1)} %param.21) | copy-start | bytes 3145732
  81.9 96.7 %reduce-scatter.5.cloned.1.call-start = ((), (), s32[]{:S(2)}) async-start(), calls=%async_computation.7 | async-start | bytes 3538944 | tf_op jit(solution)/shard_map/reduce_scatter | solution.py:196
  127.3 1.7 copy-start.8
  131.9 48.6 %all-to-all-start.1 = ((bf16[16,32,128]{2,1,0:T(8,128)(2,1)}), bf16[16,32,128]{2,1,0:T(8,128)(2,1)S(1)}, u32[]{:S(2)}, u32[]{:S(2)}) async-start(bf16[16,32,128]{2,1,0:T(8,128)(2,1)} %bitcast.23), calls=%async_computation.2 | async-start | bytes 262144 | tf_op jit(solution)/shard_map/all_to_all | solution.py:150
  180.5 15.4 %all-to-all-start.3 = ((bf16[16,96,128]{2,1,0:T(8,128)(2,1)}), bf16[16,96,128]{2,1,0:T(8,128)(2,1)S(1)}, u32[]{:S(2)}, u32[]{:S(2)}) async-start(bf16[16,96,128]{2,1,0:T(8,128)(2,1)} %reshape.212), calls=%async_computation.5 | async-start | bytes 786432 | tf_op jit(solution)/shard_map/all_to_all | solution.py:150
Sparse Core Ops, SparseCore 0:
  82.0 45.3 reduce-scatter.2
  130.0 48.5 reduce-scatter.4

commit v3 on v2

v3 whole, which is shorter than its diff:
```python
import functools

import jax
import jax.numpy as jnp
from jax import lax
from jax.experimental import pallas as pl
from jax.experimental.pallas import tpu as pltpu
from jax.sharding import Mesh
from jax.sharding import PartitionSpec as P


TAPS = 3
EXPERTS = 16
GROUPS = 4
TOPK = 2
MOE_SHARE = 16
EPG = 4
CAP = 4

EP = ("y", "x")
TP = ("z", "core")
ALL = EP + TP


def route_weights(normed, routes, router_group, router_expert):
    group_logit = jnp.dot(normed, router_group, preferred_element_type=jnp.float32)
    expert_logit = jnp.dot(normed, router_expert, preferred_element_type=jnp.float32)
    group_exp = jnp.exp(group_logit)
    group_id = routes[:, 0] // EPG
    group_pick = (group_id[:, None] == jnp.arange(GROUPS, dtype=jnp.int32)[None, :]).astype(
        jnp.float32
    )
    group_gate = jnp.sum(group_exp * group_pick, axis=1) / jnp.sum(group_exp, axis=1)
    expert_pick = (
        routes[:, :, None] == jnp.arange(EXPERTS, dtype=jnp.int32)[None, None, :]
    ).astype(jnp.float32)
    chosen = jnp.exp(jnp.sum(expert_logit[:, None, :] * expert_pick, axis=2))
    return group_gate[:, None] * chosen / jnp.sum(chosen, axis=1, keepdims=True)


def swap_cores(value):
    return lax.ppermute(value, "core", [(0, 1), (1, 0)])


def iota(shape, dim):
    return lax.broadcasted_iota(jnp.int32, shape, dim)


def select_matrix(mask):
    return jnp.where(mask, 1.0, 0.0).astype(jnp.bfloat16)


def product(left, right):
    return jnp.dot(left, right, preferred_element_type=jnp.float32)


def scaled_rows(rows, gain):
    values = rows.astype(jnp.float32)
    inverse = lax.rsqrt(jnp.mean(values * values, axis=-1, keepdims=True) + 1e-06)
    return (values * inverse * gain).astype(jnp.bfloat16)


def prep_kernel(zs, core_ref, tokens_ref, gain_ref, routes_ref, first_ref, late_ref, normed_ref, ranks_ref):
    share = MOE_SHARE
    rows = zs * share
    width = tokens_ref.shape[-1]
    normed_ref[...] = scaled_rows(tokens_ref[...].reshape(rows, width), gain_ref[...])
    token = iota((2 * rows, rows), 1)
    source = (token // share) * (2 * share) + core_ref[0] * share + token % share
    pick = select_matrix(iota((2 * rows, rows), 0) == source)
    routes = product(routes_ref[...].astype(jnp.float32).astype(jnp.bfloat16), pick).astype(jnp.int32)
    expert = iota((EXPERTS, rows), 0)
    named = [expert == routes[k : k + 1] for k in range(TOPK)]
    earlier, later = iota((rows, rows), 0), iota((rows, rows), 1)
    before = (earlier // share == later // share) & (earlier < later)
    counts = product(select_matrix(named[0] | named[1]), select_matrix(before))
    ranks = [
        jnp.sum(jnp.where(named[k], counts, 0.0), axis=0, keepdims=True).astype(jnp.int32)
        for k in range(TOPK)
    ]
    block = iota((1, rows), 1) // share
    late = CAP - 1
    slots_first = iota((EXPERTS * zs, rows), 0)
    slots_late = iota((EXPERTS * late * zs, rows), 0)
    in_first, in_late = [], []
    for k in range(TOPK):
        ranks_ref[k : k + 1, :] = ranks[k]
        chosen = routes[k : k + 1]
        spot = jnp.where(ranks[k] == 0, chosen * zs + block, -1)
        in_first.append(slots_first == spot)
        spot = jnp.where(ranks[k] > 0, (chosen * late + ranks[k] - 1) * zs + block, -1)
        in_late.append(slots_late == spot)
    select_first = select_matrix(in_first[0] | in_first[1])
    select_late = select_matrix(in_late[0] | in_late[1])
    step = 512

    @pl.loop(0, width // step)
    def _(index):
        columns = pl.ds(pl.multiple_of(index * step, step), step)
        piece = normed_ref[:, columns]
        first_ref[:, columns] = product(select_first, piece).astype(jnp.bfloat16)
        late_ref[:, columns] = product(select_late, piece).astype(jnp.bfloat16)


def prepare(core, tokens, gain, routes, zs):
    rows, width = tokens.shape
    half = rows // 2
    late = CAP - 1
    return pl.pallas_call(
        functools.partial(prep_kernel, zs),
        grid_spec=pltpu.PrefetchScalarGridSpec(
            num_scalar_prefetch=1,
            grid=(1,),
            in_specs=[
                pl.BlockSpec((zs, 1, MOE_SHARE, width), lambda i, c: (0, c[0], 0, 0)),
                pl.BlockSpec((1, width), lambda i, c: (0, 0)),
                pl.BlockSpec((TOPK, rows), lambda i, c: (0, 0)),
            ],
            out_specs=[
                pl.BlockSpec((EXPERTS * zs, width), lambda i, c: (0, 0)),
                pl.BlockSpec((EXPERTS * late * zs, width), lambda i, c: (0, 0)),
                pl.BlockSpec((half, width), lambda i, c: (0, 0)),
                pl.BlockSpec((TOPK, half), lambda i, c: (0, 0)),
            ],
        ),
        out_shape=[
            jax.ShapeDtypeStruct((EXPERTS * zs, width), jnp.bfloat16),
            jax.ShapeDtypeStruct((EXPERTS * late * zs, width), jnp.bfloat16),
            jax.ShapeDtypeStruct((half, width), jnp.bfloat16),
            jax.ShapeDtypeStruct((TOPK, half), jnp.int32),
        ],
        cost_estimate=pl.CostEstimate(
            flops=2 * EXPERTS * CAP * zs * half * width,
            bytes_accessed=2 * width * (rows + EXPERTS * CAP * zs),
            transcendentals=0,
        ),
        name="prepare",
    )(
        core,
        tokens.reshape(zs, 2, MOE_SHARE, width),
        gain.reshape(1, width),
        routes.T,
    )


def mixer_kernel(
    core_ref, tokens_ref, halo_ref, before_ref, gain_ref, taps_mine, taps_theirs, *refs
):
    weights, (out_ref, normed_ref, sums_ref) = refs[:6], refs[6:]
    step = pl.program_id(0)
    last = pl.num_programs(0) - 1
    rows, _ = out_ref.shape
    depth = weights[0].shape[0]
    width = tokens_ref.shape[-1]
    blocks, _, tail_rows, _ = halo_ref.shape
    halos = blocks * tail_rows
    total = normed_ref.shape[0]
    reach = TAPS - 1

    @pl.when(step == 0)
    def _():
        gain = gain_ref[...]
        normed_ref[0:rows, :] = scaled_rows(tokens_ref[...].reshape(rows, width), gain)
        normed_ref[rows : rows + halos, :] = scaled_rows(halo_ref[...].reshape(halos, width), gain)
        normed_ref[rows + halos :, :] = scaled_rows(before_ref[...], gain)
        sums_ref[...] = jnp.zeros_like(sums_ref)

    piece = normed_ref[:, pl.ds(pl.multiple_of(step * depth, depth), depth)]
    for index in range(6):
        sums_ref[index] += product(piece, weights[index][...])

    @pl.when(step == last)
    def _():
        def pair(index):
            return jnp.concatenate([sums_ref[index], sums_ref[index + 1]], axis=1)

        gated = (pair(2) * pair(0)).astype(jnp.bfloat16)
        row, source = iota((rows, total), 0), iota((rows, total), 1)
        place = row % MOE_SHARE
        ahead = row // MOE_SHARE + core_ref[0]
        tail = jnp.where(ahead == 0, total, rows + ahead * tail_rows)
        taps = jnp.concatenate([taps_mine[...], taps_theirs[...]], axis=1)
        mixed = None
        for tap in range(TAPS):
            back = reach - tap
            wanted = jnp.where(place >= back, row, tail + place) - back
            shifted = product(select_matrix(source == wanted), gated)
            term = taps[tap : tap + 1] * shifted
            mixed = term if mixed is None else mixed + term
        out_ref[...] = (pair(4)[0:rows] * mixed).astype(jnp.bfloat16)


def mixer_channels(core, tokens, before, gain, taps, weights, zs):
    rows, width = tokens.shape
    half = rows // 2
    channels = weights[0].shape[1]
    depth = 512
    tail_rows = MOE_SHARE // 2
    total = half + zs * tail_rows + before.shape[0]
    fixed = lambda i, c: (0, 0)
    split = tokens.reshape(zs, 2, MOE_SHARE, width)
    return pl.pallas_call(
        mixer_kernel,
        grid_spec=pltpu.PrefetchScalarGridSpec(
            num_scalar_prefetch=1,
            grid=(width // depth,),
            in_specs=[
                pl.BlockSpec((zs, 1, MOE_SHARE, width), lambda i, c: (0, c[0], 0, 0)),
                pl.BlockSpec((zs, 1, tail_rows, width), lambda i, c: (0, 1 - c[0], 1, 0)),
                pl.BlockSpec(before.shape, fixed),
                pl.BlockSpec((1, width), fixed),
                pl.BlockSpec((TAPS, channels), fixed),
                pl.BlockSpec((TAPS, channels), fixed),
            ]
            + [pl.BlockSpec((depth, channels), lambda i, c: (i, 0))] * 6,
            out_specs=pl.BlockSpec((half, 2 * channels), fixed),
            scratch_shapes=[
                pltpu.VMEM((total, width), jnp.bfloat16),
                pltpu.VMEM((6, total, channels), jnp.float32),
            ],
        ),
        out_shape=jax.ShapeDtypeStruct((half, 2 * channels), jnp.bfloat16),
        cost_estimate=pl.CostEstimate(
            flops=2 * (total) * width * 6 * channels,
            bytes_accessed=2 * width * (total + 6 * channels),
            transcendentals=0,
        ),
        name="mixer",
    )(core, split, split, before, gain.reshape(1, width), *taps, *weights)


def expert_kernel(zs, steps, joined, rows_ref, g0, g1, u0, u1, d0, d1, *refs):
    if joined:
        channels_ref, m0, m1, out_ref, sums_ref, units_ref, mixed_ref = refs
    else:
        out_ref, sums_ref, units_ref = refs
    step = pl.program_id(0)
    count = rows_ref.shape[0]
    given = out_ref.shape[0]
    half = g0.shape[1]

    @pl.when(step == 0)
    def _():
        sums_ref[...] = jnp.zeros_like(sums_ref)

    @pl.when(step < steps)
    def _():
        for index, weight in enumerate((g0, g1, u0, u1)):
            sums_ref[index] += product(rows_ref[...], weight[...])

    @pl.when(step == steps - 1)
    def _():
        target, source = iota((given, count), 0), iota((given, count), 1)
        order = select_matrix(target == (source % zs) * (given // zs) + source // zs)
        for index in range(2):
            gate, up = sums_ref[index], sums_ref[index + 2]
            hidden = (gate * jax.nn.sigmoid(gate) * up).astype(jnp.bfloat16)
            units_ref[:, index * half : (index + 1) * half] = product(order, hidden).astype(
                jnp.bfloat16
            )
        if joined:
            rows = channels_ref.shape[0]
            target, source = iota((given, rows), 0), iota((given, rows), 1)
            place = (source // MOE_SHARE + 1) * (given // zs) - MOE_SHARE + source % MOE_SHARE
            mixed_ref[...] = product(
                select_matrix(target == place), channels_ref[...]
            ).astype(jnp.bfloat16)

    @pl.when(step >= steps)
    def _():
        total = product(units_ref[:, :half], d0[...]) + product(units_ref[:, half:], d1[...])
        if joined:
            total = total + (
                product(mixed_ref[:, :half], m0[...]) + product(mixed_ref[:, half:], m1[...])
            )
        out_ref[...] = total.astype(jnp.bfloat16)


def expert_partial(rows, weights, downs, zs, channels=None, mixes=()):
    count, width = rows.shape
    half = weights[0].shape[1]
    depth = 512
    steps = width // depth
    joined = channels is not None
    given = count + (channels.shape[0] if joined else 0)
    early = lambda i: jnp.minimum(i, steps - 1)
    after = lambda i: jnp.maximum(i - steps, 0)
    in_specs = [pl.BlockSpec((count, depth), lambda i: (0, early(i)))]
    in_specs += [pl.BlockSpec((depth, half), lambda i: (early(i), 0))] * 4
    in_specs += [pl.BlockSpec((half, depth), lambda i: (0, after(i)))] * 2
    scratch = [
        pltpu.VMEM((4, count, half), jnp.float32),
        pltpu.VMEM((given, 2 * half), jnp.bfloat16),
    ]
    operands = (rows, *weights, *downs)
    if joined:
        in_specs += [pl.BlockSpec(channels.shape, lambda i: (0, 0))]
        in_specs += [pl.BlockSpec((half, depth), lambda i: (0, after(i)))] * 2
        scratch += [pltpu.VMEM((given, 2 * half), jnp.bfloat16)]
        operands += (channels, *mixes)
    return pl.pallas_call(
        functools.partial(expert_kernel, zs, steps, joined),
        grid=(2 * steps,),
        in_specs=in_specs,
        out_specs=pl.BlockSpec((given, depth), lambda i: (0, after(i))),
        scratch_shapes=scratch,
        out_shape=jax.ShapeDtypeStruct((given, width), jnp.bfloat16),
        cost_estimate=pl.CostEstimate(
            flops=2 * width * half * (4 * count + 2 * given),
            bytes_accessed=2 * width * (count + given + 6 * half),
            transcendentals=2 * count * half,
        ),
        name="experts_joined" if joined else "experts",
    )(*operands)


def layer(
    mix_tokens,
    mix_gain,
    value_weight,
    inner_weight,
    outer_weight,
    conv_taps,
    mix_weight,
    moe_tokens,
    moe_gain,
    router_group,
    router_expert,
    expert_routes,
    gate_weight,
    up_weight,
    down_weight,
):
    z_index = lax.axis_index("z")
    core = lax.axis_index("core")
    zs = lax.axis_size("z")
    eps = lax.axis_size(EP)
    width = moe_tokens.shape[1]
    core_ref = core.reshape(1).astype(jnp.int32)

    before = lax.ppermute(
        mix_tokens[mix_tokens.shape[0] - MOE_SHARE :], EP, [(i, i + 1) for i in range(eps - 1)]
    )
    gate, up, down = gate_weight[0], up_weight[0], down_weight[0]

    placed_first, placed_late, half_normed, half_ranks = prepare(
        core_ref, moe_tokens, moe_gain, expert_routes, zs
    )

    def exchange(array):
        return lax.all_to_all(array, EP, split_axis=0, concat_axis=0, tiled=True)

    late = CAP - 1
    arrived_first = exchange(placed_first.reshape(EXPERTS, zs, width))
    arrived_late = exchange(placed_late.reshape(EXPERTS, late * zs, width))

    taps = (conv_taps, swap_cores(conv_taps))
    projections = (
        value_weight,
        swap_cores(value_weight),
        inner_weight,
        swap_cores(inner_weight),
        outer_weight,
        swap_cores(outer_weight),
    )
    channels = mixer_channels(core_ref, mix_tokens, before, mix_gain, taps, projections, zs)
    arrived_first, channels = lax.optimization_barrier((arrived_first, channels))

    weights = (gate, swap_cores(gate), up, swap_cores(up))
    downs = (down, swap_cores(down))
    mixes = (mix_weight, swap_cores(mix_weight))
    partial_first = expert_partial(
        arrived_first.reshape(-1, width), weights, downs, zs, channels, mixes
    )
    arrived_late, _ = lax.optimization_barrier((arrived_late, partial_first))
    summed_first = lax.psum_scatter(partial_first, "z", scatter_dimension=0, tiled=True)
    mixer_out = summed_first[eps:]

    partial_late = expert_partial(arrived_late.reshape(-1, width), weights, downs, zs)
    summed_late = lax.psum_scatter(partial_late, "z", scatter_dimension=0, tiled=True)

    own_routes = lax.dynamic_slice_in_dim(
        expert_routes, (2 * z_index + core) * MOE_SHARE, MOE_SHARE, 0
    )
    own_normed = lax.dynamic_slice_in_dim(half_normed, z_index * MOE_SHARE, MOE_SHARE, 0)
    own_ranks = lax.dynamic_slice_in_dim(half_ranks, z_index * MOE_SHARE, MOE_SHARE, 1).T
    token_weights = route_weights(own_normed, own_routes, router_group, router_expert)

    def combine(summed, first, count):
        returned = exchange(summed.reshape(eps, count * width // 128, 128)).reshape(-1, width)
        position = own_routes * count + own_ranks - first
        inside = (own_ranks >= first) & (own_ranks < first + count)
        position = jnp.where(inside, position, -1)
        targets = jnp.arange(EXPERTS * count, dtype=jnp.int32)
        spread = jnp.sum(
            jnp.where(position[:, :, None] == targets, token_weights[:, :, None], 0.0), axis=1
        )
        return jnp.dot(
            spread,
            returned.astype(jnp.float32),
            precision=lax.Precision.HIGHEST,
            preferred_element_type=jnp.float32,
        )

    expert_out = combine(summed_first[:eps], 0, 1) + combine(summed_late, 1, late)
    return (mixer_out, expert_out.astype(jnp.bfloat16))


def solution(mesh):
    torus = Mesh(mesh.devices.reshape(4, 4, 8, 2), ALL)
    return jax.shard_map(
        layer,
        mesh=torus,
        in_specs=(
            P(EP, None),
            P(),
            P(None, TP),
            P(None, TP),
            P(None, TP),
            P(None, TP),
            P(TP, None),
            P(EP, None),
            P(),
            P(),
            P(),
            P(EP, None),
            P(EP, None, TP),
            P(EP, None, TP),
            P(EP, TP, None),
        ),
        out_specs=(P(ALL, None), P(ALL, None)),
        check_vma=False,
    )
```

time: 206 us -> 196 us (0.951)
  Pallas kernels: 0 us -> 45 us
  blocking collectives: 0 us -> 44.4 us
  matrix products: 32.8 us -> 3.35 us
  waiting for transfers between devices: 81.9 us -> 54.3 us
  local copies, waits for them, and re-layouts: 29 us -> 8.61 us
  starting transfers between devices: 35.8 us -> 24.7 us
  other arithmetic: 9.88 us -> 0.52 us
    pallas_call x0 -> x4, Pallas kernels: none -> 45 us  [the longest x2 29 us: expert_partial(): pl.pallas_call(functools.partial(expert_kernel, zs, steps, joined), grid=...]
    all_to_all x0 -> x1, blocking collectives: none -> 44.4 us  [exchange(): return lax.all_to_all(array, EP, split_axis=0, concat_axis=0, tiled=True)]
    dot_general x12 -> x0, matrix products: 31.2 us -> none  [the longest x6 10.9 us: mixer_channels(): jnp.dot(normed, part, preferred_element_type=jnp.float32)]
    all_to_all x4 -> x3, waiting for transfers between devices: 43.8 us -> 14.4 us  [exchange(): return lax.all_to_all(array, EP, split_axis=0, concat_axis=0, tiled=True)]
    concatenate x6 -> x0, local copies, waits for them, and re-layouts: 20.3 us -> none  [the longest x1 14.7 us: mixer_channels(): normed = rms_rows(jnp.concatenate(windows, axis=0), mix_gain)]
    all_to_all x4 -> x3, starting transfers between devices: 30.4 us -> 19.4 us  [exchange(): return lax.all_to_all(array, EP, split_axis=0, concat_axis=0, tiled=True)]
    convert_element_type x5 -> x0, other arithmetic: 3.19 us -> none  [the longest x1 1.45 us: rms_rows(): values = inputs.astype(jnp.float32)]
    ppermute x8, waiting for transfers between devices: 0.02 us -> 2.51 us  [swap_cores(): return lax.ppermute(value, 'core', [(0, 1), (1, 0)])]
  transfers between devices with their start and end apart: 15 -> 14, of which waited for: 3 -> 5; matrix products, arithmetic and copies ran while one was open for 34% -> 4% of each run, Pallas kernels for 0% -> 16%
where the time goes in v3:
time: 196 us; the launch traced here: 195 us
  waiting for transfers between devices  54.3 us (28%)
  Pallas kernels  45 us (23%)
  blocking collectives  44.4 us (23%)
  starting transfers between devices  24.7 us (13%)
  between operations  14.2 us (7%)
  local copies, waits for them, and re-layouts  8.61 us (4%)
  matrix products  3.35 us (2%)
    all_to_all x1, blocking collectives, exchange(): return lax.all_to_all(array, EP, split_axis=0, concat_axis=0, tiled=True)  44.4 us
    reduce_scatter x1, waiting for transfers between devices, layer(): lax.psum_scatter(partial_late, 'z', scatter_dimension=0, tiled=True)  36.6 us
    pallas_call x2, Pallas kernels, expert_partial(): pl.pallas_call(functools.partial(expert_kernel, zs, steps, joined), grid=...  29 us
    all_to_all x3, starting transfers between devices, exchange(): return lax.all_to_all(array, EP, split_axis=0, concat_axis=0, tiled=True)  19.4 us
    all_to_all x3, waiting for transfers between devices, exchange(): return lax.all_to_all(array, EP, split_axis=0, concat_axis=0, tiled=True)  14.4 us
    pallas_call x1, Pallas kernels, mixer_channels(): pl.pallas_call(mixer_kernel, grid_spec=pltpu.PrefetchScalarGridSpec(num_s...  9.71 us
    pallas_call x1, Pallas kernels, prepare(): pl.pallas_call(functools.partial(prep_kernel, zs), grid_spec=pltpu.Prefet...  6.3 us
    unnamed x22, local copies, waits for them, and re-layouts  5.61 us
  transfers between devices with their start and end apart: 14, of which 5 were waited for; matrix products, arithmetic and copies ran while one was open for 4% of the time, Pallas kernels for 16%

profile of v3, /device:TPU:2, one launch (start us, length us, event | category | flops | bytes accessed | tf_op | source)
XLA Modules:
  0.0 195.2 jit_solution(2014268306112694465)
XLA Ops:
  7.2 0.0 copy-start
  7.2 0.1 collective-permute-start.2
  7.3 0.5 collective-permute-start.3
  7.8 0.9 slice.12
  8.7 3.4 %collective-permute-start = (bf16[16,4096]{1,0:T(8,128)(2,1)S(1)}, bf16[16,4096]{1,0:T(8,128)(2,1)S(1)}, u32[]{:S(2)}, u32[]{:S(2)}) collective-permute-start(bf16[16,4096]{1,0:T(8,128)(2,1)S(1)} %slice.12), channel_id=1, source_target_pairs={{0,16},{16,32},{32,48},{48,64},{64,80},{80,96},{96,112},{112,128},... | collective-permute-start | bytes 393224 | tf_op jit(solution)/shard_map/ppermute | solution.py:341
  12.1 0.1 collective-permute-start.4
  12.2 0.5 collective-permute-start.1
  12.7 2.5 %collective-permute-done.1.taps_theirs = f32[3,128]{1,0:T(4,128)S(1)} collective-permute-done((f32[3,128]{1,0:T(4,128)}, f32[3,128]{1,0:T(4,128)S(1)}, u32[]{:S(2)}, u32[]{:S(2)}) %collective-permute-start.1) | collective-permute-done | bytes 1568 | tf_op jit(solution)/shard_map/ppermute | solution.py:42
  15.2 0.1 collective-permute-start.5
  15.3 0.8 collective-permute-done.before_ref
  16.1 0.0 collective-permute-start.6
  16.1 0.0 collective-permute-done.2.refs_1_
  16.1 0.0 copy-start.4
  16.1 1.0 copy-done.4
  17.1 0.5 collective-permute-start.7
  17.6 0.0 collective-permute-done.3.refs_3_
  17.6 0.0 collective-permute-start.8
  17.6 6.3 %prepare.1 = (bf16[128,4096]{1,0:T(8,128)(2,1)}, bf16[384,4096]{1,0:T(8,128)(2,1)}, bf16[128,4096]{1,0:T(8,128)(2,1)}, s32[2,128]{1,0:T(2,128)}) custom-call(s32[1]{0:T(128)} %bitcast.core_ref, bf16[8,2,16,4096]{3,2,1,0:T(8,128)(2,1)} %bitcast.51, f32[1,4096]{1,0:T(1,128)} %bitcast.54, s32[2,256]{1,0:T(2,128)} %bitcast.56), custom_call_target="tpu_custom_call" | custom-call | flops 536870912 | bytes 6291456 | tf_op jit(solution)/shard_map/prepare/pallas_call | solution.py:109
  23.9 7.5 %all-to-all-start = ((bf16[16,8,4096]{2,1,0:T(8,128)(2,1)}), bf16[16,8,4096]{2,1,0:T(8,128)(2,1)}, u32[]{:S(2)}, u32[]{:S(2)}) async-start(bf16[16,8,4096]{2,1,0:T(8,128)(2,1)} %bitcast.52), calls=%async_computation | async-start | bytes 2097152 | tf_op jit(solution)/shard_map/all_to_all | solution.py:351
  31.4 0.0 reduce-scatter.3.cloned.1.call-start
  31.5 0.0 collective-permute-done.4.refs_5_
  31.5 0.0 copy-done.9
  31.5 0.0 copy-done.5
  31.5 9.7 %mixer.1.refs_0_ = bf16[128,256]{1,0:T(8,128)(2,1)} custom-call(s32[1]{0:T(128)} %bitcast.core_ref, bf16[8,2,16,4096]{3,2,1,0:T(8,128)(2,1)} %bitcast.39, bf16[8,2,16,4096]{3,2,1,0:T(8,128)(2,1)} %bitcast.40, bf16[16,4096]{1,0:T(8,128)(2,1)} %copy-done.5, f32[1,4096]{1,0:T(1,128)} %bitcast.55, f32[3,128]{1,0:T(4,128)} %taps_mine.1, f32[3,128]{1,0:T(4,128)} %copy-done.9, ...), custom_call_target="tpu_custom_call" | custom-call | flops 1308622848 | bytes 7995392 | tf_op jit(solution)/shard_map/mixer/pallas_call | solution.py:202
  41.2 6.7 %all-to-all-done = bf16[16,8,4096]{2,1,0:T(8,128)(2,1)} async-done(((bf16[16,8,4096]{2,1,0:T(8,128)(2,1)}), bf16[16,8,4096]{2,1,0:T(8,128)(2,1)}, u32[]{:S(2)}, u32[]{:S(2)}) %all-to-all-start) | async-done | bytes 1048608 | tf_op jit(solution)/shard_map/all_to_all | solution.py:351
  48.0 0.0 collective-permute-done.5.g1
  48.0 0.0 collective-permute-done.6.u1
  48.0 0.0 copy-start.2
  48.0 0.0 collective-permute-done.7.d1
  48.0 0.0 copy-start.3
  48.0 0.0 collective-permute-done.8.refs_2_
  48.0 0.9 copy-done.1
  48.9 0.4 copy-done.2
  49.3 0.3 copy-done.3
  49.6 13.9 %experts_joined.1 = bf16[256,4096]{1,0:T(8,128)(2,1)} custom-call(bf16[128,4096]{1,0:T(8,128)(2,1)} %bitcast.7.rows_ref, bf16[4096,128]{1,0:T(8,128)(2,1)} %bitcast.42, bf16[4096,128]{1,0:T(8,128)(2,1)} %copy-done.1, bf16[4096,128]{1,0:T(8,128)(2,1)} %bitcast.45, bf16[4096,128]{1,0:T(8,128)(2,1)} %copy-done.2, bf16[128,4096]{1,0:T(8,128)(2,1)} %bitcast.48, ...), custom_call_target="tpu_custom_call" | custom-call | flops 1073741824 | bytes 9437184 | tf_op jit(solution)/shard_map/experts_joined/pallas_call | solution.py:301
  63.5 0.0 reduce-scatter.3.cloned.1.call-update
  63.5 0.0 reduce-scatter.5.cloned.1.call-start
  63.6 44.4 %all_to_all.20 = bf16[16,24,4096]{2,1,0:T(8,128)(2,1)} all-to-all(bf16[16,24,4096]{2,1,0:T(8,128)(2,1)} %bitcast.50), channel_id=1, replica_groups=mesh['y'=4,'x'=4,'z'=8,'core'=2] {'y','x'}, dimensions={0} | all-to-all | bytes 6291456 | tf_op jit(solution)/shard_map/all_to_all | solution.py:351
  108.0 15.1 %experts.1 = bf16[384,4096]{1,0:T(8,128)(2,1)} custom-call(bf16[384,4096]{1,0:T(8,128)(2,1)} %bitcast.38, bf16[4096,128]{1,0:T(8,128)(2,1)} %bitcast.43, bf16[4096,128]{1,0:T(8,128)(2,1)} %copy-done.1, bf16[4096,128]{1,0:T(8,128)(2,1)} %bitcast.46, bf16[4096,128]{1,0:T(8,128)(2,1)} %copy-done.2, bf16[128,4096]{1,0:T(8,128)(2,1)} %bitcast.49, ...), custom_call_target="tpu_custom_call" | custom-call | flops 2415919104 | bytes 12582912 | tf_op jit(solution)/shard_map/experts/pallas_call | solution.py:301
  123.1 0.0 copy-start.6
  123.2 0.0 reduce-scatter.5.cloned.1.call-update
  123.2 0.6 copy-done.7
  123.8 0.0 copy-done.8
  123.8 0.1 and_select_fusion
  123.9 0.0 copy-done.6
  123.9 1.1 fusion.11
  125.0 0.0 copy-done
  125.0 1.1 fusion.4
  126.1 0.2 select_reduce_fusion.2
  126.3 0.0 reduce-scatter.3.cloned.1.call-done
  126.4 1.6 slice_bitcast_fusion
  128.0 0.7 copy.20
  128.7 4.7 %all-to-all-start.1 = ((bf16[16,32,128]{2,1,0:T(8,128)(2,1)}), bf16[16,32,128]{2,1,0:T(8,128)(2,1)S(1)}, u32[]{:S(2)}, u32[]{:S(2)}) async-start(bf16[16,32,128]{2,1,0:T(8,128)(2,1)} %bitcast.16), calls=%async_computation.2 | async-start | bytes 262144 | tf_op jit(solution)/shard_map/all_to_all | solution.py:351
  133.4 0.1 and_select_fusion.2
  133.5 36.6 %reduce-scatter.5.cloned.1.call-done = bf16[48,4096]{1,0:T(8,128)(2,1)} async-done(((bf16[384,4096]{1,0:T(8,128)(2,1)}), bf16[48,4096]{1,0:T(8,128)(2,1)}) %reduce-scatter.5.cloned.1.call-update) | async-done | bytes 393232 | tf_op jit(solution)/shard_map/reduce_scatter | solution.py:380
  170.0 1.9 reshape.97
  172.0 0.0 all-to-all-done.1
  172.0 7.3 %all-to-all-start.3 = ((bf16[16,96,128]{2,1,0:T(8,128)(2,1)}), bf16[16,96,128]{2,1,0:T(8,128)(2,1)S(1)}, u32[]{:S(2)}, u32[]{:S(2)}) async-start(bf16[16,96,128]{2,1,0:T(8,128)(2,1)} %reshape.97), calls=%async_computation.5 | async-start | bytes 786432 | tf_op jit(solution)/shard_map/all_to_all | solution.py:351
  179.2 0.1 select_reduce_fusion
  179.3 0.1 select_reduce_fusion.1
  179.4 0.3 fusion.1
  179.6 7.6 %all-to-all-done.3 = bf16[16,96,128]{2,1,0:T(8,128)(2,1)S(1)} async-done(((bf16[16,96,128]{2,1,0:T(8,128)(2,1)}), bf16[16,96,128]{2,1,0:T(8,128)(2,1)S(1)}, u32[]{:S(2)}, u32[]{:S(2)}) %all-to-all-start.3) | async-done | bytes 393248 | tf_op jit(solution)/shard_map/all_to_all | solution.py:351
  187.2 0.2 reshape.98
  187.4 0.9 fusion
  (9 shorter events, 0.1 us)
Async XLA Ops:
  7.2 117.9 %copy-start = (bf16[4096,16]{0,1:T(8,128)(2,1)S(1)}, bf16[4096,16]{0,1:T(8,128)(2,1)}, u32[]{:S(2)}) copy-start(bf16[4096,16]{0,1:T(8,128)(2,1)} %param.25) | copy-start | bytes 393220
  7.2 8.9 %collective-permute-start.2 = (bf16[4096,128]{1,0:T(8,128)(2,1)}, bf16[4096,128]{1,0:T(8,128)(2,1)S(1)}, u32[]{:S(2)}, u32[]{:S(2)}) collective-permute-start(bf16[4096,128]{1,0:T(8,128)(2,1)} %refs_0_.1), channel_id=1, source_target_pairs={{0,1},{1,0},{2,3},{3,2},{4,5},{5,4},{6,7},{7,6},{8,9},{9,8},{10,11... | collective-permute-start | bytes 3145736 | tf_op jit(solution)/shard_map/ppermute | solution.py:42
  7.3 10.3 %collective-permute-start.3 = (bf16[4096,128]{1,0:T(8,128)(2,1)}, bf16[4096,128]{1,0:T(8,128)(2,1)}, u32[]{:S(2)}, u32[]{:S(2)}) collective-permute-start(bf16[4096,128]{1,0:T(8,128)(2,1)} %refs_2_.1), channel_id=1, source_target_pairs={{0,1},{1,0},{2,3},{3,2},{4,5},{5,4},{6,7},{7,6},{8,9},{9,8},{10,11... | collective-permute-start | bytes 3145736 | tf_op jit(solution)/shard_map/ppermute | solution.py:42
  8.7 7.4 %collective-permute-start = (bf16[16,4096]{1,0:T(8,128)(2,1)S(1)}, bf16[16,4096]{1,0:T(8,128)(2,1)S(1)}, u32[]{:S(2)}, u32[]{:S(2)}) collective-permute-start(bf16[16,4096]{1,0:T(8,128)(2,1)S(1)} %slice.12), channel_id=1, source_target_pairs={{0,16},{16,32},{32,48},{48,64},{64,80},{80,96},{96,112},{112,128},... | collective-permute-start | bytes 393224 | tf_op jit(solution)/shard_map/ppermute | solution.py:341
  12.1 19.4 %collective-permute-start.4 = (bf16[4096,128]{1,0:T(8,128)(2,1)}, bf16[4096,128]{1,0:T(8,128)(2,1)}, u32[]{:S(2)}, u32[]{:S(2)}) collective-permute-start(bf16[4096,128]{1,0:T(8,128)(2,1)} %refs_4_.1), channel_id=1, source_target_pairs={{0,1},{1,0},{2,3},{3,2},{4,5},{5,4},{6,7},{7,6},{8,9},{9,8},{10,11... | collective-permute-start | bytes 3145736 | tf_op jit(solution)/shard_map/ppermute | solution.py:42
  12.2 3.0 %collective-permute-start.1 = (f32[3,128]{1,0:T(4,128)}, f32[3,128]{1,0:T(4,128)S(1)}, u32[]{:S(2)}, u32[]{:S(2)}) collective-permute-start(f32[3,128]{1,0:T(4,128)} %taps_mine.1), channel_id=1, source_target_pairs={{0,1},{1,0},{2,3},{3,2},{4,5},{5,4},{6,7},{7,6},{8,9},{9,8},{10,11... | collective-permute-start | bytes 4616 | tf_op jit(solution)/shard_map/ppermute | solution.py:42
  15.2 16.3 %copy-start.9 = (f32[3,128]{1,0:T(4,128)}, f32[3,128]{1,0:T(4,128)S(1)}, u32[]{:S(2)}) copy-start(f32[3,128]{1,0:T(4,128)S(1)} %collective-permute-done.1.taps_theirs) | copy-start | bytes 4612
  15.2 32.8 %collective-permute-start.5 = (bf16[4096,128]{1,0:T(8,128)(2,1)}, bf16[4096,128]{1,0:T(8,128)(2,1)S(1)}, u32[]{:S(2)}, u32[]{:S(2)}) collective-permute-start(bf16[4096,128]{1,0:T(8,128)(2,1)} %bitcast.41), channel_id=1, source_target_pairs={{0,1},{1,0},{2,3},{3,2},{4,5},{5,4},{6,7},{7,6},{8,9},{9,8},{10,11... | collective-permute-start | bytes 3145736 | tf_op jit(solution)/shard_map/ppermute | solution.py:42
  16.1 15.4 %copy-start.5 = (bf16[16,4096]{1,0:T(8,128)(2,1)}, bf16[16,4096]{1,0:T(8,128)(2,1)S(1)}, u32[]{:S(2)}) copy-start(bf16[16,4096]{1,0:T(8,128)(2,1)S(1)} %collective-permute-done.before_ref) | copy-start | bytes 393220
  16.1 31.9 %collective-permute-start.6 = (bf16[4096,128]{1,0:T(8,128)(2,1)}, bf16[4096,128]{1,0:T(8,128)(2,1)S(1)}, u32[]{:S(2)}, u32[]{:S(2)}) collective-permute-start(bf16[4096,128]{1,0:T(8,128)(2,1)} %bitcast.44), channel_id=1, source_target_pairs={{0,1},{1,0},{2,3},{3,2},{4,5},{5,4},{6,7},{7,6},{8,9},{9,8},{10,11... | collective-permute-start | bytes 3145736 | tf_op jit(solution)/shard_map/ppermute | solution.py:42
  16.1 1.0 copy-start.4
  17.1 30.9 %collective-permute-start.7 = (bf16[128,4096]{1,0:T(8,128)(2,1)}, bf16[128,4096]{1,0:T(8,128)(2,1)S(1)}, u32[]{:S(2)}, u32[]{:S(2)}) collective-permute-start(bf16[128,4096]{1,0:T(8,128)(2,1)} %bitcast.47), channel_id=1, source_target_pairs={{0,1},{1,0},{2,3},{3,2},{4,5},{5,4},{6,7},{7,6},{8,9},{9,8},{10,11... | collective-permute-start | bytes 3145736 | tf_op jit(solution)/shard_map/ppermute | solution.py:42
  17.6 30.4 %collective-permute-start.8 = (bf16[128,4096]{1,0:T(8,128)(2,1)}, bf16[128,4096]{1,0:T(8,128)(2,1)}, u32[]{:S(2)}, u32[]{:S(2)}) collective-permute-start(bf16[128,4096]{1,0:T(8,128)(2,1)} %refs_1_.1), channel_id=1, source_target_pairs={{0,1},{1,0},{2,3},{3,2},{4,5},{5,4},{6,7},{7,6},{8,9},{9,8},{10,11... | collective-permute-start | bytes 3145736 | tf_op jit(solution)/shard_map/ppermute | solution.py:42
  23.9 24.0 %all-to-all-start = ((bf16[16,8,4096]{2,1,0:T(8,128)(2,1)}), bf16[16,8,4096]{2,1,0:T(8,128)(2,1)}, u32[]{:S(2)}, u32[]{:S(2)}) async-start(bf16[16,8,4096]{2,1,0:T(8,128)(2,1)} %bitcast.52), calls=%async_computation | async-start | bytes 2097152 | tf_op jit(solution)/shard_map/all_to_all | solution.py:351
  31.4 94.9 %reduce-scatter.3.cloned.1.call-start = ((), (), s32[]{:S(2)}) async-start(), calls=%async_computation.6 | async-start | bytes 2359296 | tf_op jit(solution)/shard_map/reduce_scatter | solution.py:376
  48.0 1.0 copy-start.1
  48.0 1.3 copy-start.2
  48.0 1.6 copy-start.3
  63.5 106.5 %reduce-scatter.5.cloned.1.call-start = ((), (), s32[]{:S(2)}) async-start(), calls=%async_computation.7 | async-start | bytes 3538944 | tf_op jit(solution)/shard_map/reduce_scatter | solution.py:380
  123.1 0.7 copy-start.7
  123.1 0.7 copy-start.8
  123.1 0.8 copy-start.6
  128.7 43.3 %all-to-all-start.1 = ((bf16[16,32,128]{2,1,0:T(8,128)(2,1)}), bf16[16,32,128]{2,1,0:T(8,128)(2,1)S(1)}, u32[]{:S(2)}, u32[]{:S(2)}) async-start(bf16[16,32,128]{2,1,0:T(8,128)(2,1)} %bitcast.16), calls=%async_computation.2 | async-start | bytes 262144 | tf_op jit(solution)/shard_map/all_to_all | solution.py:351
  172.0 15.3 %all-to-all-start.3 = ((bf16[16,96,128]{2,1,0:T(8,128)(2,1)}), bf16[16,96,128]{2,1,0:T(8,128)(2,1)S(1)}, u32[]{:S(2)}, u32[]{:S(2)}) async-start(bf16[16,96,128]{2,1,0:T(8,128)(2,1)} %reshape.97), calls=%async_computation.5 | async-start | bytes 786432 | tf_op jit(solution)/shard_map/all_to_all | solution.py:351
Sparse Core Ops, SparseCore 0:
  63.7 43.1 reduce-scatter.2
  123.3 46.6 reduce-scatter.4

commit v4 on v3

v4 whole, which is shorter than its diff:
```python
import functools

import jax
import jax.numpy as jnp
from jax import lax
from jax.experimental import pallas as pl
from jax.experimental.pallas import tpu as pltpu
from jax.sharding import Mesh
from jax.sharding import PartitionSpec as P


TAPS = 3
EXPERTS = 16
GROUPS = 4
TOPK = 2
MOE_SHARE = 16
EPG = 4
CAP = 4


EP = ("y", "x")
TP = ("z", "core")
ALL = EP + TP


def route_weights(normed, routes, router_group, router_expert):
    group_logit = jnp.dot(normed, router_group, preferred_element_type=jnp.float32)
    expert_logit = jnp.dot(normed, router_expert, preferred_element_type=jnp.float32)
    group_exp = jnp.exp(group_logit)
    group_id = routes[:, 0] // EPG
    group_pick = (group_id[:, None] == jnp.arange(GROUPS, dtype=jnp.int32)[None, :]).astype(
        jnp.float32
    )
    group_gate = jnp.sum(group_exp * group_pick, axis=1) / jnp.sum(group_exp, axis=1)
    expert_pick = (
        routes[:, :, None] == jnp.arange(EXPERTS, dtype=jnp.int32)[None, None, :]
    ).astype(jnp.float32)
    chosen = jnp.exp(jnp.sum(expert_logit[:, None, :] * expert_pick, axis=2))
    return group_gate[:, None] * chosen / jnp.sum(chosen, axis=1, keepdims=True)


def swap_cores(value):
    return lax.ppermute(value, "core", [(0, 1), (1, 0)])


def iota(shape, dim):
    return lax.broadcasted_iota(jnp.int32, shape, dim)


def select_matrix(mask):
    return jnp.where(mask, 1.0, 0.0).astype(jnp.bfloat16)


def product(left, right):
    return jnp.dot(left, right, preferred_element_type=jnp.float32)


def scaled_rows(rows, gain):
    values = rows.astype(jnp.float32)
    inverse = lax.rsqrt(jnp.mean(values * values, axis=-1, keepdims=True) + 1e-06)
    return (values * inverse * gain).astype(jnp.bfloat16)


def prep_kernel(zs, core_ref, tokens_ref, gain_ref, routes_ref, placed_ref, normed_ref, ranks_ref):
    share = MOE_SHARE
    rows = zs * share
    width = tokens_ref.shape[-1]
    normed_ref[...] = scaled_rows(tokens_ref[...].reshape(rows, width), gain_ref[...])
    token = iota((2 * rows, rows), 1)
    source = (token // share) * (2 * share) + core_ref[0] * share + token % share
    pick = select_matrix(iota((2 * rows, rows), 0) == source)
    routes = product(routes_ref[...].astype(jnp.float32).astype(jnp.bfloat16), pick).astype(jnp.int32)
    expert = iota((EXPERTS, rows), 0)
    named = [expert == routes[k : k + 1] for k in range(TOPK)]
    earlier, later = iota((rows, rows), 0), iota((rows, rows), 1)
    before = (earlier // share == later // share) & (earlier < later)
    counts = product(select_matrix(named[0] | named[1]), select_matrix(before))
    ranks = [
        jnp.sum(jnp.where(named[k], counts, 0.0), axis=0, keepdims=True).astype(jnp.int32)
        for k in range(TOPK)
    ]
    block = iota((1, rows), 1) // share
    slots = iota((EXPERTS * CAP * zs, rows), 0)
    inside = []
    for k in range(TOPK):
        ranks_ref[k : k + 1, :] = ranks[k]
        inside.append(slots == (routes[k : k + 1] * CAP + ranks[k]) * zs + block)
    select = select_matrix(inside[0] | inside[1])
    step = 512

    @pl.loop(0, width // step)
    def _(index):
        columns = pl.ds(pl.multiple_of(index * step, step), step)
        placed_ref[:, columns] = product(select, normed_ref[:, columns]).astype(jnp.bfloat16)


def prepare(core, tokens, gain, routes, zs):
    rows, width = tokens.shape
    half = rows // 2
    return pl.pallas_call(
        functools.partial(prep_kernel, zs),
        grid_spec=pltpu.PrefetchScalarGridSpec(
            num_scalar_prefetch=1,
            grid=(1,),
            in_specs=[
                pl.BlockSpec((zs, 1, MOE_SHARE, width), lambda i, c: (0, c[0], 0, 0)),
                pl.BlockSpec((1, width), lambda i, c: (0, 0)),
                pl.BlockSpec((TOPK, rows), lambda i, c: (0, 0)),
            ],
            out_specs=[
                pl.BlockSpec((EXPERTS * CAP * zs, width), lambda i, c: (0, 0)),
                pl.BlockSpec((half, width), lambda i, c: (0, 0)),
                pl.BlockSpec((TOPK, half), lambda i, c: (0, 0)),
            ],
        ),
        out_shape=[
            jax.ShapeDtypeStruct((EXPERTS * CAP * zs, width), jnp.bfloat16),
            jax.ShapeDtypeStruct((half, width), jnp.bfloat16),
            jax.ShapeDtypeStruct((TOPK, half), jnp.int32),
        ],
        cost_estimate=pl.CostEstimate(
            flops=2 * EXPERTS * CAP * zs * half * width,
            bytes_accessed=2 * width * (rows + EXPERTS * CAP * zs),
            transcendentals=0,
        ),
        name="prepare",
    )(
        core,
        tokens.reshape(zs, 2, MOE_SHARE, width),
        gain.reshape(1, width),
        routes.T,
    )


def mixer_kernel(
    steps, core_ref, tokens_ref, halo_ref, before_ref, gain_ref, taps_mine, taps_theirs, *refs
):
    weights, (m0, m1, out_ref, normed_ref, sums_ref, channels_ref) = refs[:6], refs[6:]
    step = pl.program_id(0)
    rows = out_ref.shape[0]
    depth, half = weights[0].shape
    width = tokens_ref.shape[-1]
    blocks, _, tail_rows, _ = halo_ref.shape
    halos = blocks * tail_rows
    total = normed_ref.shape[0]
    reach = TAPS - 1

    @pl.when(step == 0)
    def _():
        gain = gain_ref[...]
        normed_ref[0:rows, :] = scaled_rows(tokens_ref[...].reshape(rows, width), gain)
        normed_ref[rows : rows + halos, :] = scaled_rows(halo_ref[...].reshape(halos, width), gain)
        normed_ref[rows + halos :, :] = scaled_rows(before_ref[...], gain)
        sums_ref[...] = jnp.zeros_like(sums_ref)

    @pl.when(step < steps)
    def _():
        piece = normed_ref[:, pl.ds(pl.multiple_of(step * depth, depth), depth)]
        joint = jnp.concatenate([weight[...] for weight in weights], axis=1)
        sums_ref[...] += product(piece, joint)

    @pl.when(step == steps - 1)
    def _():
        def pair(index):
            return sums_ref[:, 2 * index * half : 2 * (index + 1) * half]

        gated = (pair(1) * pair(0)).astype(jnp.bfloat16)
        row, source = iota((rows, total), 0), iota((rows, total), 1)
        place = row % MOE_SHARE
        ahead = row // MOE_SHARE + core_ref[0]
        tail = jnp.where(ahead == 0, total, rows + ahead * tail_rows)
        taps = jnp.concatenate([taps_mine[...], taps_theirs[...]], axis=1)
        mixed = None
        for tap in range(TAPS):
            back = reach - tap
            wanted = jnp.where(place >= back, row, tail + place) - back
            shifted = product(select_matrix(source == wanted), gated)
            term = taps[tap : tap + 1] * shifted
            mixed = term if mixed is None else mixed + term
        channels_ref[...] = (pair(2)[0:rows] * mixed).astype(jnp.bfloat16)

    @pl.when(step >= steps)
    def _():
        joint = jnp.concatenate([m0[...], m1[...]], axis=0)
        out_ref[...] = product(channels_ref[...], joint).astype(jnp.bfloat16)


def mixer_partial(core, tokens, before, gain, taps, weights, mixes, zs):
    rows, width = tokens.shape
    half = rows // 2
    channels = weights[0].shape[1]
    depth = 1024
    steps = width // depth
    tail_rows = MOE_SHARE // 2
    total = half + zs * tail_rows + before.shape[0]
    fixed = lambda i, c: (0, 0)
    after = lambda i, c: (0, jnp.maximum(i - steps, 0))
    split = tokens.reshape(zs, 2, MOE_SHARE, width)
    return pl.pallas_call(
        functools.partial(mixer_kernel, steps),
        grid_spec=pltpu.PrefetchScalarGridSpec(
            num_scalar_prefetch=1,
            grid=(2 * steps,),
            in_specs=[
                pl.BlockSpec((zs, 1, MOE_SHARE, width), lambda i, c: (0, c[0], 0, 0)),
                pl.BlockSpec((zs, 1, tail_rows, width), lambda i, c: (0, 1 - c[0], 1, 0)),
                pl.BlockSpec(before.shape, fixed),
                pl.BlockSpec((1, width), fixed),
                pl.BlockSpec((TAPS, channels), fixed),
                pl.BlockSpec((TAPS, channels), fixed),
            ]
            + [pl.BlockSpec((depth, channels), lambda i, c: (jnp.minimum(i, steps - 1), 0))] * 6
            + [pl.BlockSpec((channels, depth), after)] * 2,
            out_specs=pl.BlockSpec((half, depth), after),
            scratch_shapes=[
                pltpu.VMEM((total, width), jnp.bfloat16),
                pltpu.VMEM((total, 6 * channels), jnp.float32),
                pltpu.VMEM((half, 2 * channels), jnp.bfloat16),
            ],
        ),
        out_shape=jax.ShapeDtypeStruct((half, width), jnp.bfloat16),
        cost_estimate=pl.CostEstimate(
            flops=2 * width * channels * (6 * total + 2 * half),
            bytes_accessed=2 * width * (total + half + 8 * channels),
            transcendentals=0,
        ),
        name="mixer",
    )(core, split, split, before, gain.reshape(1, width), *taps, *weights, *mixes)


def expert_kernel(zs, steps, rows_ref, g0, g1, u0, u1, d0, d1, out_ref, sums_ref, units_ref):
    step = pl.program_id(0)
    count = rows_ref.shape[0]
    units = 2 * g0.shape[1]

    @pl.when(step == 0)
    def _():
        sums_ref[...] = jnp.zeros_like(sums_ref)

    @pl.when(step < steps)
    def _():
        joint = jnp.concatenate([g0[...], g1[...], u0[...], u1[...]], axis=1)
        sums_ref[...] += product(rows_ref[...], joint)

    @pl.when(step == steps - 1)
    def _():
        target, source = iota((count, count), 0), iota((count, count), 1)
        order = select_matrix(target == (source % zs) * (count // zs) + source // zs)
        gate, up = sums_ref[:, :units], sums_ref[:, units:]
        hidden = (gate * jax.nn.sigmoid(gate) * up).astype(jnp.bfloat16)
        units_ref[...] = product(order, hidden).astype(jnp.bfloat16)

    @pl.when(step >= steps)
    def _():
        joint = jnp.concatenate([d0[...], d1[...]], axis=0)
        out_ref[...] = product(units_ref[...], joint).astype(jnp.bfloat16)


def expert_partial(rows, weights, downs, zs):
    count, width = rows.shape
    half = weights[0].shape[1]
    depth = 1024
    steps = width // depth
    early = lambda i: jnp.minimum(i, steps - 1)
    after = lambda i: jnp.maximum(i - steps, 0)
    return pl.pallas_call(
        functools.partial(expert_kernel, zs, steps),
        grid=(2 * steps,),
        in_specs=[pl.BlockSpec((count, depth), lambda i: (0, early(i)))]
        + [pl.BlockSpec((depth, half), lambda i: (early(i), 0))] * 4
        + [pl.BlockSpec((half, depth), lambda i: (0, after(i)))] * 2,
        out_specs=pl.BlockSpec((count, depth), lambda i: (0, after(i))),
        scratch_shapes=[
            pltpu.VMEM((count, 4 * half), jnp.float32),
            pltpu.VMEM((count, 2 * half), jnp.bfloat16),
        ],
        out_shape=jax.ShapeDtypeStruct((count, width), jnp.bfloat16),
        cost_estimate=pl.CostEstimate(
            flops=12 * width * half * count,
            bytes_accessed=2 * width * (2 * count + 6 * half),
            transcendentals=2 * count * half,
        ),
        name="experts",
    )(rows, *weights, *downs)


def layer(
    mix_tokens,
    mix_gain,
    value_weight,
    inner_weight,
    outer_weight,
    conv_taps,
    mix_weight,
    moe_tokens,
    moe_gain,
    router_group,
    router_expert,
    expert_routes,
    gate_weight,
    up_weight,
    down_weight,
):
    z_index = lax.axis_index("z")
    core = lax.axis_index("core")
    zs = lax.axis_size("z")
    eps = lax.axis_size(EP)
    width = moe_tokens.shape[1]
    core_ref = core.reshape(1).astype(jnp.int32)

    before = lax.ppermute(
        mix_tokens[mix_tokens.shape[0] - MOE_SHARE :], EP, [(i, i + 1) for i in range(eps - 1)]
    )
    gate, up, down = gate_weight[0], up_weight[0], down_weight[0]

    placed, half_normed, half_ranks = prepare(
        core_ref, moe_tokens, moe_gain, expert_routes, zs
    )
    placed, before = lax.optimization_barrier((placed, before))

    def exchange(array):
        return lax.all_to_all(array, EP, split_axis=0, concat_axis=0, tiled=True)

    arrived = exchange(placed.reshape(EXPERTS, CAP * zs, width)).reshape(-1, width)

    taps = (conv_taps, swap_cores(conv_taps))
    projections = (
        value_weight,
        swap_cores(value_weight),
        inner_weight,
        swap_cores(inner_weight),
        outer_weight,
        swap_cores(outer_weight),
    )
    mixes = (mix_weight, swap_cores(mix_weight))
    partial_mix = mixer_partial(
        core_ref, mix_tokens, before, mix_gain, taps, projections, mixes, zs
    )
    mixer_out = lax.psum_scatter(partial_mix, "z", scatter_dimension=0, tiled=True)

    weights = (gate, swap_cores(gate), up, swap_cores(up))
    downs = (down, swap_cores(down))
    partial_value = expert_partial(arrived, weights, downs, zs)
    partial_value, mixer_out = lax.optimization_barrier((partial_value, mixer_out))
    summed = lax.psum_scatter(partial_value, "z", scatter_dimension=0, tiled=True)
    returned = exchange(summed.reshape(eps, CAP * width // 128, 128)).reshape(-1, width)

    own_routes = lax.dynamic_slice_in_dim(
        expert_routes, (2 * z_index + core) * MOE_SHARE, MOE_SHARE, 0
    )
    own_normed = lax.dynamic_slice_in_dim(half_normed, z_index * MOE_SHARE, MOE_SHARE, 0)
    own_ranks = lax.dynamic_slice_in_dim(half_ranks, z_index * MOE_SHARE, MOE_SHARE, 1).T
    token_weights = route_weights(own_normed, own_routes, router_group, router_expert)

    position = own_routes * CAP + own_ranks
    targets = jnp.arange(EXPERTS * CAP, dtype=jnp.int32)
    spread = jnp.sum(
        jnp.where(position[:, :, None] == targets, token_weights[:, :, None], 0.0), axis=1
    )
    expert_out = jnp.dot(
        spread,
        returned.astype(jnp.float32),
        precision=lax.Precision.HIGHEST,
        preferred_element_type=jnp.float32,
    )
    return (mixer_out, expert_out.astype(jnp.bfloat16))


def solution(mesh):
    torus = Mesh(mesh.devices.reshape(4, 4, 8, 2), ALL)
    return jax.shard_map(
        layer,
        mesh=torus,
        in_specs=(
            P(EP, None),
            P(),
            P(None, TP),
            P(None, TP),
            P(None, TP),
            P(None, TP),
            P(TP, None),
            P(EP, None),
            P(),
            P(),
            P(),
            P(EP, None),
            P(EP, None, TP),
            P(EP, None, TP),
            P(EP, TP, None),
        ),
        out_specs=(P(ALL, None), P(ALL, None)),
        check_vma=False,
    )
```

time: 196 us -> 183 us (0.934)
  waiting for transfers between devices: 54.3 us -> 110 us
  blocking collectives: 44.4 us -> 0 us
  Pallas kernels: 45 us -> 26.7 us
  starting transfers between devices: 24.7 us -> 20 us
    all_to_all x1 -> x0, blocking collectives: 44.4 us -> none  [exchange(): return lax.all_to_all(array, EP, split_axis=0, concat_axis=0, tiled=True)]
    all_to_all x3 -> x2, waiting for transfers between devices: 14.4 us -> 42.9 us  [exchange(): return lax.all_to_all(array, EP, split_axis=0, concat_axis=0, tiled=True)]
    reduce_scatter x2, waiting for transfers between devices: 36.6 us -> 56.9 us  [the longest x1 56.9 us: layer(): lax.psum_scatter(partial_value, 'z', scatter_dimension=0, tiled=True)]
    pallas_call x3 -> x2, Pallas kernels: 38.7 us -> 20.5 us  [the longest x1 10.5 us: expert_partial(): pl.pallas_call(functools.partial(expert_kernel, zs, steps), grid=(2 * ste...]
    ppermute x8, waiting for transfers between devices: 2.51 us -> 10.2 us  [swap_cores(): return lax.ppermute(value, 'core', [(0, 1), (1, 0)])]
    all_to_all x3 -> x2, starting transfers between devices: 19.4 us -> 14.6 us  [exchange(): return lax.all_to_all(array, EP, split_axis=0, concat_axis=0, tiled=True)]
    unnamed x22 -> x38, local copies, waits for them, and re-layouts: 5.61 us -> 4.32 us
  transfers between devices with their start and end apart: 14 -> 13, of which waited for: 5 -> 7; matrix products, arithmetic and copies ran while one was open for 4% -> 1% of each run, Pallas kernels for 16% -> 15%
where the time goes in v4:
time: 183 us; the launch traced here: 182 us
  waiting for transfers between devices  110 us (60%)
  Pallas kernels  26.7 us (15%)
  starting transfers between devices  20 us (11%)
  between operations  14.3 us (8%)
  local copies, waits for them, and re-layouts  7.57 us (4%)
  matrix products  3.14 us (2%)
    reduce_scatter x1, waiting for transfers between devices, layer(): lax.psum_scatter(partial_value, 'z', scatter_dimension=0, tiled=True)  56.9 us
    all_to_all x2, waiting for transfers between devices, exchange(): return lax.all_to_all(array, EP, split_axis=0, concat_axis=0, tiled=True)  42.9 us
    all_to_all x2, starting transfers between devices, exchange(): return lax.all_to_all(array, EP, split_axis=0, concat_axis=0, tiled=True)  14.6 us
    pallas_call x1, Pallas kernels, expert_partial(): pl.pallas_call(functools.partial(expert_kernel, zs, steps), grid=(2 * ste...  10.5 us
    ppermute x8, waiting for transfers between devices, swap_cores(): return lax.ppermute(value, 'core', [(0, 1), (1, 0)])  10.2 us
    pallas_call x1, Pallas kernels, mixer_partial(): pl.pallas_call(functools.partial(mixer_kernel, steps), grid_spec=pltpu.Pr...  10 us
    pallas_call x1, Pallas kernels, prepare(): pl.pallas_call(functools.partial(prep_kernel, zs), grid_spec=pltpu.Prefet...  6.14 us
    unnamed x38, local copies, waits for them, and re-layouts  4.32 us
  transfers between devices with their start and end apart: 13, of which 7 were waited for; matrix products, arithmetic and copies ran while one was open for 1% of the time, Pallas kernels for 15%

profile of v4, /device:TPU:2, one launch (start us, length us, event | category | flops | bytes accessed | tf_op | source)
XLA Modules:
  0.0 182.0 jit_solution(4997242753962235915)
XLA Ops:
  7.2 0.0 copy-start
  7.2 1.0 slice.6
  8.1 3.4 %collective-permute-start = (bf16[16,4096]{1,0:T(8,128)(2,1)S(1)}, bf16[16,4096]{1,0:T(8,128)(2,1)S(1)}, u32[]{:S(2)}, u32[]{:S(2)}) collective-permute-start(bf16[16,4096]{1,0:T(8,128)(2,1)S(1)} %slice.6), channel_id=1, source_target_pairs={{0,16},{16,32},{32,48},{48,64},{64,80},{80,96},{96,112},{112,128},... | collective-permute-start | bytes 393224 | tf_op jit(solution)/shard_map/ppermute | solution.py:311
  11.5 6.1 %prepare.1 = (bf16[512,4096]{1,0:T(8,128)(2,1)}, bf16[128,4096]{1,0:T(8,128)(2,1)}, s32[2,128]{1,0:T(2,128)}) custom-call(s32[1]{0:T(128)} %bitcast.core_ref, bf16[8,2,16,4096]{3,2,1,0:T(8,128)(2,1)} %bitcast.22, f32[1,4096]{1,0:T(1,128)} %bitcast.29, s32[2,256]{1,0:T(2,128)} %bitcast.31), custom_call_target="tpu_custom_call" | custom-call | flops 536870912 | bytes 6291456 | tf_op jit(solution)/shard_map/prepare/pallas_call | solution.py:100
  17.7 0.0 collective-permute-done.before_ref
  17.7 0.0 copy-start.7
  17.7 0.0 copy-start.8
  17.7 0.0 copy-start.16
  17.7 0.6 copy-done.13
  18.3 7.3 %all-to-all-start = ((bf16[16,32,4096]{2,1,0:T(8,128)(2,1)}), bf16[16,32,4096]{2,1,0:T(8,128)(2,1)}, u32[]{:S(2)}, u32[]{:S(2)}) async-start(bf16[16,32,4096]{2,1,0:T(8,128)(2,1)} %bitcast.21), calls=%async_computation | async-start | bytes 8388608 | tf_op jit(solution)/shard_map/all_to_all | solution.py:322
  25.6 0.0 reduce-scatter.3.cloned.1.call-start
  25.7 0.0 copy-done.6
  25.7 0.1 collective-permute-start.5
  25.8 0.0 copy-done.7
  25.8 0.5 collective-permute-start.6
  26.3 0.0 copy-done.8
  26.3 0.1 collective-permute-start.7
  26.4 0.4 collective-permute-start.8
  26.8 0.0 copy-done.16
  26.8 0.1 collective-permute-start.4
  26.9 6.0 %collective-permute-done.4.taps_theirs = f32[3,128]{1,0:T(4,128)S(1)} collective-permute-done((f32[3,128]{1,0:T(4,128)S(1)}, f32[3,128]{1,0:T(4,128)S(1)}, u32[]{:S(2)}, u32[]{:S(2)}) %collective-permute-start.4) | collective-permute-done | bytes 1568 | tf_op jit(solution)/shard_map/ppermute | solution.py:43
  33.0 0.0 collective-permute-done.5.refs_1_
  33.0 0.0 collective-permute-done.6.refs_3_
  33.0 0.0 copy-start.10
  33.0 0.0 collective-permute-done.7.refs_5_
  33.0 0.0 copy-start.11
  33.0 0.0 collective-permute-done.8.refs_7_
  33.0 0.0 copy-start.12
  33.0 0.9 copy-done.9
  33.9 0.4 copy-done.10
  34.3 0.4 copy-done.11
  34.7 0.3 copy-done.12
  35.0 0.0 copy-done.17
  35.1 10.0 %mixer.1 = bf16[128,4096]{1,0:T(8,128)(2,1)} custom-call(s32[1]{0:T(128)} %bitcast.core_ref, bf16[8,2,16,4096]{3,2,1,0:T(8,128)(2,1)} %bitcast.19, bf16[8,2,16,4096]{3,2,1,0:T(8,128)(2,1)} %bitcast.20, bf16[16,4096]{1,0:T(8,128)(2,1)} %copy-done.13, f32[1,4096]{1,0:T(1,128)} %bitcast.30, f32[3,128]{1,0:T(4,128)} %taps_mine.1, f32[3,128]{1,0:T(4,128)} %copy-done.17, ...), custom_call_target="tpu_custom_call" | custom-call | flops 1577058304 | bytes 11141120 | tf_op jit(solution)/shard_map/mixer/pallas_call | solution.py:199
  45.1 0.0 reduce-scatter.3.cloned.1.call-update
  45.1 0.0 reduce-scatter.5.cloned.1.call-start
  45.2 0.0 copy-done.1
  45.2 0.2 collective-permute-start.1
  45.4 0.0 copy-done.2
  45.4 0.4 collective-permute-start.2
  45.8 0.1 collective-permute-start.3
  45.9 2.0 %collective-permute-done.1.g1 = bf16[4096,128]{1,0:T(8,128)(2,1)S(1)} collective-permute-done((bf16[4096,128]{1,0:T(8,128)(2,1)S(1)}, bf16[4096,128]{1,0:T(8,128)(2,1)S(1)}, u32[]{:S(2)}, u32[]{:S(2)}) %collective-permute-start.1) | collective-permute-done | bytes 1048608 | tf_op jit(solution)/shard_map/ppermute | solution.py:43
  47.9 1.5 collective-permute-done.2.u1
  49.4 1.0 copy-done.5
  50.4 0.6 collective-permute-done.3.d1
  51.1 33.1 %all-to-all-done = bf16[16,32,4096]{2,1,0:T(8,128)(2,1)} async-done(((bf16[16,32,4096]{2,1,0:T(8,128)(2,1)}), bf16[16,32,4096]{2,1,0:T(8,128)(2,1)}, u32[]{:S(2)}, u32[]{:S(2)}) %all-to-all-start) | async-done | bytes 4194336 | tf_op jit(solution)/shard_map/all_to_all | solution.py:322
  84.1 10.5 %experts.1 = bf16[512,4096]{1,0:T(8,128)(2,1)} custom-call(bf16[512,4096]{1,0:T(8,128)(2,1)} %bitcast.5.rows_ref, bf16[4096,128]{1,0:T(8,128)(2,1)} %bitcast.23, bf16[4096,128]{1,0:T(8,128)(2,1)} %copy-done.4, bf16[4096,128]{1,0:T(8,128)(2,1)} %bitcast.25, bf16[4096,128]{1,0:T(8,128)(2,1)} %copy-done.5, bf16[128,4096]{1,0:T(8,128)(2,1)} %bitcast.27, ...), custom_call_target="tpu_custom_call" | custom-call | flops 3221225472 | bytes 14680064 | tf_op jit(solution)/shard_map/experts/pallas_call | solution.py:266
  94.6 0.0 copy-start.14
  94.6 0.0 reduce-scatter.3.cloned.1.call-done
  94.7 0.0 reduce-scatter.5.cloned.1.call-update
  94.7 0.6 copy-done.15
  95.3 0.0 copy-done.18
  95.3 0.1 bitcast_add_fusion
  95.4 0.0 copy-done.14
  95.4 1.1 fusion.6
  96.5 1.1 fusion
  97.6 56.9 %reduce-scatter.5.cloned.1.call-done = bf16[64,4096]{1,0:T(8,128)(2,1)} async-done(((bf16[512,4096]{1,0:T(8,128)(2,1)}), bf16[64,4096]{1,0:T(8,128)(2,1)}) %reduce-scatter.5.cloned.1.call-update) | async-done | bytes 524304 | tf_op jit(solution)/shard_map/reduce_scatter | solution.py:345
  154.5 2.1 %reshape.80 = bf16[16,128,128]{2,1,0:T(8,128)(2,1)} reshape(bf16[64,4096]{1,0:T(8,128)(2,1)} %reduce-scatter.5.cloned.1.call-done) | data formatting | bytes 1048576 | tf_op jit(solution)/shard_map/reshape | solution.py:346
  156.5 7.3 %all-to-all-start.1 = ((bf16[16,128,128]{2,1,0:T(8,128)(2,1)}), bf16[16,128,128]{2,1,0:T(8,128)(2,1)S(1)}, u32[]{:S(2)}, u32[]{:S(2)}) async-start(bf16[16,128,128]{2,1,0:T(8,128)(2,1)} %reshape.80), calls=%async_computation.3 | async-start | bytes 1048576 | tf_op jit(solution)/shard_map/all_to_all | solution.py:322
  163.8 0.2 select_reduce_fusion.1
  164.0 0.1 select_reduce_fusion
  164.1 9.8 %all-to-all-done.1 = bf16[16,128,128]{2,1,0:T(8,128)(2,1)S(1)} async-done(((bf16[16,128,128]{2,1,0:T(8,128)(2,1)}), bf16[16,128,128]{2,1,0:T(8,128)(2,1)S(1)}, u32[]{:S(2)}, u32[]{:S(2)}) %all-to-all-start.1) | async-done | bytes 524320 | tf_op jit(solution)/shard_map/all_to_all | solution.py:322
  173.9 0.2 reshape.81
  174.2 1.0 convolution_convert_fusion
  (18 shorter events, 0.1 us)
Async XLA Ops:
  7.2 89.3 %copy-start = (bf16[4096,16]{0,1:T(8,128)(2,1)S(1)}, bf16[4096,16]{0,1:T(8,128)(2,1)}, u32[]{:S(2)}) copy-start(bf16[4096,16]{0,1:T(8,128)(2,1)} %param.25) | copy-start | bytes 393220
  8.1 9.6 %collective-permute-start = (bf16[16,4096]{1,0:T(8,128)(2,1)S(1)}, bf16[16,4096]{1,0:T(8,128)(2,1)S(1)}, u32[]{:S(2)}, u32[]{:S(2)}) collective-permute-start(bf16[16,4096]{1,0:T(8,128)(2,1)S(1)} %slice.6), channel_id=1, source_target_pairs={{0,16},{16,32},{32,48},{48,64},{64,80},{80,96},{96,112},{112,128},... | collective-permute-start | bytes 393224 | tf_op jit(solution)/shard_map/ppermute | solution.py:311
  17.7 0.7 copy-start.13
  17.7 8.0 %copy-start.6 = (bf16[4096,128]{1,0:T(8,128)(2,1)S(1)}, bf16[4096,128]{1,0:T(8,128)(2,1)}, u32[]{:S(2)}) copy-start(bf16[4096,128]{1,0:T(8,128)(2,1)} %refs_0_.1) | copy-start | bytes 3145732
  17.7 8.1 %copy-start.7 = (bf16[4096,128]{1,0:T(8,128)(2,1)S(1)}, bf16[4096,128]{1,0:T(8,128)(2,1)}, u32[]{:S(2)}) copy-start(bf16[4096,128]{1,0:T(8,128)(2,1)} %refs_2_.1) | copy-start | bytes 3145732
  17.7 8.6 %copy-start.8 = (bf16[4096,128]{1,0:T(8,128)(2,1)S(1)}, bf16[4096,128]{1,0:T(8,128)(2,1)}, u32[]{:S(2)}) copy-start(bf16[4096,128]{1,0:T(8,128)(2,1)} %refs_4_.1) | copy-start | bytes 3145732
  17.7 9.1 %copy-start.16 = (f32[3,128]{1,0:T(4,128)S(1)}, f32[3,128]{1,0:T(4,128)}, u32[]{:S(2)}) copy-start(f32[3,128]{1,0:T(4,128)} %taps_mine.1) | copy-start | bytes 4612
  18.3 65.8 %all-to-all-start = ((bf16[16,32,4096]{2,1,0:T(8,128)(2,1)}), bf16[16,32,4096]{2,1,0:T(8,128)(2,1)}, u32[]{:S(2)}, u32[]{:S(2)}) async-start(bf16[16,32,4096]{2,1,0:T(8,128)(2,1)} %bitcast.21), calls=%async_computation | async-start | bytes 8388608 | tf_op jit(solution)/shard_map/all_to_all | solution.py:322
  25.6 69.0 %reduce-scatter.3.cloned.1.call-start = ((), (), s32[]{:S(2)}) async-start(), calls=%async_computation.4 | async-start | bytes 1179648 | tf_op jit(solution)/shard_map/reduce_scatter | solution.py:339
  25.7 7.3 %collective-permute-start.5 = (bf16[4096,128]{1,0:T(8,128)(2,1)S(1)}, bf16[4096,128]{1,0:T(8,128)(2,1)S(1)}, u32[]{:S(2)}, u32[]{:S(2)}) collective-permute-start(bf16[4096,128]{1,0:T(8,128)(2,1)S(1)} %copy-done.6), channel_id=1, source_target_pairs={{0,1},{1,0},{2,3},{3,2},{4,5},{5,4},{6,7},{7,6},{8,9},{9,8},{10,11... | collective-permute-start | bytes 3145736 | tf_op jit(solution)/shard_map/ppermute | solution.py:43
  25.8 7.1 %collective-permute-start.6 = (bf16[4096,128]{1,0:T(8,128)(2,1)S(1)}, bf16[4096,128]{1,0:T(8,128)(2,1)S(1)}, u32[]{:S(2)}, u32[]{:S(2)}) collective-permute-start(bf16[4096,128]{1,0:T(8,128)(2,1)S(1)} %copy-done.7), channel_id=1, source_target_pairs={{0,1},{1,0},{2,3},{3,2},{4,5},{5,4},{6,7},{7,6},{8,9},{9,8},{10,11... | collective-permute-start | bytes 3145736 | tf_op jit(solution)/shard_map/ppermute | solution.py:43
  26.3 6.7 %collective-permute-start.7 = (bf16[4096,128]{1,0:T(8,128)(2,1)S(1)}, bf16[4096,128]{1,0:T(8,128)(2,1)S(1)}, u32[]{:S(2)}, u32[]{:S(2)}) collective-permute-start(bf16[4096,128]{1,0:T(8,128)(2,1)S(1)} %copy-done.8), channel_id=1, source_target_pairs={{0,1},{1,0},{2,3},{3,2},{4,5},{5,4},{6,7},{7,6},{8,9},{9,8},{10,11... | collective-permute-start | bytes 3145736 | tf_op jit(solution)/shard_map/ppermute | solution.py:43
  26.4 6.6 %collective-permute-start.8 = (bf16[128,4096]{1,0:T(8,128)(2,1)}, bf16[128,4096]{1,0:T(8,128)(2,1)S(1)}, u32[]{:S(2)}, u32[]{:S(2)}) collective-permute-start(bf16[128,4096]{1,0:T(8,128)(2,1)} %refs_6_.1), channel_id=1, source_target_pairs={{0,1},{1,0},{2,3},{3,2},{4,5},{5,4},{6,7},{7,6},{8,9},{9,8},{10,11... | collective-permute-start | bytes 3145736 | tf_op jit(solution)/shard_map/ppermute | solution.py:43
  26.8 6.1 %collective-permute-start.4 = (f32[3,128]{1,0:T(4,128)S(1)}, f32[3,128]{1,0:T(4,128)S(1)}, u32[]{:S(2)}, u32[]{:S(2)}) collective-permute-start(f32[3,128]{1,0:T(4,128)S(1)} %copy-done.16), channel_id=1, source_target_pairs={{0,1},{1,0},{2,3},{3,2},{4,5},{5,4},{6,7},{7,6},{8,9},{9,8},{10,11... | collective-permute-start | bytes 4616 | tf_op jit(solution)/shard_map/ppermute | solution.py:43
  32.9 2.1 %copy-start.17 = (f32[3,128]{1,0:T(4,128)}, f32[3,128]{1,0:T(4,128)S(1)}, u32[]{:S(2)}) copy-start(f32[3,128]{1,0:T(4,128)S(1)} %collective-permute-done.4.taps_theirs) | copy-start | bytes 4612
  33.0 1.0 copy-start.9
  33.0 1.3 copy-start.10
  33.0 1.7 copy-start.11
  33.0 2.0 %copy-start.12 = (bf16[128,4096]{1,0:T(8,128)(2,1)}, bf16[128,4096]{1,0:T(8,128)(2,1)S(1)}, u32[]{:S(2)}) copy-start(bf16[128,4096]{1,0:T(8,128)(2,1)S(1)} %collective-permute-done.8.refs_7_) | copy-start | bytes 3145732
  35.0 10.1 %copy-start.1 = (bf16[1,4096,128]{2,1,0:T(8,128)(2,1)S(1)}, bf16[1,4096,128]{2,1,0:T(8,128)(2,1)}, u32[]{:S(2)}) copy-start(bf16[1,4096,128]{2,1,0:T(8,128)(2,1)} %param.27) | copy-start | bytes 3145732
  35.0 10.4 %copy-start.2 = (bf16[1,4096,128]{2,1,0:T(8,128)(2,1)S(1)}, bf16[1,4096,128]{2,1,0:T(8,128)(2,1)}, u32[]{:S(2)}) copy-start(bf16[1,4096,128]{2,1,0:T(8,128)(2,1)} %param.28) | copy-start | bytes 3145732
  35.0 10.7 %copy-start.3 = (bf16[1,128,4096]{2,1,0:T(8,128)(2,1)S(1)}, bf16[1,128,4096]{2,1,0:T(8,128)(2,1)}, u32[]{:S(2)}) copy-start(bf16[1,128,4096]{2,1,0:T(8,128)(2,1)} %param.29) | copy-start | bytes 3145732
  45.1 109.3 %reduce-scatter.5.cloned.1.call-start = ((), (), s32[]{:S(2)}) async-start(), calls=%async_computation.5 | async-start | bytes 4718592 | tf_op jit(solution)/shard_map/reduce_scatter | solution.py:345
  45.2 2.7 %collective-permute-start.1 = (bf16[4096,128]{1,0:T(8,128)(2,1)S(1)}, bf16[4096,128]{1,0:T(8,128)(2,1)S(1)}, u32[]{:S(2)}, u32[]{:S(2)}) collective-permute-start(bf16[4096,128]{1,0:T(8,128)(2,1)S(1)} %bitcast.24), channel_id=1, source_target_pairs={{0,1},{1,0},{2,3},{3,2},{4,5},{5,4},{6,7},{7,6},{8,9},{9,8},{10,11... | collective-permute-start | bytes 3145736 | tf_op jit(solution)/shard_map/ppermute | solution.py:43
  45.4 4.0 %collective-permute-start.2 = (bf16[4096,128]{1,0:T(8,128)(2,1)S(1)}, bf16[4096,128]{1,0:T(8,128)(2,1)S(1)}, u32[]{:S(2)}, u32[]{:S(2)}) collective-permute-start(bf16[4096,128]{1,0:T(8,128)(2,1)S(1)} %bitcast.26), channel_id=1, source_target_pairs={{0,1},{1,0},{2,3},{3,2},{4,5},{5,4},{6,7},{7,6},{8,9},{9,8},{10,11... | collective-permute-start | bytes 3145736 | tf_op jit(solution)/shard_map/ppermute | solution.py:43
  45.8 5.3 %collective-permute-start.3 = (bf16[128,4096]{1,0:T(8,128)(2,1)S(1)}, bf16[128,4096]{1,0:T(8,128)(2,1)}, u32[]{:S(2)}, u32[]{:S(2)}) collective-permute-start(bf16[128,4096]{1,0:T(8,128)(2,1)S(1)} %bitcast.28), channel_id=1, source_target_pairs={{0,1},{1,0},{2,3},{3,2},{4,5},{5,4},{6,7},{7,6},{8,9},{9,8},{10,11... | collective-permute-start | bytes 3145736 | tf_op jit(solution)/shard_map/ppermute | solution.py:43
  47.9 1.5 copy-start.4
  49.4 1.0 copy-start.5
  94.6 0.7 copy-start.15
  94.6 0.7 copy-start.18
  94.6 0.8 copy-start.14
  156.5 17.4 %all-to-all-start.1 = ((bf16[16,128,128]{2,1,0:T(8,128)(2,1)}), bf16[16,128,128]{2,1,0:T(8,128)(2,1)S(1)}, u32[]{:S(2)}, u32[]{:S(2)}) async-start(bf16[16,128,128]{2,1,0:T(8,128)(2,1)} %reshape.80), calls=%async_computation.3 | async-start | bytes 1048576 | tf_op jit(solution)/shard_map/all_to_all | solution.py:322
Sparse Core Ops, SparseCore 0:
  45.2 41.7 reduce-scatter.2
  94.8 59.6 reduce-scatter.4

commit v5 on v4

--- a/solution.py
+++ b/solution.py
@@ -61,13 +61,13 @@
     return (values * inverse * gain).astype(jnp.bfloat16)
 
 
-def prep_kernel(zs, core_ref, tokens_ref, gain_ref, routes_ref, placed_ref, normed_ref, ranks_ref):
+def prep_kernel(zs, place_ref, tokens_ref, gain_ref, routes_ref, placed_ref, normed_ref, ranks_ref):
     share = MOE_SHARE
     rows = zs * share
     width = tokens_ref.shape[-1]
     normed_ref[...] = scaled_rows(tokens_ref[...].reshape(rows, width), gain_ref[...])
     token = iota((2 * rows, rows), 1)
-    source = (token // share) * (2 * share) + core_ref[0] * share + token % share
+    source = (token // share) * (2 * share) + place_ref[0] * share + token % share
     pick = select_matrix(iota((2 * rows, rows), 0) == source)
     routes = product(routes_ref[...].astype(jnp.float32).astype(jnp.bfloat16), pick).astype(jnp.int32)
     expert = iota((EXPERTS, rows), 0)
@@ -80,11 +80,15 @@
         for k in range(TOPK)
     ]
     block = iota((1, rows), 1) // share
-    slots = iota((EXPERTS * CAP * zs, rows), 0)
+    part = CAP // 2
+    slots = iota((EXPERTS * part * zs, rows), 0)
     inside = []
     for k in range(TOPK):
         ranks_ref[k : k + 1, :] = ranks[k]
-        inside.append(slots == (routes[k : k + 1] * CAP + ranks[k]) * zs + block)
+        slot = ranks[k] - part * (place_ref[1] % 2)
+        held = (slot >= 0) & (slot < part)
+        spot = (routes[k : k + 1] * part + slot) * zs + block
+        inside.append(slots == jnp.where(held, spot, -1))
     select = select_matrix(inside[0] | inside[1])
     step = 512
 
@@ -94,7 +98,7 @@
         placed_ref[:, columns] = product(select, normed_ref[:, columns]).astype(jnp.bfloat16)
 
 
-def prepare(core, tokens, gain, routes, zs):
+def prepare(place, tokens, gain, routes, zs):
     rows, width = tokens.shape
     half = rows // 2
     return pl.pallas_call(
@@ -108,24 +112,24 @@
                 pl.BlockSpec((TOPK, rows), lambda i, c: (0, 0)),
             ],
             out_specs=[
-                pl.BlockSpec((EXPERTS * CAP * zs, width), lambda i, c: (0, 0)),
+                pl.BlockSpec((EXPERTS * (CAP // 2) * zs, width), lambda i, c: (0, 0)),
                 pl.BlockSpec((half, width), lambda i, c: (0, 0)),
                 pl.BlockSpec((TOPK, half), lambda i, c: (0, 0)),
             ],
         ),
         out_shape=[
-            jax.ShapeDtypeStruct((EXPERTS * CAP * zs, width), jnp.bfloat16),
+            jax.ShapeDtypeStruct((EXPERTS * (CAP // 2) * zs, width), jnp.bfloat16),
             jax.ShapeDtypeStruct((half, width), jnp.bfloat16),
             jax.ShapeDtypeStruct((TOPK, half), jnp.int32),
         ],
         cost_estimate=pl.CostEstimate(
-            flops=2 * EXPERTS * CAP * zs * half * width,
-            bytes_accessed=2 * width * (rows + EXPERTS * CAP * zs),
+            flops=2 * EXPERTS * (CAP // 2) * zs * half * width,
+            bytes_accessed=2 * width * (rows + EXPERTS * (CAP // 2) * zs),
             transcendentals=0,
         ),
         name="prepare",
     )(
-        core,
+        place,
         tokens.reshape(zs, 2, MOE_SHARE, width),
         gain.reshape(1, width),
         routes.T,
@@ -228,60 +232,125 @@
     )(core, split, split, before, gain.reshape(1, width), *taps, *weights, *mixes)
 
 
-def expert_kernel(zs, steps, rows_ref, g0, g1, u0, u1, d0, d1, out_ref, sums_ref, units_ref):
+def gated_units(sums):
+    units = sums.shape[1] // 2
+    gate, up = sums[:, :units], sums[:, units:]
+    return (gate * jax.nn.sigmoid(gate) * up).astype(jnp.bfloat16)
+
+
+def units_kernel(steps, rows_ref, g0, g1, u0, u1, out_ref, sums_ref):
     step = pl.program_id(0)
-    count = rows_ref.shape[0]
-    units = 2 * g0.shape[1]
+    joint = jnp.concatenate([g0[...], g1[...], u0[...], u1[...]], axis=1)
+    piece = product(rows_ref[...], joint)
 
     @pl.when(step == 0)
     def _():
-        sums_ref[...] = jnp.zeros_like(sums_ref)
-
-    @pl.when(step < steps)
-    def _():
-        joint = jnp.concatenate([g0[...], g1[...], u0[...], u1[...]], axis=1)
-        sums_ref[...] += product(rows_ref[...], joint)
+        sums_ref[...] = piece
+
+    @pl.when(step > 0)
+    def _():
+        sums_ref[...] += piece
 
     @pl.when(step == steps - 1)
     def _():
-        target, source = iota((count, count), 0), iota((count, count), 1)
-        order = select_matrix(target == (source % zs) * (count // zs) + source // zs)
-        gate, up = sums_ref[:, :units], sums_ref[:, units:]
-        hidden = (gate * jax.nn.sigmoid(gate) * up).astype(jnp.bfloat16)
-        units_ref[...] = product(order, hidden).astype(jnp.bfloat16)
-
-    @pl.when(step >= steps)
-    def _():
-        joint = jnp.concatenate([d0[...], d1[...]], axis=0)
-        out_ref[...] = product(units_ref[...], joint).astype(jnp.bfloat16)
-
-
-def expert_partial(rows, weights, downs, zs):
+        out_ref[...] = gated_units(sums_ref[...])
+
+
+def expert_units(rows, weights):
     count, width = rows.shape
     half = weights[0].shape[1]
     depth = 1024
     steps = width // depth
+    return pl.pallas_call(
+        functools.partial(units_kernel, steps),
+        grid=(steps,),
+        in_specs=[pl.BlockSpec((count, depth), lambda i: (0, i))]
+        + [pl.BlockSpec((depth, half), lambda i: (i, 0))] * 4,
+        out_specs=pl.BlockSpec((count, 2 * half), lambda i: (0, 0)),
+        scratch_shapes=[pltpu.VMEM((count, 4 * half), jnp.float32)],
+        out_shape=jax.ShapeDtypeStruct((count, 2 * half), jnp.bfloat16),
+        cost_estimate=pl.CostEstimate(
+            flops=8 * width * half * count,
+            bytes_accessed=2 * width * (count + 4 * half),
+            transcendentals=2 * count * half,
+        ),
+        name="units",
+    )(rows, *weights)
+
+
+def expert_kernel(
+    zs, steps, place_ref, before_ref, after_ref, own_ref, g0, g1, u0, u1, d0, d1, out_ref,
+    sums_ref, units_ref
+):
+    step = pl.program_id(0)
+    count = own_ref.shape[0]
+    given = units_ref.shape[0]
+
+    @pl.when(step < steps)
+    def _():
+        joint = jnp.concatenate([g0[...], g1[...], u0[...], u1[...]], axis=1)
+        rows = jnp.concatenate([before_ref[...], after_ref[...]], axis=0)
+        piece = product(rows, joint)
+
+        @pl.when(step == 0)
+        def _():
+            sums_ref[...] = piece
+
+        @pl.when(step > 0)
+        def _():
+            sums_ref[...] += piece
+
+    @pl.when(step == steps - 1)
+    def _():
+        part = CAP // 2
+        target, source = iota((given, count), 0), iota((given, count), 1)
+        line = source // zs
+        first = (source % zs) * (given // zs) + (line // part) * CAP + line % part
+        odd = place_ref[1] % 2
+        own = select_matrix(target == first + part * odd)
+        other = select_matrix(target == first + part * (1 - odd))
+        units_ref[...] = (
+            product(own, own_ref[...]) + product(other, gated_units(sums_ref[...]))
+        ).astype(jnp.bfloat16)
+
+    @pl.when(step >= steps)
+    def _():
+        joint = jnp.concatenate([d0[...], d1[...]], axis=0)
+        out_ref[...] = product(units_ref[...], joint).astype(jnp.bfloat16)
+
+
+def expert_partial(place, before, after, own_units, weights, downs, zs):
+    rows, width = before.shape
+    count = own_units.shape[0]
+    given = 2 * count
+    half = weights[0].shape[1]
+    depth = 1024
+    steps = width // depth
     early = lambda i: jnp.minimum(i, steps - 1)
-    after = lambda i: jnp.maximum(i - steps, 0)
+    late = lambda i: jnp.maximum(i - steps, 0)
     return pl.pallas_call(
         functools.partial(expert_kernel, zs, steps),
-        grid=(2 * steps,),
-        in_specs=[pl.BlockSpec((count, depth), lambda i: (0, early(i)))]
-        + [pl.BlockSpec((depth, half), lambda i: (early(i), 0))] * 4
-        + [pl.BlockSpec((half, depth), lambda i: (0, after(i)))] * 2,
-        out_specs=pl.BlockSpec((count, depth), lambda i: (0, after(i))),
-        scratch_shapes=[
-            pltpu.VMEM((count, 4 * half), jnp.float32),
-            pltpu.VMEM((count, 2 * half), jnp.bfloat16),
-        ],
-        out_shape=jax.ShapeDtypeStruct((count, width), jnp.bfloat16),
+        grid_spec=pltpu.PrefetchScalarGridSpec(
+            num_scalar_prefetch=1,
+            grid=(2 * steps,),
+            in_specs=[pl.BlockSpec((rows, depth), lambda i, p: (0, early(i)))] * 2
+            + [pl.BlockSpec((count, 2 * half), lambda i, p: (0, 0))]
+            + [pl.BlockSpec((depth, half), lambda i, p: (early(i), 0))] * 4
+            + [pl.BlockSpec((half, depth), lambda i, p: (0, late(i)))] * 2,
+            out_specs=pl.BlockSpec((given, depth), lambda i, p: (0, late(i))),
+            scratch_shapes=[
+                pltpu.VMEM((count, 4 * half), jnp.float32),
+                pltpu.VMEM((given, 2 * half), jnp.bfloat16),
+            ],
+        ),
+        out_shape=jax.ShapeDtypeStruct((given, width), jnp.bfloat16),
         cost_estimate=pl.CostEstimate(
-            flops=12 * width * half * count,
-            bytes_accessed=2 * width * (2 * count + 6 * half),
+            flops=8 * width * half * count + 4 * width * half * given,
+            bytes_accessed=2 * width * (count + given + 6 * half),
             transcendentals=2 * count * half,
         ),
         name="experts",
-    )(rows, *weights, *downs)
+    )(place, before, after, own_units, *weights, *downs)
 
 
 def layer(
@@ -306,7 +375,7 @@
     zs = lax.axis_size("z")
     eps = lax.axis_size(EP)
     width = moe_tokens.shape[1]
-    core_ref = core.reshape(1).astype(jnp.int32)
+    core_ref = jnp.stack([core, z_index]).astype(jnp.int32)
 
     before = lax.ppermute(
         mix_tokens[mix_tokens.shape[0] - MOE_SHARE :], EP, [(i, i + 1) for i in range(eps - 1)]
@@ -321,7 +390,7 @@
     def exchange(array):
         return lax.all_to_all(array, EP, split_axis=0, concat_axis=0, tiled=True)
 
-    arrived = exchange(placed.reshape(EXPERTS, CAP * zs, width)).reshape(-1, width)
+    arrived = exchange(placed.reshape(EXPERTS, CAP // 2 * zs, width)).reshape(-1, width)
 
     taps = (conv_taps, swap_cores(conv_taps))
     projections = (
@@ -340,7 +409,13 @@
 
     weights = (gate, swap_cores(gate), up, swap_cores(up))
     downs = (down, swap_cores(down))
-    partial_value = expert_partial(arrived, weights, downs, zs)
+    middle = arrived.shape[0] // 2
+    from_before = lax.ppermute(arrived[:middle], "z", [(i, (i + 1) % zs) for i in range(zs)])
+    from_after = lax.ppermute(arrived[middle:], "z", [(i, (i - 1) % zs) for i in range(zs)])
+    own_units = expert_units(arrived, weights)
+    partial_value = expert_partial(
+        core_ref, from_before, from_after, own_units, weights, downs, zs
+    )
     partial_value, mixer_out = lax.optimization_barrier((partial_value, mixer_out))
     summed = lax.psum_scatter(partial_value, "z", scatter_dimension=0, tiled=True)
     returned = exchange(summed.reshape(eps, CAP * width // 128, 128)).reshape(-1, width)

time: 183 us -> 189 us (1.033)
  waiting for transfers between devices: 110 us -> 104 us
  starting transfers between devices: 20 us -> 25.7 us
  Pallas kernels: 26.7 us -> 31.4 us
    ppermute x0 -> x2, waiting for transfers between devices: none -> 27.1 us  [the longest x1 27.1 us: layer(): lax.ppermute(arrived[:middle], 'z', [(i, (i + 1) % zs) for i in range(zs)])]
    all_to_all x2, waiting for transfers between devices: 42.9 us -> 17.8 us  [exchange(): return lax.all_to_all(array, EP, split_axis=0, concat_axis=0, tiled=True)]
    ppermute x0 -> x2, starting transfers between devices: none -> 5.85 us  [the longest x1 3.94 us: layer(): lax.ppermute(arrived[middle:], 'z', [(i, (i - 1) % zs) for i in range(zs)])]
    pallas_call x1 -> x2, Pallas kernels: 10.5 us -> 15.2 us  [the longest x1 10.2 us: expert_partial(): pl.pallas_call(functools.partial(expert_kernel, zs, steps), grid_spec=plt...]
    reduce_scatter x1, waiting for transfers between devices: 56.9 us -> 53.1 us  [layer(): lax.psum_scatter(partial_value, 'z', scatter_dimension=0, tiled=True)]
    ppermute x8, waiting for transfers between devices: 10.2 us -> 6.39 us  [swap_cores(): return lax.ppermute(value, 'core', [(0, 1), (1, 0)])]
    unnamed x38 -> x22, local copies, waits for them, and re-layouts: 4.32 us -> 3.66 us
  transfers between devices with their start and end apart: 13 -> 15, of which waited for: 7 -> 5; matrix products, arithmetic and copies ran while one was open for 1% -> 2% of each run, Pallas kernels for 15% -> 17%
where the time goes in v5:
time: 189 us; the launch traced here: 188 us
  waiting for transfers between devices  104 us (55%)
  Pallas kernels  31.4 us (17%)
  starting transfers between devices  25.7 us (14%)
  between operations  14.2 us (8%)
  local copies, waits for them, and re-layouts  8.45 us (4%)
  matrix products  3.14 us (2%)
    reduce_scatter x1, waiting for transfers between devices, layer(): lax.psum_scatter(partial_value, 'z', scatter_dimension=0, tiled=True)  53.1 us
    ppermute x1, waiting for transfers between devices, layer(): lax.ppermute(arrived[:middle], 'z', [(i, (i + 1) % zs) for i in range(zs)])  27.1 us
    all_to_all x2, waiting for transfers between devices, exchange(): return lax.all_to_all(array, EP, split_axis=0, concat_axis=0, tiled=True)  17.8 us
    all_to_all x2, starting transfers between devices, exchange(): return lax.all_to_all(array, EP, split_axis=0, concat_axis=0, tiled=True)  14.5 us
    pallas_call x1, Pallas kernels, mixer_partial(): pl.pallas_call(functools.partial(mixer_kernel, steps), grid_spec=pltpu.Pr...  10.5 us
    pallas_call x1, Pallas kernels, expert_partial(): pl.pallas_call(functools.partial(expert_kernel, zs, steps), grid_spec=plt...  10.2 us
    ppermute x8, waiting for transfers between devices, swap_cores(): return lax.ppermute(value, 'core', [(0, 1), (1, 0)])  6.39 us
    pallas_call x1, Pallas kernels, prepare(): pl.pallas_call(functools.partial(prep_kernel, zs), grid_spec=pltpu.Prefet...  5.61 us
  transfers between devices with their start and end apart: 15, of which 5 were waited for; matrix products, arithmetic and copies ran while one was open for 2% of the time, Pallas kernels for 17%

profile of v5, /device:TPU:2, one launch (start us, length us, event | category | flops | bytes accessed | tf_op | source)
XLA Modules:
  0.0 188.2 jit_solution(15903907585914001365)
XLA Ops:
  7.2 0.0 copy-start
  7.2 1.0 slice.18
  8.1 3.4 %collective-permute-start = (bf16[16,4096]{1,0:T(8,128)(2,1)S(1)}, bf16[16,4096]{1,0:T(8,128)(2,1)S(1)}, u32[]{:S(2)}, u32[]{:S(2)}) collective-permute-start(bf16[16,4096]{1,0:T(8,128)(2,1)S(1)} %slice.18), channel_id=1, source_target_pairs={{0,16},{16,32},{32,48},{48,64},{64,80},{80,96},{96,112},{112,128},... | collective-permute-start | bytes 393224 | tf_op jit(solution)/shard_map/ppermute | solution.py:380
  11.5 0.6 pad_add_fusion.place_ref.core_ref
  12.1 5.6 %prepare.1 = (bf16[256,4096]{1,0:T(8,128)(2,1)}, bf16[128,4096]{1,0:T(8,128)(2,1)}, s32[2,128]{1,0:T(2,128)}) custom-call(s32[2]{0:T(128)} %pad_add_fusion.place_ref.core_ref, bf16[8,2,16,4096]{3,2,1,0:T(8,128)(2,1)} %bitcast.31, f32[1,4096]{1,0:T(1,128)} %bitcast.35, s32[2,256]{1,0:T(2,128)} %bitcast.37), custom_call_target="tpu_custom_call" | custom-call | flops 268435456 | bytes 4194304 | tf_op jit(solution)/shard_map/prepare/pallas_call | solution.py:104
  17.8 0.0 collective-permute-done.before_ref
  17.8 0.0 copy-start.5
  17.8 0.0 copy-start.8
  17.8 0.0 copy-start.2
  17.8 0.6 copy-done.5
  18.4 7.2 %all-to-all-start = ((bf16[16,16,4096]{2,1,0:T(8,128)(2,1)}), bf16[16,16,4096]{2,1,0:T(8,128)(2,1)S(1)}, u32[]{:S(2)}, u32[]{:S(2)}) async-start(bf16[16,16,4096]{2,1,0:T(8,128)(2,1)} %bitcast.32), calls=%async_computation | async-start | bytes 4194304 | tf_op jit(solution)/shard_map/all_to_all | solution.py:391
  25.6 0.0 reduce-scatter.3.cloned.1.call-start
  25.6 0.1 collective-permute-start.10
  25.7 0.5 collective-permute-start.7
  26.2 0.1 collective-permute-start.8
  26.3 0.4 collective-permute-start.9
  26.8 0.0 copy-done.8
  26.8 0.1 collective-permute-start.6
  26.9 6.4 %collective-permute-done.6.taps_theirs = f32[3,128]{1,0:T(4,128)S(1)} collective-permute-done((f32[3,128]{1,0:T(4,128)S(1)}, f32[3,128]{1,0:T(4,128)S(1)}, u32[]{:S(2)}, u32[]{:S(2)}) %collective-permute-start.6) | collective-permute-done | bytes 1568 | tf_op jit(solution)/shard_map/ppermute | solution.py:43
  33.2 0.0 copy-done.2
  33.2 0.1 collective-permute-start.3
  33.4 0.0 collective-permute-done.10.refs_7_
  33.4 0.4 collective-permute-start.4
  33.8 0.0 collective-permute-done.7.refs_1_
  33.8 0.1 collective-permute-start.5
  33.9 0.0 collective-permute-done.8.refs_3_
  33.9 0.0 collective-permute-done.9.refs_5_
  33.9 0.0 copy-done.9
  33.9 10.5 %mixer.1 = bf16[128,4096]{1,0:T(8,128)(2,1)} custom-call(s32[2]{0:T(128)} %pad_add_fusion.place_ref.core_ref, bf16[8,2,16,4096]{3,2,1,0:T(8,128)(2,1)} %bitcast.23, bf16[8,2,16,4096]{3,2,1,0:T(8,128)(2,1)} %bitcast.24, bf16[16,4096]{1,0:T(8,128)(2,1)} %copy-done.5, f32[1,4096]{1,0:T(1,128)} %bitcast.36, f32[3,128]{1,0:T(4,128)} %taps_mine.1, ...), custom_call_target="tpu_custom_call" | custom-call | flops 1577058304 | bytes 11141120 | tf_op jit(solution)/shard_map/mixer/pallas_call | solution.py:203
  44.4 0.0 reduce-scatter.3.cloned.1.call-update
  44.5 0.0 reduce-scatter.5.cloned.1.call-start
  44.5 7.9 %all-to-all-done = bf16[16,16,4096]{2,1,0:T(8,128)(2,1)S(1)} async-done(((bf16[16,16,4096]{2,1,0:T(8,128)(2,1)}), bf16[16,16,4096]{2,1,0:T(8,128)(2,1)S(1)}, u32[]{:S(2)}, u32[]{:S(2)}) %all-to-all-start) | async-done | bytes 2097184 | tf_op jit(solution)/shard_map/all_to_all | solution.py:391
  52.5 1.5 fusion.7
  54.0 0.5 copy-done.1
  54.4 1.9 %collective-permute-start.1 = (bf16[128,4096]{1,0:T(8,128)(2,1)}, bf16[128,4096]{1,0:T(8,128)(2,1)S(1)}, u32[]{:S(2)}, u32[]{:S(2)}) collective-permute-start(bf16[128,4096]{1,0:T(8,128)(2,1)} %bitcast.6), channel_id=1, source_target_pairs={{0,2},{2,4},{4,6},{6,8},{8,10},{10,12},{12,14},{14,0},{1,3},{3,5},... | collective-permute-start | bytes 3145736 | tf_op jit(solution)/shard_map/ppermute | solution.py:413
  56.4 3.9 %collective-permute-start.2 = (bf16[128,4096]{1,0:T(8,128)(2,1)}, bf16[128,4096]{1,0:T(8,128)(2,1)S(1)}, u32[]{:S(2)}, u32[]{:S(2)}) collective-permute-start(bf16[128,4096]{1,0:T(8,128)(2,1)} %bitcast.7), channel_id=1, source_target_pairs={{0,14},{2,0},{4,2},{6,4},{8,6},{10,8},{12,10},{14,12},{1,15},{3,1}... | collective-permute-start | bytes 3145736 | tf_op jit(solution)/shard_map/ppermute | solution.py:414
  60.3 0.0 collective-permute-done.3.g1
  60.3 0.0 collective-permute-done.4.u1
  60.3 5.0 %units.1.own_ref = bf16[256,256]{1,0:T(8,128)(2,1)} custom-call(bf16[256,4096]{1,0:T(8,128)(2,1)} %bitcast.22, bf16[4096,128]{1,0:T(8,128)(2,1)} %bitcast.25, bf16[4096,128]{1,0:T(8,128)(2,1)} %collective-permute-done.3.g1, bf16[4096,128]{1,0:T(8,128)(2,1)} %bitcast.29, bf16[4096,128]{1,0:T(8,128)(2,1)} %collective-permute-done.4.u1), custom_call_target="tpu_custom_call" | custom-call | flops 1073741824 | bytes 6291456 | tf_op jit(solution)/shard_map/units/pallas_call | solution.py:264
  65.3 0.0 collective-permute-done.5.d1
  65.3 27.1 %collective-permute-done.1.before_ref = bf16[128,4096]{1,0:T(8,128)(2,1)S(1)} collective-permute-done((bf16[128,4096]{1,0:T(8,128)(2,1)}, bf16[128,4096]{1,0:T(8,128)(2,1)S(1)}, u32[]{:S(2)}, u32[]{:S(2)}) %collective-permute-start.1) | collective-permute-done | bytes 1048608 | tf_op jit(solution)/shard_map/ppermute | solution.py:413
  92.4 0.0 collective-permute-done.2.after_ref
  92.4 1.0 copy-done.3
  93.4 1.0 copy-done.4
  94.4 10.2 %experts.1 = bf16[512,4096]{1,0:T(8,128)(2,1)} custom-call(s32[2]{0:T(128)} %pad_add_fusion.place_ref.core_ref, bf16[128,4096]{1,0:T(8,128)(2,1)} %copy-done.3, bf16[128,4096]{1,0:T(8,128)(2,1)} %copy-done.4, bf16[256,256]{1,0:T(8,128)(2,1)} %units.1.own_ref, bf16[4096,128]{1,0:T(8,128)(2,1)} %bitcast.26, bf16[4096,128]{1,0:T(8,128)(2,1)} %collective-permute-done.3.g1, ...), custom_call_target="tpu_custom_call" | custom-call | flops 2147483648 | bytes 12582912 | tf_op jit(solution)/shard_map/experts/pallas_call | solution.py:331
  104.6 0.0 copy-start.10
  104.6 0.0 copy-start.6
  104.6 0.0 reduce-scatter.3.cloned.1.call-done
  104.7 0.0 reduce-scatter.5.cloned.1.call-update
  104.7 0.6 copy-done.7
  105.3 0.0 copy-done.10
  105.3 0.1 bitcast_add_fusion
  105.4 0.0 copy-done.6
  105.4 1.1 fusion.6
  106.5 0.0 copy-done
  106.5 1.1 fusion
  107.5 53.1 %reduce-scatter.5.cloned.1.call-done = bf16[64,4096]{1,0:T(8,128)(2,1)} async-done(((bf16[512,4096]{1,0:T(8,128)(2,1)}), bf16[64,4096]{1,0:T(8,128)(2,1)}) %reduce-scatter.5.cloned.1.call-update) | async-done | bytes 524304 | tf_op jit(solution)/shard_map/reduce_scatter | solution.py:420
  160.6 2.1 %reshape.78 = bf16[16,128,128]{2,1,0:T(8,128)(2,1)} reshape(bf16[64,4096]{1,0:T(8,128)(2,1)} %reduce-scatter.5.cloned.1.call-done) | data formatting | bytes 1048576 | tf_op jit(solution)/shard_map/reshape | solution.py:421
  162.7 7.3 %all-to-all-start.1 = ((bf16[16,128,128]{2,1,0:T(8,128)(2,1)}), bf16[16,128,128]{2,1,0:T(8,128)(2,1)S(1)}, u32[]{:S(2)}, u32[]{:S(2)}) async-start(bf16[16,128,128]{2,1,0:T(8,128)(2,1)} %reshape.78), calls=%async_computation.3 | async-start | bytes 1048576 | tf_op jit(solution)/shard_map/all_to_all | solution.py:391
  170.0 0.2 select_reduce_fusion.1
  170.2 0.1 select_reduce_fusion
  170.3 9.8 %all-to-all-done.1 = bf16[16,128,128]{2,1,0:T(8,128)(2,1)S(1)} async-done(((bf16[16,128,128]{2,1,0:T(8,128)(2,1)}), bf16[16,128,128]{2,1,0:T(8,128)(2,1)S(1)}, u32[]{:S(2)}, u32[]{:S(2)}) %all-to-all-start.1) | async-done | bytes 524320 | tf_op jit(solution)/shard_map/all_to_all | solution.py:391
  180.1 0.2 reshape.79
  180.3 1.0 convolution_convert_fusion
  (9 shorter events, 0.1 us)
Async XLA Ops:
  7.2 99.3 %copy-start = (bf16[4096,16]{0,1:T(8,128)(2,1)S(1)}, bf16[4096,16]{0,1:T(8,128)(2,1)}, u32[]{:S(2)}) copy-start(bf16[4096,16]{0,1:T(8,128)(2,1)} %param.25) | copy-start | bytes 393220
  8.1 9.6 %collective-permute-start = (bf16[16,4096]{1,0:T(8,128)(2,1)S(1)}, bf16[16,4096]{1,0:T(8,128)(2,1)S(1)}, u32[]{:S(2)}, u32[]{:S(2)}) collective-permute-start(bf16[16,4096]{1,0:T(8,128)(2,1)S(1)} %slice.18), channel_id=1, source_target_pairs={{0,16},{16,32},{32,48},{48,64},{64,80},{80,96},{96,112},{112,128},... | collective-permute-start | bytes 393224 | tf_op jit(solution)/shard_map/ppermute | solution.py:380
  17.8 0.7 copy-start.5
  17.8 9.0 %copy-start.8 = (f32[3,128]{1,0:T(4,128)S(1)}, f32[3,128]{1,0:T(4,128)}, u32[]{:S(2)}) copy-start(f32[3,128]{1,0:T(4,128)} %taps_mine.1) | copy-start | bytes 4612
  17.8 15.5 %copy-start.2 = (bf16[1,4096,128]{2,1,0:T(8,128)(2,1)S(1)}, bf16[1,4096,128]{2,1,0:T(8,128)(2,1)}, u32[]{:S(2)}) copy-start(bf16[1,4096,128]{2,1,0:T(8,128)(2,1)} %param.27) | copy-start | bytes 3145732
  18.4 34.0 %all-to-all-start = ((bf16[16,16,4096]{2,1,0:T(8,128)(2,1)}), bf16[16,16,4096]{2,1,0:T(8,128)(2,1)S(1)}, u32[]{:S(2)}, u32[]{:S(2)}) async-start(bf16[16,16,4096]{2,1,0:T(8,128)(2,1)} %bitcast.32), calls=%async_computation | async-start | bytes 4194304 | tf_op jit(solution)/shard_map/all_to_all | solution.py:391
  25.6 79.0 %reduce-scatter.3.cloned.1.call-start = ((), (), s32[]{:S(2)}) async-start(), calls=%async_computation.4 | async-start | bytes 1179648 | tf_op jit(solution)/shard_map/reduce_scatter | solution.py:408
  25.6 7.7 %collective-permute-start.10 = (bf16[128,4096]{1,0:T(8,128)(2,1)}, bf16[128,4096]{1,0:T(8,128)(2,1)}, u32[]{:S(2)}, u32[]{:S(2)}) collective-permute-start(bf16[128,4096]{1,0:T(8,128)(2,1)} %refs_6_.1), channel_id=1, source_target_pairs={{0,1},{1,0},{2,3},{3,2},{4,5},{5,4},{6,7},{7,6},{8,9},{9,8},{10,11... | collective-permute-start | bytes 3145736 | tf_op jit(solution)/shard_map/ppermute | solution.py:43
  25.7 8.0 %collective-permute-start.7 = (bf16[4096,128]{1,0:T(8,128)(2,1)}, bf16[4096,128]{1,0:T(8,128)(2,1)}, u32[]{:S(2)}, u32[]{:S(2)}) collective-permute-start(bf16[4096,128]{1,0:T(8,128)(2,1)} %refs_0_.1), channel_id=1, source_target_pairs={{0,1},{1,0},{2,3},{3,2},{4,5},{5,4},{6,7},{7,6},{8,9},{9,8},{10,11... | collective-permute-start | bytes 3145736 | tf_op jit(solution)/shard_map/ppermute | solution.py:43
  26.2 7.7 %collective-permute-start.8 = (bf16[4096,128]{1,0:T(8,128)(2,1)}, bf16[4096,128]{1,0:T(8,128)(2,1)}, u32[]{:S(2)}, u32[]{:S(2)}) collective-permute-start(bf16[4096,128]{1,0:T(8,128)(2,1)} %refs_2_.1), channel_id=1, source_target_pairs={{0,1},{1,0},{2,3},{3,2},{4,5},{5,4},{6,7},{7,6},{8,9},{9,8},{10,11... | collective-permute-start | bytes 3145736 | tf_op jit(solution)/shard_map/ppermute | solution.py:43
  26.3 7.6 %collective-permute-start.9 = (bf16[4096,128]{1,0:T(8,128)(2,1)}, bf16[4096,128]{1,0:T(8,128)(2,1)}, u32[]{:S(2)}, u32[]{:S(2)}) collective-permute-start(bf16[4096,128]{1,0:T(8,128)(2,1)} %refs_4_.1), channel_id=1, source_target_pairs={{0,1},{1,0},{2,3},{3,2},{4,5},{5,4},{6,7},{7,6},{8,9},{9,8},{10,11... | collective-permute-start | bytes 3145736 | tf_op jit(solution)/shard_map/ppermute | solution.py:43
  26.8 6.5 %collective-permute-start.6 = (f32[3,128]{1,0:T(4,128)S(1)}, f32[3,128]{1,0:T(4,128)S(1)}, u32[]{:S(2)}, u32[]{:S(2)}) collective-permute-start(f32[3,128]{1,0:T(4,128)S(1)} %copy-done.8), channel_id=1, source_target_pairs={{0,1},{1,0},{2,3},{3,2},{4,5},{5,4},{6,7},{7,6},{8,9},{9,8},{10,11... | collective-permute-start | bytes 4616 | tf_op jit(solution)/shard_map/ppermute | solution.py:43
  33.2 0.7 copy-start.9
  33.2 27.1 %collective-permute-start.3 = (bf16[4096,128]{1,0:T(8,128)(2,1)S(1)}, bf16[4096,128]{1,0:T(8,128)(2,1)}, u32[]{:S(2)}, u32[]{:S(2)}) collective-permute-start(bf16[4096,128]{1,0:T(8,128)(2,1)S(1)} %bitcast.27), channel_id=1, source_target_pairs={{0,1},{1,0},{2,3},{3,2},{4,5},{5,4},{6,7},{7,6},{8,9},{9,8},{10,11... | collective-permute-start | bytes 3145736 | tf_op jit(solution)/shard_map/ppermute | solution.py:43
  33.4 26.9 %collective-permute-start.4 = (bf16[4096,128]{1,0:T(8,128)(2,1)}, bf16[4096,128]{1,0:T(8,128)(2,1)}, u32[]{:S(2)}, u32[]{:S(2)}) collective-permute-start(bf16[4096,128]{1,0:T(8,128)(2,1)} %bitcast.28), channel_id=1, source_target_pairs={{0,1},{1,0},{2,3},{3,2},{4,5},{5,4},{6,7},{7,6},{8,9},{9,8},{10,11... | collective-permute-start | bytes 3145736 | tf_op jit(solution)/shard_map/ppermute | solution.py:43
  33.8 31.6 %collective-permute-start.5 = (bf16[128,4096]{1,0:T(8,128)(2,1)}, bf16[128,4096]{1,0:T(8,128)(2,1)}, u32[]{:S(2)}, u32[]{:S(2)}) collective-permute-start(bf16[128,4096]{1,0:T(8,128)(2,1)} %bitcast.33), channel_id=1, source_target_pairs={{0,1},{1,0},{2,3},{3,2},{4,5},{5,4},{6,7},{7,6},{8,9},{9,8},{10,11... | collective-permute-start | bytes 3145736 | tf_op jit(solution)/shard_map/ppermute | solution.py:43
  44.5 116.2 %reduce-scatter.5.cloned.1.call-start = ((), (), s32[]{:S(2)}) async-start(), calls=%async_computation.5 | async-start | bytes 4718592 | tf_op jit(solution)/shard_map/reduce_scatter | solution.py:420
  52.5 2.0 %copy-start.1 = (bf16[16,16,4096]{2,1,0:T(8,128)(2,1)}, bf16[16,16,4096]{2,1,0:T(8,128)(2,1)S(1)}, u32[]{:S(2)}) copy-start(bf16[16,16,4096]{2,1,0:T(8,128)(2,1)S(1)} %all-to-all-done) | copy-start | bytes 6291460
  54.4 38.0 %collective-permute-start.1 = (bf16[128,4096]{1,0:T(8,128)(2,1)}, bf16[128,4096]{1,0:T(8,128)(2,1)S(1)}, u32[]{:S(2)}, u32[]{:S(2)}) collective-permute-start(bf16[128,4096]{1,0:T(8,128)(2,1)} %bitcast.6), channel_id=1, source_target_pairs={{0,2},{2,4},{4,6},{6,8},{8,10},{10,12},{12,14},{14,0},{1,3},{3,5},... | collective-permute-start | bytes 3145736 | tf_op jit(solution)/shard_map/ppermute | solution.py:413
  56.4 36.1 %collective-permute-start.2 = (bf16[128,4096]{1,0:T(8,128)(2,1)}, bf16[128,4096]{1,0:T(8,128)(2,1)S(1)}, u32[]{:S(2)}, u32[]{:S(2)}) collective-permute-start(bf16[128,4096]{1,0:T(8,128)(2,1)} %bitcast.7), channel_id=1, source_target_pairs={{0,14},{2,0},{4,2},{6,4},{8,6},{10,8},{12,10},{14,12},{1,15},{3,1}... | collective-permute-start | bytes 3145736 | tf_op jit(solution)/shard_map/ppermute | solution.py:414
  92.4 1.0 copy-start.3
  93.4 1.0 copy-start.4
  104.6 0.7 copy-start.7
  104.6 0.7 copy-start.10
  104.6 0.8 copy-start.6
  162.7 17.4 %all-to-all-start.1 = ((bf16[16,128,128]{2,1,0:T(8,128)(2,1)}), bf16[16,128,128]{2,1,0:T(8,128)(2,1)S(1)}, u32[]{:S(2)}, u32[]{:S(2)}) async-start(bf16[16,128,128]{2,1,0:T(8,128)(2,1)} %reshape.78), calls=%async_computation.3 | async-start | bytes 1048576 | tf_op jit(solution)/shard_map/all_to_all | solution.py:391
Sparse Core Ops, SparseCore 0:
  44.6 45.2 reduce-scatter.2
  104.8 55.8 reduce-scatter.4

commit v6 on v4

--- a/solution.py
+++ b/solution.py
@@ -18,6 +18,8 @@
 CAP = 4
 
 
+MIX_CHAINS = 2
+
 EP = ("y", "x")
 TP = ("z", "core")
 ALL = EP + TP
@@ -43,6 +45,10 @@
     return lax.ppermute(value, "core", [(0, 1), (1, 0)])
 
 
+def swap_late(value):
+    return lax.ppermute(value, "core", [(0, 1), (1, 0)])
+
+
 def iota(shape, dim):
     return lax.broadcasted_iota(jnp.int32, shape, dim)
 
@@ -61,71 +67,83 @@
     return (values * inverse * gain).astype(jnp.bfloat16)
 
 
-def prep_kernel(zs, core_ref, tokens_ref, gain_ref, routes_ref, placed_ref, normed_ref, ranks_ref):
+def prep_kernel(
+    zs, place_ref, tokens_ref, gain_ref, routes_ref, placed_ref, own_ref, ranks_ref,
+    normed_ref, select_ref
+):
     share = MOE_SHARE
     rows = zs * share
     width = tokens_ref.shape[-1]
-    normed_ref[...] = scaled_rows(tokens_ref[...].reshape(rows, width), gain_ref[...])
-    token = iota((2 * rows, rows), 1)
-    source = (token // share) * (2 * share) + core_ref[0] * share + token % share
-    pick = select_matrix(iota((2 * rows, rows), 0) == source)
-    routes = product(routes_ref[...].astype(jnp.float32).astype(jnp.bfloat16), pick).astype(jnp.int32)
-    expert = iota((EXPERTS, rows), 0)
-    named = [expert == routes[k : k + 1] for k in range(TOPK)]
-    earlier, later = iota((rows, rows), 0), iota((rows, rows), 1)
-    before = (earlier // share == later // share) & (earlier < later)
-    counts = product(select_matrix(named[0] | named[1]), select_matrix(before))
-    ranks = [
-        jnp.sum(jnp.where(named[k], counts, 0.0), axis=0, keepdims=True).astype(jnp.int32)
-        for k in range(TOPK)
-    ]
-    block = iota((1, rows), 1) // share
-    slots = iota((EXPERTS * CAP * zs, rows), 0)
-    inside = []
-    for k in range(TOPK):
-        ranks_ref[k : k + 1, :] = ranks[k]
-        inside.append(slots == (routes[k : k + 1] * CAP + ranks[k]) * zs + block)
-    select = select_matrix(inside[0] | inside[1])
-    step = 512
-
-    @pl.loop(0, width // step)
-    def _(index):
-        columns = pl.ds(pl.multiple_of(index * step, step), step)
-        placed_ref[:, columns] = product(select, normed_ref[:, columns]).astype(jnp.bfloat16)
-
-
-def prepare(core, tokens, gain, routes, zs):
+    step = pl.program_id(0)
+
+    @pl.when(step == 0)
+    def _():
+        normed_ref[...] = scaled_rows(tokens_ref[...].reshape(rows, width), gain_ref[...])
+        own_ref[...] = normed_ref[pl.ds(pl.multiple_of(place_ref[1] * share, share), share), :]
+        token = iota((1, rows), 1)
+        block = token // share
+        source = block * (2 * share) + place_ref[0] * share + token % share
+        pick = select_matrix(iota((2 * rows, 1), 0) == source)
+        routes = routes_ref[...].astype(jnp.float32).astype(jnp.bfloat16)
+        routes = product(routes, pick).astype(jnp.int32)
+        expert = iota((EXPERTS, 1), 0)
+        named = [expert == routes[k : k + 1] for k in range(TOPK)]
+        earlier = iota((rows, 1), 0)
+        before = (earlier // share == block) & (earlier < token)
+        counts = product(select_matrix(named[0] | named[1]), select_matrix(before))
+        slots = iota((EXPERTS * CAP * zs, 1), 0)
+        inside = []
+        for k in range(TOPK):
+            ranks = jnp.sum(jnp.where(named[k], counts, 0.0), axis=0, keepdims=True)
+            ranks = ranks.astype(jnp.int32)
+            ranks_ref[k : k + 1, :] = ranks
+            inside.append(slots == (routes[k : k + 1] * CAP + ranks) * zs + block)
+        select_ref[...] = select_matrix(inside[0] | inside[1])
+
+    depth = placed_ref.shape[1]
+    columns = pl.ds(pl.multiple_of(step * depth, depth), depth)
+    placed_ref[...] = product(select_ref[...], normed_ref[:, columns]).astype(jnp.bfloat16)
+
+
+def prepare(place, tokens, gain, routes, zs):
     rows, width = tokens.shape
     half = rows // 2
+    depth = 1024
+    placed = EXPERTS * CAP * zs
+    fixed = lambda i, p: (0, 0)
     return pl.pallas_call(
         functools.partial(prep_kernel, zs),
         grid_spec=pltpu.PrefetchScalarGridSpec(
             num_scalar_prefetch=1,
-            grid=(1,),
+            grid=(width // depth,),
             in_specs=[
-                pl.BlockSpec((zs, 1, MOE_SHARE, width), lambda i, c: (0, c[0], 0, 0)),
-                pl.BlockSpec((1, width), lambda i, c: (0, 0)),
-                pl.BlockSpec((TOPK, rows), lambda i, c: (0, 0)),
+                pl.BlockSpec((zs, 1, MOE_SHARE, width), lambda i, p: (0, p[0], 0, 0)),
+                pl.BlockSpec((1, width), fixed),
+                pl.BlockSpec((TOPK, rows), fixed),
             ],
             out_specs=[
-                pl.BlockSpec((EXPERTS * CAP * zs, width), lambda i, c: (0, 0)),
-                pl.BlockSpec((half, width), lambda i, c: (0, 0)),
-                pl.BlockSpec((TOPK, half), lambda i, c: (0, 0)),
+                pl.BlockSpec((placed, depth), lambda i, p: (0, i)),
+                pl.BlockSpec((MOE_SHARE, width), fixed),
+                pl.BlockSpec((TOPK, half), fixed),
             ],
+            scratch_shapes=[
+                pltpu.VMEM((half, width), jnp.bfloat16),
+                pltpu.VMEM((placed, half), jnp.bfloat16),
+            ],
         ),
         out_shape=[
-            jax.ShapeDtypeStruct((EXPERTS * CAP * zs, width), jnp.bfloat16),
-            jax.ShapeDtypeStruct((half, width), jnp.bfloat16),
+            jax.ShapeDtypeStruct((placed, width), jnp.bfloat16),
+            jax.ShapeDtypeStruct((MOE_SHARE, width), jnp.bfloat16),
             jax.ShapeDtypeStruct((TOPK, half), jnp.int32),
         ],
         cost_estimate=pl.CostEstimate(
-            flops=2 * EXPERTS * CAP * zs * half * width,
-            bytes_accessed=2 * width * (rows + EXPERTS * CAP * zs),
+            flops=2 * placed * half * width,
+            bytes_accessed=2 * width * (half + placed),
             transcendentals=0,
         ),
         name="prepare",
     )(
-        core,
+        place,
         tokens.reshape(zs, 2, MOE_SHARE, width),
         gain.reshape(1, width),
         routes.T,
@@ -133,11 +151,12 @@
 
 
 def mixer_kernel(
-    steps, core_ref, tokens_ref, halo_ref, before_ref, gain_ref, taps_mine, taps_theirs, *refs
+    steps, place_ref, tokens_ref, halo_ref, before_ref, gain_ref, taps_mine, taps_theirs, *refs
 ):
-    weights, (m0, m1, out_ref, normed_ref, sums_ref, channels_ref) = refs[:6], refs[6:]
+    weights, (m0, m1), outs = refs[:6], refs[6:8], refs[8:-3]
+    normed_ref, sums_ref, channels_ref = refs[-3:]
     step = pl.program_id(0)
-    rows = out_ref.shape[0]
+    rows = channels_ref.shape[0]
     depth, half = weights[0].shape
     width = tokens_ref.shape[-1]
     blocks, _, tail_rows, _ = halo_ref.shape
@@ -165,9 +184,9 @@
             return sums_ref[:, 2 * index * half : 2 * (index + 1) * half]
 
         gated = (pair(1) * pair(0)).astype(jnp.bfloat16)
-        row, source = iota((rows, total), 0), iota((rows, total), 1)
+        row, source = iota((rows, 1), 0), iota((1, total), 1)
         place = row % MOE_SHARE
-        ahead = row // MOE_SHARE + core_ref[0]
+        ahead = row // MOE_SHARE + place_ref[0]
         tail = jnp.where(ahead == 0, total, rows + ahead * tail_rows)
         taps = jnp.concatenate([taps_mine[...], taps_theirs[...]], axis=1)
         mixed = None
@@ -177,15 +196,58 @@
             shifted = product(select_matrix(source == wanted), gated)
             term = taps[tap : tap + 1] * shifted
             mixed = term if mixed is None else mixed + term
-        channels_ref[...] = (pair(2)[0:rows] * mixed).astype(jnp.bfloat16)
-
-    @pl.when(step >= steps)
-    def _():
-        joint = jnp.concatenate([m0[...], m1[...]], axis=0)
-        out_ref[...] = product(channels_ref[...], joint).astype(jnp.bfloat16)
-
-
-def mixer_partial(core, tokens, before, gain, taps, weights, mixes, zs):
+        channels = (pair(2)[0:rows] * mixed).astype(jnp.bfloat16)
+        target, source = iota((rows, 1), 0), iota((1, rows), 1)
+        turned = (source // MOE_SHARE - place_ref[1] + blocks) % blocks
+        order = select_matrix(target == turned * MOE_SHARE + source % MOE_SHARE)
+        channels_ref[...] = product(order, channels).astype(jnp.bfloat16)
+
+    write_chains(step - steps, MOE_SHARE, outs, lambda: product(
+        channels_ref[...], jnp.concatenate([m0[...], m1[...]], axis=0)
+    ))
+
+
+def write_chains(step, rows, outs, compute):
+    chains = len(outs) // 2
+    pieces = chains * outs[0].shape[1] // 1024
+    for piece in range(pieces):
+        chain = piece * chains // pieces
+        whole, sent = outs[chain], outs[chains + chain]
+        start = (piece * 1024) % whole.shape[1]
+        first = whole.shape[0] - rows if chain % 2 == 0 else rows
+
+        @pl.when(step == piece)
+        def _():
+            total = compute().astype(jnp.bfloat16)
+            whole[:, start : start + 1024] = total
+            sent[:, start : start + 1024] = total[first : first + rows]
+
+
+def chain_outputs(count, rows, width, chains):
+    shapes = [(count, width // chains)] * chains + [(rows, width // chains)] * chains
+    return (
+        [pl.BlockSpec(shape, lambda *_: (0, 0)) for shape in shapes],
+        [jax.ShapeDtypeStruct(shape, jnp.bfloat16) for shape in shapes],
+    )
+
+
+def ring_sum(outs):
+    chains = len(outs) // 2
+    wholes, sums = outs[:chains], list(outs[chains:])
+    rows = sums[0].shape[0]
+    zs = lax.axis_size("z")
+    for hop in range(zs - 1):
+        for chain in range(chains):
+            way = 1 if chain % 2 == 0 else -1
+            came = lax.ppermute(sums[chain], "z", [(i, (i + way) % zs) for i in range(zs)])
+            block = (zs - 2 - hop) if way == 1 else (hop + 2) % zs
+            mine = wholes[chain][block * rows : (block + 1) * rows]
+            total = came.astype(jnp.float32) + mine.astype(jnp.float32)
+            sums[chain] = total.astype(jnp.bfloat16)
+    return sums
+
+
+def mixer_partial(place, tokens, before, gain, taps, weights, mixes, zs):
     rows, width = tokens.shape
     half = rows // 2
     channels = weights[0].shape[1]
@@ -195,6 +257,7 @@
     total = half + zs * tail_rows + before.shape[0]
     fixed = lambda i, c: (0, 0)
     after = lambda i, c: (0, jnp.maximum(i - steps, 0))
+    out_specs, out_shape = chain_outputs(half, MOE_SHARE, width, MIX_CHAINS)
     split = tokens.reshape(zs, 2, MOE_SHARE, width)
     return pl.pallas_call(
         functools.partial(mixer_kernel, steps),
@@ -211,21 +274,21 @@
             ]
             + [pl.BlockSpec((depth, channels), lambda i, c: (jnp.minimum(i, steps - 1), 0))] * 6
             + [pl.BlockSpec((channels, depth), after)] * 2,
-            out_specs=pl.BlockSpec((half, depth), after),
+            out_specs=out_specs,
             scratch_shapes=[
                 pltpu.VMEM((total, width), jnp.bfloat16),
                 pltpu.VMEM((total, 6 * channels), jnp.float32),
                 pltpu.VMEM((half, 2 * channels), jnp.bfloat16),
             ],
         ),
-        out_shape=jax.ShapeDtypeStruct((half, width), jnp.bfloat16),
+        out_shape=out_shape,
         cost_estimate=pl.CostEstimate(
             flops=2 * width * channels * (6 * total + 2 * half),
             bytes_accessed=2 * width * (total + half + 8 * channels),
             transcendentals=0,
         ),
         name="mixer",
-    )(core, split, split, before, gain.reshape(1, width), *taps, *weights, *mixes)
+    )(place, split, split, before, gain.reshape(1, width), *taps, *weights, *mixes)
 
 
 def expert_kernel(zs, steps, rows_ref, g0, g1, u0, u1, d0, d1, out_ref, sums_ref, units_ref):
@@ -244,7 +307,7 @@
 
     @pl.when(step == steps - 1)
     def _():
-        target, source = iota((count, count), 0), iota((count, count), 1)
+        target, source = iota((count, 1), 0), iota((1, count), 1)
         order = select_matrix(target == (source % zs) * (count // zs) + source // zs)
         gate, up = sums_ref[:, :units], sums_ref[:, units:]
         hidden = (gate * jax.nn.sigmoid(gate) * up).astype(jnp.bfloat16)
@@ -306,49 +369,53 @@
     zs = lax.axis_size("z")
     eps = lax.axis_size(EP)
     width = moe_tokens.shape[1]
-    core_ref = core.reshape(1).astype(jnp.int32)
-
+    core_ref = jnp.stack([core, z_index]).astype(jnp.int32)
+
+    gate, up, down = gate_weight[0], up_weight[0], down_weight[0]
+    theirs = [swap_cores(array) for array in (gate, up, down)]
+
+    placed, own_normed, half_ranks = prepare(
+        core_ref, moe_tokens, moe_gain, expert_routes, zs
+    )
+    placed, own_normed, half_ranks, theirs = lax.optimization_barrier(
+        (placed, own_normed, half_ranks, theirs)
+    )
+
+    def exchange(array):
+        return lax.all_to_all(array, EP, split_axis=0, concat_axis=0, tiled=True)
+
+    arrived = exchange(placed.reshape(EXPERTS, CAP * zs, width)).reshape(-1, width)
+    partial_value = expert_partial(arrived, (gate, theirs[0], up, theirs[1]), (down, theirs[2]), zs)
+    summed = lax.psum_scatter(partial_value, "z", scatter_dimension=0, tiled=True)
+
+    _, later = lax.optimization_barrier(
+        (
+            partial_value,
+            (
+                mix_tokens,
+                (value_weight, inner_weight, outer_weight),
+                (conv_taps, mix_weight),
+                own_normed,
+                half_ranks,
+                expert_routes,
+            ),
+        )
+    )
+    mix_tokens, projections, (conv_taps, mix_weight), own_normed, half_ranks, expert_routes = later
     before = lax.ppermute(
         mix_tokens[mix_tokens.shape[0] - MOE_SHARE :], EP, [(i, i + 1) for i in range(eps - 1)]
     )
-    gate, up, down = gate_weight[0], up_weight[0], down_weight[0]
-
-    placed, half_normed, half_ranks = prepare(
-        core_ref, moe_tokens, moe_gain, expert_routes, zs
-    )
-    placed, before = lax.optimization_barrier((placed, before))
-
-    def exchange(array):
-        return lax.all_to_all(array, EP, split_axis=0, concat_axis=0, tiled=True)
-
-    arrived = exchange(placed.reshape(EXPERTS, CAP * zs, width)).reshape(-1, width)
-
-    taps = (conv_taps, swap_cores(conv_taps))
-    projections = (
-        value_weight,
-        swap_cores(value_weight),
-        inner_weight,
-        swap_cores(inner_weight),
-        outer_weight,
-        swap_cores(outer_weight),
-    )
-    mixes = (mix_weight, swap_cores(mix_weight))
-    partial_mix = mixer_partial(
-        core_ref, mix_tokens, before, mix_gain, taps, projections, mixes, zs
-    )
-    mixer_out = lax.psum_scatter(partial_mix, "z", scatter_dimension=0, tiled=True)
-
-    weights = (gate, swap_cores(gate), up, swap_cores(up))
-    downs = (down, swap_cores(down))
-    partial_value = expert_partial(arrived, weights, downs, zs)
-    partial_value, mixer_out = lax.optimization_barrier((partial_value, mixer_out))
-    summed = lax.psum_scatter(partial_value, "z", scatter_dimension=0, tiled=True)
+    taps = (conv_taps, swap_late(conv_taps))
+    weights = [part for array in projections for part in (array, swap_late(array))]
+    mixes = (mix_weight, swap_late(mix_weight))
+    partial_mix = mixer_partial(core_ref, mix_tokens, before, mix_gain, taps, weights, mixes, zs)
+    mixer_out = jnp.concatenate(ring_sum(partial_mix), axis=1)
+    summed, mixer_out = lax.optimization_barrier((summed, mixer_out))
     returned = exchange(summed.reshape(eps, CAP * width // 128, 128)).reshape(-1, width)
 
     own_routes = lax.dynamic_slice_in_dim(
         expert_routes, (2 * z_index + core) * MOE_SHARE, MOE_SHARE, 0
     )
-    own_normed = lax.dynamic_slice_in_dim(half_normed, z_index * MOE_SHARE, MOE_SHARE, 0)
     own_ranks = lax.dynamic_slice_in_dim(half_ranks, z_index * MOE_SHARE, MOE_SHARE, 1).T
     token_weights = route_weights(own_normed, own_routes, router_group, router_expert)
 

time: 183 us -> 193 us (1.055)
  waiting for transfers between devices: 110 us -> 32.3 us
  blocking collectives: 0 us -> 58 us
  starting transfers between devices: 20 us -> 37.3 us
  other arithmetic: 0.35 us -> 14.2 us
  local copies, waits for them, and re-layouts: 7.57 us -> 5.49 us
    all_to_all x0 -> x1, blocking collectives: none -> 58 us  [exchange(): return lax.all_to_all(array, EP, split_axis=0, concat_axis=0, tiled=True)]
    reduce_scatter x1, waiting for transfers between devices: 56.9 us -> 0.01 us  [layer(): lax.psum_scatter(partial_value, 'z', scatter_dimension=0, tiled=True)]
    all_to_all x2 -> x1, waiting for transfers between devices: 42.9 us -> 8.51 us  [exchange(): return lax.all_to_all(array, EP, split_axis=0, concat_axis=0, tiled=True)]
    ppermute x0 -> x19, starting transfers between devices: none -> 27.8 us  [the longest x14 26.9 us: ring_sum(): lax.ppermute(sums[chain], 'z', [(i, (i + way) % zs) for i in range(zs)])]
    ppermute x0 -> x19, waiting for transfers between devices: none -> 18.9 us  [the longest x14 14.1 us: ring_sum(): lax.ppermute(sums[chain], 'z', [(i, (i + way) % zs) for i in range(zs)])]
    convert_element_type x0 -> x14, other arithmetic: none -> 12 us  [ring_sum(): sums[chain] = total.astype(jnp.bfloat16)]
    ppermute x8 -> x3, waiting for transfers between devices: 10.2 us -> 0.01 us  [swap_cores(): return lax.ppermute(value, 'core', [(0, 1), (1, 0)])]
    all_to_all x2 -> x1, starting transfers between devices: 14.6 us -> 6.83 us  [exchange(): return lax.all_to_all(array, EP, split_axis=0, concat_axis=0, tiled=True)]
  transfers between devices with their start and end apart: 13 -> 25, of which waited for: 7 -> 10; matrix products, arithmetic and copies ran while one was open for 1% -> 8% of each run, Pallas kernels for 15% -> 9%
where the time goes in v6:
time: 193 us; the launch traced here: 190 us
  blocking collectives  58 us (30%)
  starting transfers between devices  37.3 us (19%)
  waiting for transfers between devices  32.3 us (17%)
  Pallas kernels  27.5 us (14%)
  between operations  14.3 us (7%)
  other arithmetic  14.2 us (7%)
  local copies, waits for them, and re-layouts  5.49 us (3%)
    all_to_all x1, blocking collectives, exchange(): return lax.all_to_all(array, EP, split_axis=0, concat_axis=0, tiled=True)  58 us
    ppermute x14, starting transfers between devices, ring_sum(): lax.ppermute(sums[chain], 'z', [(i, (i + way) % zs) for i in range(zs)])  26.9 us
    ppermute x14, waiting for transfers between devices, ring_sum(): lax.ppermute(sums[chain], 'z', [(i, (i + way) % zs) for i in range(zs)])  14.1 us
    convert_element_type x14, other arithmetic, ring_sum(): sums[chain] = total.astype(jnp.bfloat16)  12 us
    pallas_call x1, Pallas kernels, mixer_partial(): pl.pallas_call(functools.partial(mixer_kernel, steps), grid_spec=pltpu.Pr...  11.1 us
    pallas_call x1, Pallas kernels, expert_partial(): pl.pallas_call(functools.partial(expert_kernel, zs, steps), grid=(2 * ste...  10.5 us
    all_to_all x1, waiting for transfers between devices, exchange(): return lax.all_to_all(array, EP, split_axis=0, concat_axis=0, tiled=True)  8.51 us
    all_to_all x1, starting transfers between devices, exchange(): return lax.all_to_all(array, EP, split_axis=0, concat_axis=0, tiled=True)  6.83 us
  transfers between devices with their start and end apart: 25, of which 10 were waited for; matrix products, arithmetic and copies ran while one was open for 8% of the time, Pallas kernels for 9%

profile of v6, /device:TPU:2, one launch (start us, length us, event | category | flops | bytes accessed | tf_op | source)
XLA Modules:
  0.0 190.4 jit_solution(595924121766060143)
XLA Ops:
  7.2 0.1 collective-permute-start
  7.3 0.5 collective-permute-start.1
  7.8 0.1 collective-permute-start.2
  7.9 0.6 pad_add_fusion.place_ref
  8.5 5.9 %prepare.1 = (bf16[512,4096]{1,0:T(8,128)(2,1)}, bf16[16,4096]{1,0:T(8,128)(2,1)}, s32[2,128]{1,0:T(2,128)}) custom-call(s32[2]{0:T(128)} %pad_add_fusion.place_ref, bf16[8,2,16,4096]{3,2,1,0:T(8,128)(2,1)} %bitcast.26, f32[1,4096]{1,0:T(1,128)} %bitcast.33, s32[2,256]{1,0:T(2,128)} %bitcast.35), custom_call_target="tpu_custom_call" | custom-call | flops 536870912 | bytes 5242880 | tf_op jit(solution)/shard_map/prepare/pallas_call | solution.py:114
  14.5 58.0 %all_to_all.10 = bf16[16,32,4096]{2,1,0:T(8,128)(2,1)} all-to-all(bf16[16,32,4096]{2,1,0:T(8,128)(2,1)} %bitcast.25), channel_id=1, replica_groups=mesh['y'=4,'x'=4,'z'=8,'core'=2] {'y','x'}, dimensions={0} | all-to-all | bytes 8388608 | tf_op jit(solution)/shard_map/all_to_all | solution.py:385
  72.4 10.5 %experts.1 = bf16[512,4096]{1,0:T(8,128)(2,1)} custom-call(bf16[512,4096]{1,0:T(8,128)(2,1)} %bitcast.22, bf16[4096,128]{1,0:T(8,128)(2,1)} %bitcast.28, bf16[4096,128]{1,0:T(8,128)(2,1)} %copy-done.1, bf16[4096,128]{1,0:T(8,128)(2,1)} %bitcast.30, bf16[4096,128]{1,0:T(8,128)(2,1)} %copy-done.2, bf16[128,4096]{1,0:T(8,128)(2,1)} %bitcast.32, ...), custom_call_target="tpu_custom_call" | custom-call | flops 3221225472 | bytes 14680064 | tf_op jit(solution)/shard_map/experts/pallas_call | solution.py:329
  83.0 1.1 copy-done.4
  84.2 0.3 copy-done.5
  84.5 0.2 collective-permute-start.6
  84.7 0.1 copy-done.6
  84.8 0.2 collective-permute-start.7
  85.0 0.3 collective-permute-start.8
  85.3 0.2 collective-permute-start.4
  85.5 0.2 fusion.2
  85.7 0.1 bitcast_add_fusion
  85.8 0.9 slice.48
  86.7 4.8 %collective-permute-done.4.taps_theirs = f32[3,128]{1,0:T(4,128)} collective-permute-done((f32[3,128]{1,0:T(4,128)S(1)}, f32[3,128]{1,0:T(4,128)}, u32[]{:S(2)}, u32[]{:S(2)}) %collective-permute-start.4) | collective-permute-done | bytes 1568 | tf_op jit(solution)/shard_map/ppermute | solution.py:49
  91.5 1.9 %collective-permute-start.3 = (bf16[16,4096]{1,0:T(8,128)(2,1)S(1)}, bf16[16,4096]{1,0:T(8,128)(2,1)S(1)}, u32[]{:S(2)}, u32[]{:S(2)}) collective-permute-start(bf16[16,4096]{1,0:T(8,128)(2,1)S(1)} %slice.48), channel_id=1, source_target_pairs={{0,16},{16,32},{32,48},{48,64},{64,80},{80,96},{96,112},{112,128},... | collective-permute-start | bytes 393224 | tf_op jit(solution)/shard_map/ppermute | solution.py:405
  93.4 0.6 fusion
  94.0 4.9 %collective-permute-done.3.before_ref = bf16[16,4096]{1,0:T(8,128)(2,1)S(1)} collective-permute-done((bf16[16,4096]{1,0:T(8,128)(2,1)S(1)}, bf16[16,4096]{1,0:T(8,128)(2,1)S(1)}, u32[]{:S(2)}, u32[]{:S(2)}) %collective-permute-start.3) | collective-permute-done | bytes 131104 | tf_op jit(solution)/shard_map/ppermute | solution.py:405
  98.9 0.6 copy-done.7
  99.5 11.1 %mixer.1 = (bf16[128,2048]{1,0:T(8,128)(2,1)}, bf16[128,2048]{1,0:T(8,128)(2,1)}, bf16[16,2048]{1,0:T(8,128)(2,1)}, bf16[16,2048]{1,0:T(8,128)(2,1)}) custom-call(s32[2]{0:T(128)} %pad_add_fusion.place_ref, bf16[8,2,16,4096]{3,2,1,0:T(8,128)(2,1)} %bitcast.23, bf16[8,2,16,4096]{3,2,1,0:T(8,128)(2,1)} %bitcast.24, bf16[16,4096]{1,0:T(8,128)(2,1)} %copy-done.7, ...), custom_call_target="tpu_custom_call" | custom-call | flops 1577058304 | bytes 11141120 | tf_op jit(solution)/shard_map/mixer/pallas_call | solution.py:262
  110.7 2.0 %collective-permute-start.9 = (bf16[16,2048]{1,0:T(8,128)(2,1)}, bf16[16,2048]{1,0:T(8,128)(2,1)S(1)}, u32[]{:S(2)}, u32[]{:S(2)}) collective-permute-start(bf16[16,2048]{1,0:T(8,128)(2,1)} %get-tuple-element.41), channel_id=1, source_target_pairs={{0,2},{2,4},{4,6},{6,8},{8,10},{10,12},{12,14},{14,0},{1,3},{3,5},... | collective-permute-start | bytes 196616 | tf_op jit(solution)/shard_map/ppermute | solution.py:242
  112.7 0.2 fusion.1
  112.9 4.0 %collective-permute-start.16 = (bf16[16,2048]{1,0:T(8,128)(2,1)}, bf16[16,2048]{1,0:T(8,128)(2,1)S(1)}, u32[]{:S(2)}, u32[]{:S(2)}) collective-permute-start(bf16[16,2048]{1,0:T(8,128)(2,1)} %get-tuple-element.43), channel_id=1, source_target_pairs={{0,14},{2,0},{4,2},{6,4},{8,6},{10,8},{12,10},{14,12},{1,15},{3,1}... | collective-permute-start | bytes 196616 | tf_op jit(solution)/shard_map/ppermute | solution.py:242
  116.9 3.9 %collective-permute-done.9 = bf16[16,2048]{1,0:T(8,128)(2,1)S(1)} collective-permute-done((bf16[16,2048]{1,0:T(8,128)(2,1)}, bf16[16,2048]{1,0:T(8,128)(2,1)S(1)}, u32[]{:S(2)}, u32[]{:S(2)}) %collective-permute-start.9) | collective-permute-done | bytes 65568 | tf_op jit(solution)/shard_map/ppermute | solution.py:242
  120.8 0.9 add_convert_fusion.13
  121.6 0.1 collective-permute-start.10
  121.7 0.9 add_convert_fusion.6
  122.6 3.5 %collective-permute-start.17 = (bf16[16,2048]{1,0:T(8,128)(2,1)S(1)}, bf16[16,2048]{1,0:T(8,128)(2,1)S(1)}, u32[]{:S(2)}, u32[]{:S(2)}) collective-permute-start(bf16[16,2048]{1,0:T(8,128)(2,1)S(1)} %add_convert_fusion.6), channel_id=1, source_target_pairs={{0,14},{2,0},{4,2},{6,4},{8,6},{10,8},{12,10},{14,12},{1,15},{3,1}... | collective-permute-start | bytes 196616 | tf_op jit(solution)/shard_map/ppermute | solution.py:242
  126.1 2.6 %collective-permute-done.10 = bf16[16,2048]{1,0:T(8,128)(2,1)S(1)} collective-permute-done((bf16[16,2048]{1,0:T(8,128)(2,1)S(1)}, bf16[16,2048]{1,0:T(8,128)(2,1)S(1)}, u32[]{:S(2)}, u32[]{:S(2)}) %collective-permute-start.10) | collective-permute-done | bytes 65568 | tf_op jit(solution)/shard_map/ppermute | solution.py:242
  128.7 0.9 add_convert_fusion.12
  129.5 0.1 collective-permute-start.11
  129.6 0.9 add_convert_fusion.5
  130.5 3.4 %collective-permute-start.18 = (bf16[16,2048]{1,0:T(8,128)(2,1)S(1)}, bf16[16,2048]{1,0:T(8,128)(2,1)S(1)}, u32[]{:S(2)}, u32[]{:S(2)}) collective-permute-start(bf16[16,2048]{1,0:T(8,128)(2,1)S(1)} %add_convert_fusion.5), channel_id=1, source_target_pairs={{0,14},{2,0},{4,2},{6,4},{8,6},{10,8},{12,10},{14,12},{1,15},{3,1}... | collective-permute-start | bytes 196616 | tf_op jit(solution)/shard_map/ppermute | solution.py:242
  133.9 2.7 %collective-permute-done.11 = bf16[16,2048]{1,0:T(8,128)(2,1)S(1)} collective-permute-done((bf16[16,2048]{1,0:T(8,128)(2,1)S(1)}, bf16[16,2048]{1,0:T(8,128)(2,1)S(1)}, u32[]{:S(2)}, u32[]{:S(2)}) %collective-permute-start.11) | collective-permute-done | bytes 65568 | tf_op jit(solution)/shard_map/ppermute | solution.py:242
  136.6 0.9 add_convert_fusion.11
  137.5 0.1 collective-permute-start.12
  137.6 0.9 add_convert_fusion.4
  138.4 3.4 %collective-permute-start.19 = (bf16[16,2048]{1,0:T(8,128)(2,1)S(1)}, bf16[16,2048]{1,0:T(8,128)(2,1)S(1)}, u32[]{:S(2)}, u32[]{:S(2)}) collective-permute-start(bf16[16,2048]{1,0:T(8,128)(2,1)S(1)} %add_convert_fusion.4), channel_id=1, source_target_pairs={{0,14},{2,0},{4,2},{6,4},{8,6},{10,8},{12,10},{14,12},{1,15},{3,1}... | collective-permute-start | bytes 196616 | tf_op jit(solution)/shard_map/ppermute | solution.py:242
  141.8 1.2 collective-permute-done.12
  143.0 0.9 add_convert_fusion.10
  143.9 0.1 collective-permute-start.13
  144.0 0.9 add_convert_fusion.3
  144.9 3.4 %collective-permute-start.20 = (bf16[16,2048]{1,0:T(8,128)(2,1)S(1)}, bf16[16,2048]{1,0:T(8,128)(2,1)S(1)}, u32[]{:S(2)}, u32[]{:S(2)}) collective-permute-start(bf16[16,2048]{1,0:T(8,128)(2,1)S(1)} %add_convert_fusion.3), channel_id=1, source_target_pairs={{0,14},{2,0},{4,2},{6,4},{8,6},{10,8},{12,10},{14,12},{1,15},{3,1}... | collective-permute-start | bytes 196616 | tf_op jit(solution)/shard_map/ppermute | solution.py:242
  148.2 1.2 collective-permute-done.13
  149.5 0.9 add_convert_fusion.9
  150.4 0.9 add_convert_fusion.2
  151.3 3.4 %collective-permute-start.21 = (bf16[16,2048]{1,0:T(8,128)(2,1)S(1)}, bf16[16,2048]{1,0:T(8,128)(2,1)S(1)}, u32[]{:S(2)}, u32[]{:S(2)}) collective-permute-start(bf16[16,2048]{1,0:T(8,128)(2,1)S(1)} %add_convert_fusion.2), channel_id=1, source_target_pairs={{0,14},{2,0},{4,2},{6,4},{8,6},{10,8},{12,10},{14,12},{1,15},{3,1}... | collective-permute-start | bytes 196616 | tf_op jit(solution)/shard_map/ppermute | solution.py:242
  154.7 1.2 collective-permute-done.14
  155.9 0.9 add_convert_fusion.8
  156.8 0.9 add_convert_fusion.1
  157.7 3.4 %collective-permute-start.22 = (bf16[16,2048]{1,0:T(8,128)(2,1)S(1)}, bf16[16,2048]{1,0:T(8,128)(2,1)S(1)}, u32[]{:S(2)}, u32[]{:S(2)}) collective-permute-start(bf16[16,2048]{1,0:T(8,128)(2,1)S(1)} %add_convert_fusion.1), channel_id=1, source_target_pairs={{0,14},{2,0},{4,2},{6,4},{8,6},{10,8},{12,10},{14,12},{1,15},{3,1}... | collective-permute-start | bytes 196616 | tf_op jit(solution)/shard_map/ppermute | solution.py:242
  161.1 1.2 collective-permute-done.15
  162.3 0.9 add_convert_fusion.7
  163.2 0.9 add_convert_fusion
  164.0 0.7 pad_maximum_fusion
  164.7 2.1 %reshape.76 = bf16[16,128,128]{2,1,0:T(8,128)(2,1)} reshape(bf16[64,4096]{1,0:T(8,128)(2,1)} %reduce-scatter.2.cloned.1.call-done) | data formatting | bytes 1048576 | tf_op jit(solution)/shard_map/reshape | solution.py:414
  166.8 6.8 %all-to-all-start.1 = ((bf16[16,128,128]{2,1,0:T(8,128)(2,1)}), bf16[16,128,128]{2,1,0:T(8,128)(2,1)S(1)}, u32[]{:S(2)}, u32[]{:S(2)}) async-start(bf16[16,128,128]{2,1,0:T(8,128)(2,1)} %reshape.76), calls=%async_computation.2 | async-start | bytes 1048576 | tf_op jit(solution)/shard_map/all_to_all | solution.py:385
  173.6 0.2 select_reduce_fusion.1
  173.9 8.5 %all-to-all-done.1 = bf16[16,128,128]{2,1,0:T(8,128)(2,1)S(1)} async-done(((bf16[16,128,128]{2,1,0:T(8,128)(2,1)}), bf16[16,128,128]{2,1,0:T(8,128)(2,1)S(1)}, u32[]{:S(2)}, u32[]{:S(2)}) %all-to-all-start.1) | async-done | bytes 524320 | tf_op jit(solution)/shard_map/all_to_all | solution.py:385
  182.4 0.2 reshape.77
  182.6 1.0 convolution_convert_fusion
  (48 shorter events, 0.4 us)
Async XLA Ops:
  7.2 78.3 %copy-start = (bf16[4096,16]{0,1:T(8,128)(2,1)S(1)}, bf16[4096,16]{0,1:T(8,128)(2,1)}, u32[]{:S(2)}) copy-start(bf16[4096,16]{0,1:T(8,128)(2,1)} %param.25) | copy-start | bytes 393220
  7.2 157.5 %reduce-scatter.2.cloned.1.call-start = ((), (), s32[]{:S(2)}) async-start(), calls=%async_computation.3 | async-start | bytes 4718592 | tf_op jit(solution)/shard_map/reduce_scatter | solution.py:389
  7.2 7.2 %collective-permute-start = (bf16[4096,128]{1,0:T(8,128)(2,1)}, bf16[4096,128]{1,0:T(8,128)(2,1)S(1)}, u32[]{:S(2)}, u32[]{:S(2)}) collective-permute-start(bf16[4096,128]{1,0:T(8,128)(2,1)} %bitcast.27), channel_id=1, source_target_pairs={{0,1},{1,0},{2,3},{3,2},{4,5},{5,4},{6,7},{7,6},{8,9},{9,8},{10,11... | collective-permute-start | bytes 3145736 | tf_op jit(solution)/shard_map/ppermute | solution.py:45
  7.3 7.1 %collective-permute-start.1 = (bf16[4096,128]{1,0:T(8,128)(2,1)}, bf16[4096,128]{1,0:T(8,128)(2,1)S(1)}, u32[]{:S(2)}, u32[]{:S(2)}) collective-permute-start(bf16[4096,128]{1,0:T(8,128)(2,1)} %bitcast.29), channel_id=1, source_target_pairs={{0,1},{1,0},{2,3},{3,2},{4,5},{5,4},{6,7},{7,6},{8,9},{9,8},{10,11... | collective-permute-start | bytes 3145736 | tf_op jit(solution)/shard_map/ppermute | solution.py:45
  7.8 6.6 %collective-permute-start.2 = (bf16[128,4096]{1,0:T(8,128)(2,1)}, bf16[128,4096]{1,0:T(8,128)(2,1)S(1)}, u32[]{:S(2)}, u32[]{:S(2)}) collective-permute-start(bf16[128,4096]{1,0:T(8,128)(2,1)} %bitcast.31), channel_id=1, source_target_pairs={{0,1},{1,0},{2,3},{3,2},{4,5},{5,4},{6,7},{7,6},{8,9},{9,8},{10,11... | collective-permute-start | bytes 3145736 | tf_op jit(solution)/shard_map/ppermute | solution.py:45
  14.4 58.0 %copy-start.1 = (bf16[4096,128]{1,0:T(8,128)(2,1)}, bf16[4096,128]{1,0:T(8,128)(2,1)S(1)}, u32[]{:S(2)}) copy-start(bf16[4096,128]{1,0:T(8,128)(2,1)S(1)} %collective-permute-done.g1) | copy-start | bytes 3145732
  14.4 58.0 %copy-start.2 = (bf16[4096,128]{1,0:T(8,128)(2,1)}, bf16[4096,128]{1,0:T(8,128)(2,1)S(1)}, u32[]{:S(2)}) copy-start(bf16[4096,128]{1,0:T(8,128)(2,1)S(1)} %collective-permute-done.1.u1) | copy-start | bytes 3145732
  14.4 58.0 %copy-start.3 = (bf16[128,4096]{1,0:T(8,128)(2,1)}, bf16[128,4096]{1,0:T(8,128)(2,1)S(1)}, u32[]{:S(2)}) copy-start(bf16[128,4096]{1,0:T(8,128)(2,1)S(1)} %collective-permute-done.2.d1) | copy-start | bytes 3145732
  82.9 1.2 copy-start.4
  82.9 1.5 copy-start.5
  82.9 1.9 copy-start.6
  83.0 2.4 %copy-start.10 = (f32[3,128]{1,0:T(4,128)S(1)}, f32[3,128]{1,0:T(4,128)}, u32[]{:S(2)}) copy-start(f32[3,128]{1,0:T(4,128)} %taps_mine) | copy-start | bytes 4612
  83.0 2.5 %copy-start.8 = (bf16[16,4096]{1,0:T(8,128)(2,1)S(1)}, bf16[16,4096]{1,0:T(8,128)(2,1)}, u32[]{:S(2)}) copy-start(bf16[16,4096]{1,0:T(8,128)(2,1)} %get-tuple-element.48) | copy-start | bytes 393220
  83.0 2.7 %copy-start.9 = (s32[256,2]{0,1:T(2,128)S(1)}, s32[256,2]{0,1:T(2,128)}, u32[]{:S(2)}) copy-start(s32[256,2]{0,1:T(2,128)} %param.26) | copy-start | bytes 6148
  83.0 2.7 %copy-start.11 = (s32[2,128]{1,0:T(2,128)S(1)}, s32[2,128]{1,0:T(2,128)}, u32[]{:S(2)}) copy-start(s32[2,128]{1,0:T(2,128)} %get-tuple-element.47) | copy-start | bytes 3076
  84.2 14.7 %collective-permute-start.5 = (bf16[4096,128]{1,0:T(8,128)(2,1)S(1)}, bf16[4096,128]{1,0:T(8,128)(2,1)}, u32[]{:S(2)}, u32[]{:S(2)}) collective-permute-start(bf16[4096,128]{1,0:T(8,128)(2,1)S(1)} %copy-done.4), channel_id=1, source_target_pairs={{0,1},{1,0},{2,3},{3,2},{4,5},{5,4},{6,7},{7,6},{8,9},{9,8},{10,11... | collective-permute-start | bytes 3145736 | tf_op jit(solution)/shard_map/ppermute | solution.py:49
  84.5 14.4 %collective-permute-start.6 = (bf16[4096,128]{1,0:T(8,128)(2,1)S(1)}, bf16[4096,128]{1,0:T(8,128)(2,1)}, u32[]{:S(2)}, u32[]{:S(2)}) collective-permute-start(bf16[4096,128]{1,0:T(8,128)(2,1)S(1)} %copy-done.5), channel_id=1, source_target_pairs={{0,1},{1,0},{2,3},{3,2},{4,5},{5,4},{6,7},{7,6},{8,9},{9,8},{10,11... | collective-permute-start | bytes 3145736 | tf_op jit(solution)/shard_map/ppermute | solution.py:49
  84.8 14.1 %collective-permute-start.7 = (bf16[4096,128]{1,0:T(8,128)(2,1)S(1)}, bf16[4096,128]{1,0:T(8,128)(2,1)}, u32[]{:S(2)}, u32[]{:S(2)}) collective-permute-start(bf16[4096,128]{1,0:T(8,128)(2,1)S(1)} %copy-done.6), channel_id=1, source_target_pairs={{0,1},{1,0},{2,3},{3,2},{4,5},{5,4},{6,7},{7,6},{8,9},{9,8},{10,11... | collective-permute-start | bytes 3145736 | tf_op jit(solution)/shard_map/ppermute | solution.py:49
  85.0 13.9 %collective-permute-start.8 = (bf16[128,4096]{1,0:T(8,128)(2,1)}, bf16[128,4096]{1,0:T(8,128)(2,1)}, u32[]{:S(2)}, u32[]{:S(2)}) collective-permute-start(bf16[128,4096]{1,0:T(8,128)(2,1)} %refs_6_), channel_id=1, source_target_pairs={{0,1},{1,0},{2,3},{3,2},{4,5},{5,4},{6,7},{7,6},{8,9},{9,8},{10,11... | collective-permute-start | bytes 3145736 | tf_op jit(solution)/shard_map/ppermute | solution.py:49
  85.3 6.1 %collective-permute-start.4 = (f32[3,128]{1,0:T(4,128)S(1)}, f32[3,128]{1,0:T(4,128)}, u32[]{:S(2)}, u32[]{:S(2)}) collective-permute-start(f32[3,128]{1,0:T(4,128)S(1)} %copy-done.10), channel_id=1, source_target_pairs={{0,1},{1,0},{2,3},{3,2},{4,5},{5,4},{6,7},{7,6},{8,9},{9,8},{10,11... | collective-permute-start | bytes 4616 | tf_op jit(solution)/shard_map/ppermute | solution.py:49
  91.5 7.4 %collective-permute-start.3 = (bf16[16,4096]{1,0:T(8,128)(2,1)S(1)}, bf16[16,4096]{1,0:T(8,128)(2,1)S(1)}, u32[]{:S(2)}, u32[]{:S(2)}) collective-permute-start(bf16[16,4096]{1,0:T(8,128)(2,1)S(1)} %slice.48), channel_id=1, source_target_pairs={{0,16},{16,32},{32,48},{48,64},{64,80},{80,96},{96,112},{112,128},... | collective-permute-start | bytes 393224 | tf_op jit(solution)/shard_map/ppermute | solution.py:405
  98.9 0.7 copy-start.7
  99.5 13.1 %copy-start.12 = (bf16[4096,4]{0,1:T(4,128)(2,1)S(1)}, bf16[4096,4]{0,1:T(4,128)(2,1)}, u32[]{:S(2)}) copy-start(bf16[4096,4]{0,1:T(4,128)(2,1)} %param.24) | copy-start | bytes 98308
  99.5 13.1 %copy-start.13 = (s32[16]{0:T(128)S(1)}, s32[16]{0:T(128)}, u32[]{:S(2)}) copy-start(s32[16]{0:T(128)} %fusion) | copy-start | bytes 196
  110.7 10.1 %collective-permute-start.9 = (bf16[16,2048]{1,0:T(8,128)(2,1)}, bf16[16,2048]{1,0:T(8,128)(2,1)S(1)}, u32[]{:S(2)}, u32[]{:S(2)}) collective-permute-start(bf16[16,2048]{1,0:T(8,128)(2,1)} %get-tuple-element.41), channel_id=1, source_target_pairs={{0,2},{2,4},{4,6},{6,8},{8,10},{10,12},{12,14},{14,0},{1,3},{3,5},... | collective-permute-start | bytes 196616 | tf_op jit(solution)/shard_map/ppermute | solution.py:242
  112.9 8.9 %collective-permute-start.16 = (bf16[16,2048]{1,0:T(8,128)(2,1)}, bf16[16,2048]{1,0:T(8,128)(2,1)S(1)}, u32[]{:S(2)}, u32[]{:S(2)}) collective-permute-start(bf16[16,2048]{1,0:T(8,128)(2,1)} %get-tuple-element.43), channel_id=1, source_target_pairs={{0,14},{2,0},{4,2},{6,4},{8,6},{10,8},{12,10},{14,12},{1,15},{3,1}... | collective-permute-start | bytes 196616 | tf_op jit(solution)/shard_map/ppermute | solution.py:242
  121.6 7.1 %collective-permute-start.10 = (bf16[16,2048]{1,0:T(8,128)(2,1)S(1)}, bf16[16,2048]{1,0:T(8,128)(2,1)S(1)}, u32[]{:S(2)}, u32[]{:S(2)}) collective-permute-start(bf16[16,2048]{1,0:T(8,128)(2,1)S(1)} %add_convert_fusion.13), channel_id=1, source_target_pairs={{0,2},{2,4},{4,6},{6,8},{8,10},{10,12},{12,14},{14,0},{1,3},{3,5},... | collective-permute-start | bytes 196616 | tf_op jit(solution)/shard_map/ppermute | solution.py:242
  122.6 7.0 %collective-permute-start.17 = (bf16[16,2048]{1,0:T(8,128)(2,1)S(1)}, bf16[16,2048]{1,0:T(8,128)(2,1)S(1)}, u32[]{:S(2)}, u32[]{:S(2)}) collective-permute-start(bf16[16,2048]{1,0:T(8,128)(2,1)S(1)} %add_convert_fusion.6), channel_id=1, source_target_pairs={{0,14},{2,0},{4,2},{6,4},{8,6},{10,8},{12,10},{14,12},{1,15},{3,1}... | collective-permute-start | bytes 196616 | tf_op jit(solution)/shard_map/ppermute | solution.py:242
  129.5 7.1 %collective-permute-start.11 = (bf16[16,2048]{1,0:T(8,128)(2,1)S(1)}, bf16[16,2048]{1,0:T(8,128)(2,1)S(1)}, u32[]{:S(2)}, u32[]{:S(2)}) collective-permute-start(bf16[16,2048]{1,0:T(8,128)(2,1)S(1)} %add_convert_fusion.12), channel_id=1, source_target_pairs={{0,2},{2,4},{4,6},{6,8},{8,10},{10,12},{12,14},{14,0},{1,3},{3,5},... | collective-permute-start | bytes 196616 | tf_op jit(solution)/shard_map/ppermute | solution.py:242
  130.5 7.1 %collective-permute-start.18 = (bf16[16,2048]{1,0:T(8,128)(2,1)S(1)}, bf16[16,2048]{1,0:T(8,128)(2,1)S(1)}, u32[]{:S(2)}, u32[]{:S(2)}) collective-permute-start(bf16[16,2048]{1,0:T(8,128)(2,1)S(1)} %add_convert_fusion.5), channel_id=1, source_target_pairs={{0,14},{2,0},{4,2},{6,4},{8,6},{10,8},{12,10},{14,12},{1,15},{3,1}... | collective-permute-start | bytes 196616 | tf_op jit(solution)/shard_map/ppermute | solution.py:242
  137.5 5.6 %collective-permute-start.12 = (bf16[16,2048]{1,0:T(8,128)(2,1)S(1)}, bf16[16,2048]{1,0:T(8,128)(2,1)S(1)}, u32[]{:S(2)}, u32[]{:S(2)}) collective-permute-start(bf16[16,2048]{1,0:T(8,128)(2,1)S(1)} %add_convert_fusion.11), channel_id=1, source_target_pairs={{0,2},{2,4},{4,6},{6,8},{8,10},{10,12},{12,14},{14,0},{1,3},{3,5},... | collective-permute-start | bytes 196616 | tf_op jit(solution)/shard_map/ppermute | solution.py:242
  138.4 5.5 %collective-permute-start.19 = (bf16[16,2048]{1,0:T(8,128)(2,1)S(1)}, bf16[16,2048]{1,0:T(8,128)(2,1)S(1)}, u32[]{:S(2)}, u32[]{:S(2)}) collective-permute-start(bf16[16,2048]{1,0:T(8,128)(2,1)S(1)} %add_convert_fusion.4), channel_id=1, source_target_pairs={{0,14},{2,0},{4,2},{6,4},{8,6},{10,8},{12,10},{14,12},{1,15},{3,1}... | collective-permute-start | bytes 196616 | tf_op jit(solution)/shard_map/ppermute | solution.py:242
  143.9 5.6 %collective-permute-start.13 = (bf16[16,2048]{1,0:T(8,128)(2,1)S(1)}, bf16[16,2048]{1,0:T(8,128)(2,1)S(1)}, u32[]{:S(2)}, u32[]{:S(2)}) collective-permute-start(bf16[16,2048]{1,0:T(8,128)(2,1)S(1)} %add_convert_fusion.10), channel_id=1, source_target_pairs={{0,2},{2,4},{4,6},{6,8},{8,10},{10,12},{12,14},{14,0},{1,3},{3,5},... | collective-permute-start | bytes 196616 | tf_op jit(solution)/shard_map/ppermute | solution.py:242
  144.9 5.5 %collective-permute-start.20 = (bf16[16,2048]{1,0:T(8,128)(2,1)S(1)}, bf16[16,2048]{1,0:T(8,128)(2,1)S(1)}, u32[]{:S(2)}, u32[]{:S(2)}) collective-permute-start(bf16[16,2048]{1,0:T(8,128)(2,1)S(1)} %add_convert_fusion.3), channel_id=1, source_target_pairs={{0,14},{2,0},{4,2},{6,4},{8,6},{10,8},{12,10},{14,12},{1,15},{3,1}... | collective-permute-start | bytes 196616 | tf_op jit(solution)/shard_map/ppermute | solution.py:242
  150.3 5.6 %collective-permute-start.14 = (bf16[16,2048]{1,0:T(8,128)(2,1)S(1)}, bf16[16,2048]{1,0:T(8,128)(2,1)S(1)}, u32[]{:S(2)}, u32[]{:S(2)}) collective-permute-start(bf16[16,2048]{1,0:T(8,128)(2,1)S(1)} %add_convert_fusion.9), channel_id=1, source_target_pairs={{0,2},{2,4},{4,6},{6,8},{8,10},{10,12},{12,14},{14,0},{1,3},{3,5},... | collective-permute-start | bytes 196616 | tf_op jit(solution)/shard_map/ppermute | solution.py:242
  151.3 5.5 %collective-permute-start.21 = (bf16[16,2048]{1,0:T(8,128)(2,1)S(1)}, bf16[16,2048]{1,0:T(8,128)(2,1)S(1)}, u32[]{:S(2)}, u32[]{:S(2)}) collective-permute-start(bf16[16,2048]{1,0:T(8,128)(2,1)S(1)} %add_convert_fusion.2), channel_id=1, source_target_pairs={{0,14},{2,0},{4,2},{6,4},{8,6},{10,8},{12,10},{14,12},{1,15},{3,1}... | collective-permute-start | bytes 196616 | tf_op jit(solution)/shard_map/ppermute | solution.py:242
  156.7 5.6 %collective-permute-start.15 = (bf16[16,2048]{1,0:T(8,128)(2,1)S(1)}, bf16[16,2048]{1,0:T(8,128)(2,1)S(1)}, u32[]{:S(2)}, u32[]{:S(2)}) collective-permute-start(bf16[16,2048]{1,0:T(8,128)(2,1)S(1)} %add_convert_fusion.8), channel_id=1, source_target_pairs={{0,2},{2,4},{4,6},{6,8},{8,10},{10,12},{12,14},{14,0},{1,3},{3,5},... | collective-permute-start | bytes 196616 | tf_op jit(solution)/shard_map/ppermute | solution.py:242
  157.7 5.5 %collective-permute-start.22 = (bf16[16,2048]{1,0:T(8,128)(2,1)S(1)}, bf16[16,2048]{1,0:T(8,128)(2,1)S(1)}, u32[]{:S(2)}, u32[]{:S(2)}) collective-permute-start(bf16[16,2048]{1,0:T(8,128)(2,1)S(1)} %add_convert_fusion.1), channel_id=1, source_target_pairs={{0,14},{2,0},{4,2},{6,4},{8,6},{10,8},{12,10},{14,12},{1,15},{3,1}... | collective-permute-start | bytes 196616 | tf_op jit(solution)/shard_map/ppermute | solution.py:242
  166.8 15.6 %all-to-all-start.1 = ((bf16[16,128,128]{2,1,0:T(8,128)(2,1)}), bf16[16,128,128]{2,1,0:T(8,128)(2,1)S(1)}, u32[]{:S(2)}, u32[]{:S(2)}) async-start(bf16[16,128,128]{2,1,0:T(8,128)(2,1)} %reshape.76), calls=%async_computation.2 | async-start | bytes 1048576 | tf_op jit(solution)/shard_map/all_to_all | solution.py:385
Sparse Core Ops, SparseCore 0:
  83.1 59.9 reduce-scatter.1

commit v7 on v6

--- a/solution.py
+++ b/solution.py
@@ -233,7 +233,9 @@
 
 def ring_sum(outs):
     chains = len(outs) // 2
-    wholes, sums = outs[:chains], list(outs[chains:])
+    one = lax.optimization_barrier(jnp.ones((), jnp.bfloat16))
+    wholes = [lax.optimization_barrier(whole * one) for whole in outs[:chains]]
+    sums = list(outs[chains:])
     rows = sums[0].shape[0]
     zs = lax.axis_size("z")
     for hop in range(zs - 1):
@@ -409,8 +411,9 @@
     weights = [part for array in projections for part in (array, swap_late(array))]
     mixes = (mix_weight, swap_late(mix_weight))
     partial_mix = mixer_partial(core_ref, mix_tokens, before, mix_gain, taps, weights, mixes, zs)
-    mixer_out = jnp.concatenate(ring_sum(partial_mix), axis=1)
-    summed, mixer_out = lax.optimization_barrier((summed, mixer_out))
+    mixer_sums = ring_sum(partial_mix)
+    summed, mixer_sums = lax.optimization_barrier((summed, mixer_sums))
+    mixer_out = jnp.concatenate(mixer_sums, axis=1)
     returned = exchange(summed.reshape(eps, CAP * width // 128, 128)).reshape(-1, width)
 
     own_routes = lax.dynamic_slice_in_dim(

time: 193 us -> 200 us (1.036); the launches traced: 190 us -> 200 us
  waiting for transfers between devices: 32.3 us -> 95.1 us
  blocking collectives: 58 us -> 0 us
  starting transfers between devices: 37.3 us -> 48.6 us
  other arithmetic: 14.2 us -> 4.07 us
  local copies, waits for them, and re-layouts: 5.49 us -> 8.92 us
    all_to_all x1 -> x2, waiting for transfers between devices: 8.51 us -> 68.2 us  [exchange(): return lax.all_to_all(array, EP, split_axis=0, concat_axis=0, tiled=True)]
    all_to_all x1 -> x0, blocking collectives: 58 us -> none  [exchange(): return lax.all_to_all(array, EP, split_axis=0, concat_axis=0, tiled=True)]
    convert_element_type x14, other arithmetic: 12 us -> 0.26 us  [ring_sum(): sums[chain] = total.astype(jnp.bfloat16)]
    all_to_all x1 -> x2, starting transfers between devices: 6.83 us -> 15.7 us  [exchange(): return lax.all_to_all(array, EP, split_axis=0, concat_axis=0, tiled=True)]
    ppermute x14, waiting for transfers between devices: 14.1 us -> 20.5 us  [ring_sum(): lax.ppermute(sums[chain], 'z', [(i, (i + way) % zs) for i in range(zs)])]
    ppermute x5, waiting for transfers between devices: 4.78 us -> 0.01 us  [swap_late(): return lax.ppermute(value, 'core', [(0, 1), (1, 0)])]
    unnamed x28 -> x36, local copies, waits for them, and re-layouts: 2.25 us -> 5.7 us
    mul x0 -> x2, other arithmetic: none -> 2.16 us  [ring_sum(): wholes = [lax.optimization_barrier(whole * one) for whole in outs[:chains]]]
  transfers between devices with their start and end apart: 25 -> 26, of which waited for: 10 -> 11; matrix products, arithmetic and copies ran while one was open for 8% -> 3% of each run, Pallas kernels for 9% -> 8%
where the time goes in v7:
time: 200 us
  waiting for transfers between devices  95.1 us (48%)
  starting transfers between devices  48.6 us (24%)
  Pallas kernels  27.2 us (14%)
  between operations  14.4 us (7%)
  local copies, waits for them, and re-layouts  8.92 us (4%)
  other arithmetic  4.07 us (2%)
    all_to_all x2, waiting for transfers between devices, exchange(): return lax.all_to_all(array, EP, split_axis=0, concat_axis=0, tiled=True)  68.2 us
    ppermute x14, starting transfers between devices, ring_sum(): lax.ppermute(sums[chain], 'z', [(i, (i + way) % zs) for i in range(zs)])  28.8 us
    ppermute x14, waiting for transfers between devices, ring_sum(): lax.ppermute(sums[chain], 'z', [(i, (i + way) % zs) for i in range(zs)])  20.5 us
    all_to_all x2, starting transfers between devices, exchange(): return lax.all_to_all(array, EP, split_axis=0, concat_axis=0, tiled=True)  15.7 us
    pallas_call x1, Pallas kernels, mixer_partial(): pl.pallas_call(functools.partial(mixer_kernel, steps), grid_spec=pltpu.Pr...  11 us
    pallas_call x1, Pallas kernels, expert_partial(): pl.pallas_call(functools.partial(expert_kernel, zs, steps), grid=(2 * ste...  10.5 us
    ppermute x1, waiting for transfers between devices, layer(): lax.ppermute(mix_tokens[mix_tokens.shape[0] - MOE_SHARE:], EP, [(i, i + 1...  6.4 us
    pallas_call x1, Pallas kernels, prepare(): pl.pallas_call(functools.partial(prep_kernel, zs), grid_spec=pltpu.Prefet...  5.82 us
  transfers between devices with their start and end apart: 26, of which 11 were waited for; matrix products, arithmetic and copies ran while one was open for 3% of the time, Pallas kernels for 8%

profile of v7, /device:TPU:2, one launch (start us, length us, event | category | flops | bytes accessed | tf_op | source)
XLA Modules:
  0.0 199.7 jit_solution(2241711011447024450)
XLA Ops:
  7.2 0.1 collective-permute-start
  7.3 0.5 collective-permute-start.1
  7.8 0.1 collective-permute-start.2
  7.9 0.6 pad_add_fusion.place_ref
  8.5 5.8 %prepare.1 = (bf16[512,4096]{1,0:T(8,128)(2,1)}, bf16[16,4096]{1,0:T(8,128)(2,1)}, s32[2,128]{1,0:T(2,128)}) custom-call(s32[2]{0:T(128)} %pad_add_fusion.place_ref, bf16[8,2,16,4096]{3,2,1,0:T(8,128)(2,1)} %bitcast.25, f32[1,4096]{1,0:T(1,128)} %bitcast.32, s32[2,256]{1,0:T(2,128)} %bitcast.34), custom_call_target="tpu_custom_call" | custom-call | flops 536870912 | bytes 5242880 | tf_op jit(solution)/shard_map/prepare/pallas_call | solution.py:114
  14.4 1.0 copy-done.1
  15.3 0.3 copy-done.2
  15.7 0.3 copy-done.3
  16.0 7.5 %all-to-all-start = ((bf16[16,32,4096]{2,1,0:T(8,128)(2,1)}), bf16[16,32,4096]{2,1,0:T(8,128)(2,1)}, u32[]{:S(2)}, u32[]{:S(2)}) async-start(bf16[16,32,4096]{2,1,0:T(8,128)(2,1)} %bitcast.24), calls=%async_computation | async-start | bytes 8388608 | tf_op jit(solution)/shard_map/all_to_all | solution.py:387
  23.5 60.1 %all-to-all-done = bf16[16,32,4096]{2,1,0:T(8,128)(2,1)} async-done(((bf16[16,32,4096]{2,1,0:T(8,128)(2,1)}), bf16[16,32,4096]{2,1,0:T(8,128)(2,1)}, u32[]{:S(2)}, u32[]{:S(2)}) %all-to-all-start) | async-done | bytes 4194336 | tf_op jit(solution)/shard_map/all_to_all | solution.py:387
  83.6 10.5 %experts.1 = bf16[512,4096]{1,0:T(8,128)(2,1)} custom-call(bf16[512,4096]{1,0:T(8,128)(2,1)} %bitcast.9.rows_ref, bf16[4096,128]{1,0:T(8,128)(2,1)} %bitcast.27, bf16[4096,128]{1,0:T(8,128)(2,1)} %copy-done.1, bf16[4096,128]{1,0:T(8,128)(2,1)} %bitcast.29, bf16[4096,128]{1,0:T(8,128)(2,1)} %copy-done.2, bf16[128,4096]{1,0:T(8,128)(2,1)} %bitcast.31, ...), custom_call_target="tpu_custom_call" | custom-call | flops 3221225472 | bytes 14680064 | tf_op jit(solution)/shard_map/experts/pallas_call | solution.py:331
  94.2 0.6 copy-done.14
  94.8 0.6 copy-done.4
  95.3 0.3 copy-done.5
  95.7 0.2 collective-permute-start.6
  95.9 0.1 copy-done.6
  96.0 0.2 collective-permute-start.7
  96.2 0.3 collective-permute-start.8
  96.5 0.2 fusion.2
  96.6 0.1 bitcast_add_fusion
  96.7 0.2 select_reduce_fusion.1
  96.9 0.2 fusion.1
  97.1 0.9 slice.48
  98.1 2.7 %collective-permute-start.3 = (bf16[16,4096]{1,0:T(8,128)(2,1)S(1)}, bf16[16,4096]{1,0:T(8,128)(2,1)S(1)}, u32[]{:S(2)}, u32[]{:S(2)}) collective-permute-start(bf16[16,4096]{1,0:T(8,128)(2,1)S(1)} %slice.48), channel_id=1, source_target_pairs={{0,16},{16,32},{32,48},{48,64},{64,80},{80,96},{96,112},{112,128},... | collective-permute-start | bytes 393224 | tf_op jit(solution)/shard_map/ppermute | solution.py:407
  100.8 6.4 %collective-permute-done.3.before_ref = bf16[16,4096]{1,0:T(8,128)(2,1)S(1)} collective-permute-done((bf16[16,4096]{1,0:T(8,128)(2,1)S(1)}, bf16[16,4096]{1,0:T(8,128)(2,1)S(1)}, u32[]{:S(2)}, u32[]{:S(2)}) %collective-permute-start.3) | collective-permute-done | bytes 131104 | tf_op jit(solution)/shard_map/ppermute | solution.py:407
  107.2 1.1 copy-done.7
  108.3 0.3 copy-done.8
  108.6 0.6 copy-done.9
  109.2 0.5 copy-done.10
  109.7 11.0 %mixer.1 = (bf16[128,2048]{1,0:T(8,128)(2,1)}, bf16[128,2048]{1,0:T(8,128)(2,1)}, bf16[16,2048]{1,0:T(8,128)(2,1)}, bf16[16,2048]{1,0:T(8,128)(2,1)}) custom-call(s32[2]{0:T(128)} %pad_add_fusion.place_ref, bf16[8,2,16,4096]{3,2,1,0:T(8,128)(2,1)} %bitcast.22, bf16[8,2,16,4096]{3,2,1,0:T(8,128)(2,1)} %bitcast.23, bf16[16,4096]{1,0:T(8,128)(2,1)} %copy-done.11, ...), custom_call_target="tpu_custom_call" | custom-call | flops 1577058304 | bytes 11141120 | tf_op jit(solution)/shard_map/mixer/pallas_call | solution.py:264
  120.7 2.0 %collective-permute-start.9 = (bf16[16,2048]{1,0:T(8,128)(2,1)}, bf16[16,2048]{1,0:T(8,128)(2,1)S(1)}, u32[]{:S(2)}, u32[]{:S(2)}) collective-permute-start(bf16[16,2048]{1,0:T(8,128)(2,1)} %get-tuple-element.42), channel_id=1, source_target_pairs={{0,2},{2,4},{4,6},{6,8},{8,10},{10,12},{12,14},{14,0},{1,3},{3,5},... | collective-permute-start | bytes 196616 | tf_op jit(solution)/shard_map/ppermute | solution.py:244
  122.7 4.1 %collective-permute-start.16 = (bf16[16,2048]{1,0:T(8,128)(2,1)}, bf16[16,2048]{1,0:T(8,128)(2,1)S(1)}, u32[]{:S(2)}, u32[]{:S(2)}) collective-permute-start(bf16[16,2048]{1,0:T(8,128)(2,1)} %get-tuple-element.44), channel_id=1, source_target_pairs={{0,14},{2,0},{4,2},{6,4},{8,6},{10,8},{12,10},{14,12},{1,15},{3,1}... | collective-permute-start | bytes 196616 | tf_op jit(solution)/shard_map/ppermute | solution.py:244
  126.8 1.1 broadcast_multiply_fusion.1
  127.8 1.1 broadcast_multiply_fusion
  128.9 1.6 collective-permute-done.16
  130.6 3.8 %collective-permute-start.17 = (bf16[16,2048]{1,0:T(8,128)(2,1)S(1)}, bf16[16,2048]{1,0:T(8,128)(2,1)S(1)}, u32[]{:S(2)}, u32[]{:S(2)}) collective-permute-start(bf16[16,2048]{1,0:T(8,128)(2,1)S(1)} %add_convert_fusion.6), channel_id=1, source_target_pairs={{0,14},{2,0},{4,2},{6,4},{8,6},{10,8},{12,10},{14,12},{1,15},{3,1}... | collective-permute-start | bytes 196616 | tf_op jit(solution)/shard_map/ppermute | solution.py:244
  134.4 0.1 collective-permute-start.10
  134.5 3.2 %collective-permute-done.17 = bf16[16,2048]{1,0:T(8,128)(2,1)S(1)} collective-permute-done((bf16[16,2048]{1,0:T(8,128)(2,1)S(1)}, bf16[16,2048]{1,0:T(8,128)(2,1)S(1)}, u32[]{:S(2)}, u32[]{:S(2)}) %collective-permute-start.17) | collective-permute-done | bytes 65568 | tf_op jit(solution)/shard_map/ppermute | solution.py:244
  137.7 3.8 %collective-permute-start.18 = (bf16[16,2048]{1,0:T(8,128)(2,1)S(1)}, bf16[16,2048]{1,0:T(8,128)(2,1)S(1)}, u32[]{:S(2)}, u32[]{:S(2)}) collective-permute-start(bf16[16,2048]{1,0:T(8,128)(2,1)S(1)} %add_convert_fusion.5), channel_id=1, source_target_pairs={{0,14},{2,0},{4,2},{6,4},{8,6},{10,8},{12,10},{14,12},{1,15},{3,1}... | collective-permute-start | bytes 196616 | tf_op jit(solution)/shard_map/ppermute | solution.py:244
  141.5 0.0 collective-permute-done.10
  141.6 0.1 collective-permute-start.11
  141.6 3.2 %collective-permute-done.18 = bf16[16,2048]{1,0:T(8,128)(2,1)S(1)} collective-permute-done((bf16[16,2048]{1,0:T(8,128)(2,1)S(1)}, bf16[16,2048]{1,0:T(8,128)(2,1)S(1)}, u32[]{:S(2)}, u32[]{:S(2)}) %collective-permute-start.18) | collective-permute-done | bytes 65568 | tf_op jit(solution)/shard_map/ppermute | solution.py:244
  144.8 3.8 %collective-permute-start.19 = (bf16[16,2048]{1,0:T(8,128)(2,1)S(1)}, bf16[16,2048]{1,0:T(8,128)(2,1)S(1)}, u32[]{:S(2)}, u32[]{:S(2)}) collective-permute-start(bf16[16,2048]{1,0:T(8,128)(2,1)S(1)} %add_convert_fusion.4), channel_id=1, source_target_pairs={{0,14},{2,0},{4,2},{6,4},{8,6},{10,8},{12,10},{14,12},{1,15},{3,1}... | collective-permute-start | bytes 196616 | tf_op jit(solution)/shard_map/ppermute | solution.py:244
  148.7 0.1 collective-permute-start.12
  148.7 3.2 %collective-permute-done.19 = bf16[16,2048]{1,0:T(8,128)(2,1)S(1)} collective-permute-done((bf16[16,2048]{1,0:T(8,128)(2,1)S(1)}, bf16[16,2048]{1,0:T(8,128)(2,1)S(1)}, u32[]{:S(2)}, u32[]{:S(2)}) %collective-permute-start.19) | collective-permute-done | bytes 65568 | tf_op jit(solution)/shard_map/ppermute | solution.py:244
  151.9 3.8 %collective-permute-start.20 = (bf16[16,2048]{1,0:T(8,128)(2,1)S(1)}, bf16[16,2048]{1,0:T(8,128)(2,1)S(1)}, u32[]{:S(2)}, u32[]{:S(2)}) collective-permute-start(bf16[16,2048]{1,0:T(8,128)(2,1)S(1)} %add_convert_fusion.3), channel_id=1, source_target_pairs={{0,14},{2,0},{4,2},{6,4},{8,6},{10,8},{12,10},{14,12},{1,15},{3,1}... | collective-permute-start | bytes 196616 | tf_op jit(solution)/shard_map/ppermute | solution.py:244
  155.8 0.1 collective-permute-start.13
  155.9 2.0 collective-permute-done.20
  157.9 3.4 %collective-permute-start.21 = (bf16[16,2048]{1,0:T(8,128)(2,1)S(1)}, bf16[16,2048]{1,0:T(8,128)(2,1)S(1)}, u32[]{:S(2)}, u32[]{:S(2)}) collective-permute-start(bf16[16,2048]{1,0:T(8,128)(2,1)S(1)} %add_convert_fusion.2), channel_id=1, source_target_pairs={{0,14},{2,0},{4,2},{6,4},{8,6},{10,8},{12,10},{14,12},{1,15},{3,1}... | collective-permute-start | bytes 196616 | tf_op jit(solution)/shard_map/ppermute | solution.py:244
  161.3 0.0 collective-permute-done.13
  161.3 0.1 collective-permute-start.14
  161.4 1.7 collective-permute-done.21
  163.2 3.6 %collective-permute-start.22 = (bf16[16,2048]{1,0:T(8,128)(2,1)S(1)}, bf16[16,2048]{1,0:T(8,128)(2,1)S(1)}, u32[]{:S(2)}, u32[]{:S(2)}) collective-permute-start(bf16[16,2048]{1,0:T(8,128)(2,1)S(1)} %add_convert_fusion.1), channel_id=1, source_target_pairs={{0,14},{2,0},{4,2},{6,4},{8,6},{10,8},{12,10},{14,12},{1,15},{3,1}... | collective-permute-start | bytes 196616 | tf_op jit(solution)/shard_map/ppermute | solution.py:244
  166.8 0.0 collective-permute-done.14
  166.9 0.1 collective-permute-start.15
  167.0 1.7 collective-permute-done.22
  168.8 3.7 %collective-permute-done.15 = bf16[16,2048]{1,0:T(8,128)(2,1)S(1)} collective-permute-done((bf16[16,2048]{1,0:T(8,128)(2,1)S(1)}, bf16[16,2048]{1,0:T(8,128)(2,1)S(1)}, u32[]{:S(2)}, u32[]{:S(2)}) %collective-permute-start.15) | collective-permute-done | bytes 65568 | tf_op jit(solution)/shard_map/ppermute | solution.py:244
  172.5 2.1 %reshape.76 = bf16[16,128,128]{2,1,0:T(8,128)(2,1)} reshape(bf16[64,4096]{1,0:T(8,128)(2,1)} %reduce-scatter.2.cloned.1.call-done) | data formatting | bytes 1048576 | tf_op jit(solution)/shard_map/reshape | solution.py:417
  174.6 8.2 %all-to-all-start.1 = ((bf16[16,128,128]{2,1,0:T(8,128)(2,1)}), bf16[16,128,128]{2,1,0:T(8,128)(2,1)S(1)}, u32[]{:S(2)}, u32[]{:S(2)}) async-start(bf16[16,128,128]{2,1,0:T(8,128)(2,1)} %reshape.76), calls=%async_computation.2 | async-start | bytes 1048576 | tf_op jit(solution)/shard_map/all_to_all | solution.py:387
  182.8 0.1 select_reduce_fusion
  182.9 0.7 pad_maximum_fusion
  183.6 8.0 %all-to-all-done.1 = bf16[16,128,128]{2,1,0:T(8,128)(2,1)S(1)} async-done(((bf16[16,128,128]{2,1,0:T(8,128)(2,1)}), bf16[16,128,128]{2,1,0:T(8,128)(2,1)S(1)}, u32[]{:S(2)}, u32[]{:S(2)}) %all-to-all-start.1) | async-done | bytes 524320 | tf_op jit(solution)/shard_map/all_to_all | solution.py:387
  191.6 0.2 reshape.77
  191.8 1.0 convolution_convert_fusion
  (59 shorter events, 0.6 us)
Async XLA Ops:
  7.2 89.3 %copy-start = (bf16[4096,16]{0,1:T(8,128)(2,1)S(1)}, bf16[4096,16]{0,1:T(8,128)(2,1)}, u32[]{:S(2)}) copy-start(bf16[4096,16]{0,1:T(8,128)(2,1)} %param.25) | copy-start | bytes 393220
  7.2 7.1 %collective-permute-start = (bf16[4096,128]{1,0:T(8,128)(2,1)}, bf16[4096,128]{1,0:T(8,128)(2,1)S(1)}, u32[]{:S(2)}, u32[]{:S(2)}) collective-permute-start(bf16[4096,128]{1,0:T(8,128)(2,1)} %bitcast.26), channel_id=1, source_target_pairs={{0,1},{1,0},{2,3},{3,2},{4,5},{5,4},{6,7},{7,6},{8,9},{9,8},{10,11... | collective-permute-start | bytes 3145736 | tf_op jit(solution)/shard_map/ppermute | solution.py:45
  7.3 7.0 %collective-permute-start.1 = (bf16[4096,128]{1,0:T(8,128)(2,1)}, bf16[4096,128]{1,0:T(8,128)(2,1)S(1)}, u32[]{:S(2)}, u32[]{:S(2)}) collective-permute-start(bf16[4096,128]{1,0:T(8,128)(2,1)} %bitcast.28), channel_id=1, source_target_pairs={{0,1},{1,0},{2,3},{3,2},{4,5},{5,4},{6,7},{7,6},{8,9},{9,8},{10,11... | collective-permute-start | bytes 3145736 | tf_op jit(solution)/shard_map/ppermute | solution.py:45
  7.8 6.6 %collective-permute-start.2 = (bf16[128,4096]{1,0:T(8,128)(2,1)}, bf16[128,4096]{1,0:T(8,128)(2,1)S(1)}, u32[]{:S(2)}, u32[]{:S(2)}) collective-permute-start(bf16[128,4096]{1,0:T(8,128)(2,1)} %bitcast.30), channel_id=1, source_target_pairs={{0,1},{1,0},{2,3},{3,2},{4,5},{5,4},{6,7},{7,6},{8,9},{9,8},{10,11... | collective-permute-start | bytes 3145736 | tf_op jit(solution)/shard_map/ppermute | solution.py:45
  14.3 1.0 copy-start.1
  14.3 1.4 copy-start.2
  14.3 1.6 copy-start.3
  16.0 67.7 %all-to-all-start = ((bf16[16,32,4096]{2,1,0:T(8,128)(2,1)}), bf16[16,32,4096]{2,1,0:T(8,128)(2,1)}, u32[]{:S(2)}, u32[]{:S(2)}) async-start(bf16[16,32,4096]{2,1,0:T(8,128)(2,1)} %bitcast.24), calls=%async_computation | async-start | bytes 8388608 | tf_op jit(solution)/shard_map/all_to_all | solution.py:387
  23.4 149.1 %reduce-scatter.2.cloned.1.call-start = ((), (), s32[]{:S(2)}) async-start(), calls=%async_computation.3 | async-start | bytes 4718592 | tf_op jit(solution)/shard_map/reduce_scatter | solution.py:391
  94.1 0.7 copy-start.14
  94.1 1.2 copy-start.4
  94.1 1.5 copy-start.5
  94.1 1.9 copy-start.6
  94.1 2.4 %copy-start.12 = (bf16[16,4096]{1,0:T(8,128)(2,1)S(1)}, bf16[16,4096]{1,0:T(8,128)(2,1)}, u32[]{:S(2)}) copy-start(bf16[16,4096]{1,0:T(8,128)(2,1)} %get-tuple-element.50) | copy-start | bytes 393220
  94.1 2.5 %copy-start.13 = (s32[256,2]{0,1:T(2,128)S(1)}, s32[256,2]{0,1:T(2,128)}, u32[]{:S(2)}) copy-start(s32[256,2]{0,1:T(2,128)} %param.26) | copy-start | bytes 6148
  94.2 2.5 %copy-start.16 = (s32[2,128]{1,0:T(2,128)S(1)}, s32[2,128]{1,0:T(2,128)}, u32[]{:S(2)}) copy-start(s32[2,128]{1,0:T(2,128)} %get-tuple-element.49) | copy-start | bytes 3076
  94.2 2.7 %copy-start.17 = (bf16[4096,4]{0,1:T(4,128)(2,1)S(1)}, bf16[4096,4]{0,1:T(4,128)(2,1)}, u32[]{:S(2)}) copy-start(bf16[4096,4]{0,1:T(4,128)(2,1)} %param.24) | copy-start | bytes 98308
  94.8 3.3 %collective-permute-start.4 = (f32[3,128]{1,0:T(4,128)S(1)}, f32[3,128]{1,0:T(4,128)S(1)}, u32[]{:S(2)}, u32[]{:S(2)}) collective-permute-start(f32[3,128]{1,0:T(4,128)S(1)} %copy-done.14), channel_id=1, source_target_pairs={{0,1},{1,0},{2,3},{3,2},{4,5},{5,4},{6,7},{7,6},{8,9},{9,8},{10,11... | collective-permute-start | bytes 4616 | tf_op jit(solution)/shard_map/ppermute | solution.py:49
  95.3 11.9 %collective-permute-start.5 = (bf16[4096,128]{1,0:T(8,128)(2,1)S(1)}, bf16[4096,128]{1,0:T(8,128)(2,1)S(1)}, u32[]{:S(2)}, u32[]{:S(2)}) collective-permute-start(bf16[4096,128]{1,0:T(8,128)(2,1)S(1)} %copy-done.4), channel_id=1, source_target_pairs={{0,1},{1,0},{2,3},{3,2},{4,5},{5,4},{6,7},{7,6},{8,9},{9,8},{10,11... | collective-permute-start | bytes 3145736 | tf_op jit(solution)/shard_map/ppermute | solution.py:49
  95.7 11.6 %collective-permute-start.6 = (bf16[4096,128]{1,0:T(8,128)(2,1)S(1)}, bf16[4096,128]{1,0:T(8,128)(2,1)S(1)}, u32[]{:S(2)}, u32[]{:S(2)}) collective-permute-start(bf16[4096,128]{1,0:T(8,128)(2,1)S(1)} %copy-done.5), channel_id=1, source_target_pairs={{0,1},{1,0},{2,3},{3,2},{4,5},{5,4},{6,7},{7,6},{8,9},{9,8},{10,11... | collective-permute-start | bytes 3145736 | tf_op jit(solution)/shard_map/ppermute | solution.py:49
  96.0 11.3 %collective-permute-start.7 = (bf16[4096,128]{1,0:T(8,128)(2,1)S(1)}, bf16[4096,128]{1,0:T(8,128)(2,1)S(1)}, u32[]{:S(2)}, u32[]{:S(2)}) collective-permute-start(bf16[4096,128]{1,0:T(8,128)(2,1)S(1)} %copy-done.6), channel_id=1, source_target_pairs={{0,1},{1,0},{2,3},{3,2},{4,5},{5,4},{6,7},{7,6},{8,9},{9,8},{10,11... | collective-permute-start | bytes 3145736 | tf_op jit(solution)/shard_map/ppermute | solution.py:49
  96.2 12.1 %collective-permute-start.8 = (bf16[128,4096]{1,0:T(8,128)(2,1)}, bf16[128,4096]{1,0:T(8,128)(2,1)S(1)}, u32[]{:S(2)}, u32[]{:S(2)}) collective-permute-start(bf16[128,4096]{1,0:T(8,128)(2,1)} %refs_6_), channel_id=1, source_target_pairs={{0,1},{1,0},{2,3},{3,2},{4,5},{5,4},{6,7},{7,6},{8,9},{9,8},{10,11... | collective-permute-start | bytes 3145736 | tf_op jit(solution)/shard_map/ppermute | solution.py:49
  98.1 11.6 %copy-start.15 = (f32[3,128]{1,0:T(4,128)}, f32[3,128]{1,0:T(4,128)S(1)}, u32[]{:S(2)}) copy-start(f32[3,128]{1,0:T(4,128)S(1)} %collective-permute-done.4.taps_theirs) | copy-start | bytes 4612
  98.1 9.1 %collective-permute-start.3 = (bf16[16,4096]{1,0:T(8,128)(2,1)S(1)}, bf16[16,4096]{1,0:T(8,128)(2,1)S(1)}, u32[]{:S(2)}, u32[]{:S(2)}) collective-permute-start(bf16[16,4096]{1,0:T(8,128)(2,1)S(1)} %slice.48), channel_id=1, source_target_pairs={{0,16},{16,32},{32,48},{48,64},{64,80},{80,96},{96,112},{112,128},... | collective-permute-start | bytes 393224 | tf_op jit(solution)/shard_map/ppermute | solution.py:407
  107.2 2.5 %copy-start.11 = (bf16[16,4096]{1,0:T(8,128)(2,1)}, bf16[16,4096]{1,0:T(8,128)(2,1)S(1)}, u32[]{:S(2)}) copy-start(bf16[16,4096]{1,0:T(8,128)(2,1)S(1)} %collective-permute-done.3.before_ref) | copy-start | bytes 393220
  107.2 1.1 copy-start.7
  107.2 1.4 copy-start.8
  108.3 1.0 copy-start.9
  108.6 1.1 copy-start.10
  120.7 13.7 %collective-permute-start.9 = (bf16[16,2048]{1,0:T(8,128)(2,1)}, bf16[16,2048]{1,0:T(8,128)(2,1)S(1)}, u32[]{:S(2)}, u32[]{:S(2)}) collective-permute-start(bf16[16,2048]{1,0:T(8,128)(2,1)} %get-tuple-element.42), channel_id=1, source_target_pairs={{0,2},{2,4},{4,6},{6,8},{8,10},{10,12},{12,14},{14,0},{1,3},{3,5},... | collective-permute-start | bytes 196616 | tf_op jit(solution)/shard_map/ppermute | solution.py:244
  122.7 7.9 %collective-permute-start.16 = (bf16[16,2048]{1,0:T(8,128)(2,1)}, bf16[16,2048]{1,0:T(8,128)(2,1)S(1)}, u32[]{:S(2)}, u32[]{:S(2)}) collective-permute-start(bf16[16,2048]{1,0:T(8,128)(2,1)} %get-tuple-element.44), channel_id=1, source_target_pairs={{0,14},{2,0},{4,2},{6,4},{8,6},{10,8},{12,10},{14,12},{1,15},{3,1}... | collective-permute-start | bytes 196616 | tf_op jit(solution)/shard_map/ppermute | solution.py:244
  130.6 7.1 %collective-permute-start.17 = (bf16[16,2048]{1,0:T(8,128)(2,1)S(1)}, bf16[16,2048]{1,0:T(8,128)(2,1)S(1)}, u32[]{:S(2)}, u32[]{:S(2)}) collective-permute-start(bf16[16,2048]{1,0:T(8,128)(2,1)S(1)} %add_convert_fusion.6), channel_id=1, source_target_pairs={{0,14},{2,0},{4,2},{6,4},{8,6},{10,8},{12,10},{14,12},{1,15},{3,1}... | collective-permute-start | bytes 196616 | tf_op jit(solution)/shard_map/ppermute | solution.py:244
  134.4 7.1 %collective-permute-start.10 = (bf16[16,2048]{1,0:T(8,128)(2,1)S(1)}, bf16[16,2048]{1,0:T(8,128)(2,1)S(1)}, u32[]{:S(2)}, u32[]{:S(2)}) collective-permute-start(bf16[16,2048]{1,0:T(8,128)(2,1)S(1)} %add_convert_fusion.13), channel_id=1, source_target_pairs={{0,2},{2,4},{4,6},{6,8},{8,10},{10,12},{12,14},{14,0},{1,3},{3,5},... | collective-permute-start | bytes 196616 | tf_op jit(solution)/shard_map/ppermute | solution.py:244
  137.7 7.1 %collective-permute-start.18 = (bf16[16,2048]{1,0:T(8,128)(2,1)S(1)}, bf16[16,2048]{1,0:T(8,128)(2,1)S(1)}, u32[]{:S(2)}, u32[]{:S(2)}) collective-permute-start(bf16[16,2048]{1,0:T(8,128)(2,1)S(1)} %add_convert_fusion.5), channel_id=1, source_target_pairs={{0,14},{2,0},{4,2},{6,4},{8,6},{10,8},{12,10},{14,12},{1,15},{3,1}... | collective-permute-start | bytes 196616 | tf_op jit(solution)/shard_map/ppermute | solution.py:244
  141.6 7.1 %collective-permute-start.11 = (bf16[16,2048]{1,0:T(8,128)(2,1)S(1)}, bf16[16,2048]{1,0:T(8,128)(2,1)S(1)}, u32[]{:S(2)}, u32[]{:S(2)}) collective-permute-start(bf16[16,2048]{1,0:T(8,128)(2,1)S(1)} %add_convert_fusion.12), channel_id=1, source_target_pairs={{0,2},{2,4},{4,6},{6,8},{8,10},{10,12},{12,14},{14,0},{1,3},{3,5},... | collective-permute-start | bytes 196616 | tf_op jit(solution)/shard_map/ppermute | solution.py:244
  144.8 7.1 %collective-permute-start.19 = (bf16[16,2048]{1,0:T(8,128)(2,1)S(1)}, bf16[16,2048]{1,0:T(8,128)(2,1)S(1)}, u32[]{:S(2)}, u32[]{:S(2)}) collective-permute-start(bf16[16,2048]{1,0:T(8,128)(2,1)S(1)} %add_convert_fusion.4), channel_id=1, source_target_pairs={{0,14},{2,0},{4,2},{6,4},{8,6},{10,8},{12,10},{14,12},{1,15},{3,1}... | collective-permute-start | bytes 196616 | tf_op jit(solution)/shard_map/ppermute | solution.py:244
  148.7 7.1 %collective-permute-start.12 = (bf16[16,2048]{1,0:T(8,128)(2,1)S(1)}, bf16[16,2048]{1,0:T(8,128)(2,1)S(1)}, u32[]{:S(2)}, u32[]{:S(2)}) collective-permute-start(bf16[16,2048]{1,0:T(8,128)(2,1)S(1)} %add_convert_fusion.11), channel_id=1, source_target_pairs={{0,2},{2,4},{4,6},{6,8},{8,10},{10,12},{12,14},{14,0},{1,3},{3,5},... | collective-permute-start | bytes 196616 | tf_op jit(solution)/shard_map/ppermute | solution.py:244
  151.9 5.9 %collective-permute-start.20 = (bf16[16,2048]{1,0:T(8,128)(2,1)S(1)}, bf16[16,2048]{1,0:T(8,128)(2,1)S(1)}, u32[]{:S(2)}, u32[]{:S(2)}) collective-permute-start(bf16[16,2048]{1,0:T(8,128)(2,1)S(1)} %add_convert_fusion.3), channel_id=1, source_target_pairs={{0,14},{2,0},{4,2},{6,4},{8,6},{10,8},{12,10},{14,12},{1,15},{3,1}... | collective-permute-start | bytes 196616 | tf_op jit(solution)/shard_map/ppermute | solution.py:244
  155.8 5.6 %collective-permute-start.13 = (bf16[16,2048]{1,0:T(8,128)(2,1)S(1)}, bf16[16,2048]{1,0:T(8,128)(2,1)S(1)}, u32[]{:S(2)}, u32[]{:S(2)}) collective-permute-start(bf16[16,2048]{1,0:T(8,128)(2,1)S(1)} %add_convert_fusion.10), channel_id=1, source_target_pairs={{0,2},{2,4},{4,6},{6,8},{8,10},{10,12},{12,14},{14,0},{1,3},{3,5},... | collective-permute-start | bytes 196616 | tf_op jit(solution)/shard_map/ppermute | solution.py:244
  157.9 5.3 %collective-permute-start.21 = (bf16[16,2048]{1,0:T(8,128)(2,1)S(1)}, bf16[16,2048]{1,0:T(8,128)(2,1)S(1)}, u32[]{:S(2)}, u32[]{:S(2)}) collective-permute-start(bf16[16,2048]{1,0:T(8,128)(2,1)S(1)} %add_convert_fusion.2), channel_id=1, source_target_pairs={{0,14},{2,0},{4,2},{6,4},{8,6},{10,8},{12,10},{14,12},{1,15},{3,1}... | collective-permute-start | bytes 196616 | tf_op jit(solution)/shard_map/ppermute | solution.py:244
  161.3 5.6 %collective-permute-start.14 = (bf16[16,2048]{1,0:T(8,128)(2,1)S(1)}, bf16[16,2048]{1,0:T(8,128)(2,1)S(1)}, u32[]{:S(2)}, u32[]{:S(2)}) collective-permute-start(bf16[16,2048]{1,0:T(8,128)(2,1)S(1)} %add_convert_fusion.9), channel_id=1, source_target_pairs={{0,2},{2,4},{4,6},{6,8},{8,10},{10,12},{12,14},{14,0},{1,3},{3,5},... | collective-permute-start | bytes 196616 | tf_op jit(solution)/shard_map/ppermute | solution.py:244
  163.2 5.6 %collective-permute-start.22 = (bf16[16,2048]{1,0:T(8,128)(2,1)S(1)}, bf16[16,2048]{1,0:T(8,128)(2,1)S(1)}, u32[]{:S(2)}, u32[]{:S(2)}) collective-permute-start(bf16[16,2048]{1,0:T(8,128)(2,1)S(1)} %add_convert_fusion.1), channel_id=1, source_target_pairs={{0,14},{2,0},{4,2},{6,4},{8,6},{10,8},{12,10},{14,12},{1,15},{3,1}... | collective-permute-start | bytes 196616 | tf_op jit(solution)/shard_map/ppermute | solution.py:244
  166.9 5.6 %collective-permute-start.15 = (bf16[16,2048]{1,0:T(8,128)(2,1)S(1)}, bf16[16,2048]{1,0:T(8,128)(2,1)S(1)}, u32[]{:S(2)}, u32[]{:S(2)}) collective-permute-start(bf16[16,2048]{1,0:T(8,128)(2,1)S(1)} %add_convert_fusion.8), channel_id=1, source_target_pairs={{0,2},{2,4},{4,6},{6,8},{8,10},{10,12},{12,14},{14,0},{1,3},{3,5},... | collective-permute-start | bytes 196616 | tf_op jit(solution)/shard_map/ppermute | solution.py:244
  174.6 17.0 %all-to-all-start.1 = ((bf16[16,128,128]{2,1,0:T(8,128)(2,1)}), bf16[16,128,128]{2,1,0:T(8,128)(2,1)S(1)}, u32[]{:S(2)}, u32[]{:S(2)}) async-start(bf16[16,128,128]{2,1,0:T(8,128)(2,1)} %reshape.76), calls=%async_computation.2 | async-start | bytes 1048576 | tf_op jit(solution)/shard_map/all_to_all | solution.py:387
Sparse Core Ops, SparseCore 0:
  94.3 65.9 reduce-scatter.1

commit v8 on v7

--- a/solution.py
+++ b/solution.py
@@ -108,7 +108,7 @@
 def prepare(place, tokens, gain, routes, zs):
     rows, width = tokens.shape
     half = rows // 2
-    depth = 1024
+    depth = 2048
     placed = EXPERTS * CAP * zs
     fixed = lambda i, p: (0, 0)
     return pl.pallas_call(
@@ -238,7 +238,10 @@
     sums = list(outs[chains:])
     rows = sums[0].shape[0]
     zs = lax.axis_size("z")
+    held = sums
     for hop in range(zs - 1):
+        if hop == zs - 2:
+            held = list(sums)
         for chain in range(chains):
             way = 1 if chain % 2 == 0 else -1
             came = lax.ppermute(sums[chain], "z", [(i, (i + way) % zs) for i in range(zs)])
@@ -246,7 +249,7 @@
             mine = wholes[chain][block * rows : (block + 1) * rows]
             total = came.astype(jnp.float32) + mine.astype(jnp.float32)
             sums[chain] = total.astype(jnp.bfloat16)
-    return sums
+    return sums, held
 
 
 def mixer_partial(place, tokens, before, gain, taps, weights, mixes, zs):
@@ -324,7 +327,7 @@
 def expert_partial(rows, weights, downs, zs):
     count, width = rows.shape
     half = weights[0].shape[1]
-    depth = 1024
+    depth = 2048
     steps = width // depth
     early = lambda i: jnp.minimum(i, steps - 1)
     after = lambda i: jnp.maximum(i - steps, 0)
@@ -411,9 +414,12 @@
     weights = [part for array in projections for part in (array, swap_late(array))]
     mixes = (mix_weight, swap_late(mix_weight))
     partial_mix = mixer_partial(core_ref, mix_tokens, before, mix_gain, taps, weights, mixes, zs)
-    mixer_sums = ring_sum(partial_mix)
-    summed, mixer_sums = lax.optimization_barrier((summed, mixer_sums))
+    _, (own_normed, half_ranks, expert_routes) = lax.optimization_barrier(
+        (partial_mix, (own_normed, half_ranks, expert_routes))
+    )
+    mixer_sums, held = ring_sum(partial_mix)
     mixer_out = jnp.concatenate(mixer_sums, axis=1)
+    summed, _ = lax.optimization_barrier((summed, held))
     returned = exchange(summed.reshape(eps, CAP * width // 128, 128)).reshape(-1, width)
 
     own_routes = lax.dynamic_slice_in_dim(

time: 200 us -> 183 us (0.915); the launches traced: 200 us -> 180 us
  waiting for transfers between devices: 95.1 us -> 34.3 us
  blocking collectives: 0 us -> 58 us
  starting transfers between devices: 48.6 us -> 38.2 us
  local copies, waits for them, and re-layouts: 8.92 us -> 3.91 us
    all_to_all x2 -> x1, waiting for transfers between devices: 68.2 us -> 8.08 us  [exchange(): return lax.all_to_all(array, EP, split_axis=0, concat_axis=0, tiled=True)]
    all_to_all x0 -> x1, blocking collectives: none -> 58 us  [exchange(): return lax.all_to_all(array, EP, split_axis=0, concat_axis=0, tiled=True)]
    all_to_all x2 -> x1, starting transfers between devices: 15.7 us -> 5.17 us  [exchange(): return lax.all_to_all(array, EP, split_axis=0, concat_axis=0, tiled=True)]
    ppermute x5, waiting for transfers between devices: 0.01 us -> 5.13 us  [swap_late(): return lax.ppermute(value, 'core', [(0, 1), (1, 0)])]
    unnamed x36 -> x28, local copies, waits for them, and re-layouts: 5.7 us -> 0.68 us
    ppermute x14, waiting for transfers between devices: 20.5 us -> 15.5 us  [ring_sum(): lax.ppermute(sums[chain], 'z', [(i, (i + way) % zs) for i in range(zs)])]
  transfers between devices with their start and end apart: 26 -> 25, of which waited for: 11 -> 14; matrix products, arithmetic and copies ran while one was open for 3% -> 4% of each run, Pallas kernels for 8% -> 9%
where the time goes in v8:
time: 183 us; the launch traced here: 180 us
  blocking collectives  58 us (32%)
  starting transfers between devices  38.2 us (21%)
  waiting for transfers between devices  34.3 us (19%)
  Pallas kernels  25.5 us (14%)
  between operations  14.4 us (8%)
  other arithmetic  4.14 us (2%)
  local copies, waits for them, and re-layouts  3.91 us (2%)
    all_to_all x1, blocking collectives, exchange(): return lax.all_to_all(array, EP, split_axis=0, concat_axis=0, tiled=True)  58 us
    ppermute x14, starting transfers between devices, ring_sum(): lax.ppermute(sums[chain], 'z', [(i, (i + way) % zs) for i in range(zs)])  29.1 us
    ppermute x14, waiting for transfers between devices, ring_sum(): lax.ppermute(sums[chain], 'z', [(i, (i + way) % zs) for i in range(zs)])  15.5 us
    pallas_call x1, Pallas kernels, mixer_partial(): pl.pallas_call(functools.partial(mixer_kernel, steps), grid_spec=pltpu.Pr...  11.1 us
    pallas_call x1, Pallas kernels, expert_partial(): pl.pallas_call(functools.partial(expert_kernel, zs, steps), grid=(2 * ste...  9.02 us
    all_to_all x1, waiting for transfers between devices, exchange(): return lax.all_to_all(array, EP, split_axis=0, concat_axis=0, tiled=True)  8.08 us
    ppermute x1, waiting for transfers between devices, layer(): lax.ppermute(mix_tokens[mix_tokens.shape[0] - MOE_SHARE:], EP, [(i, i + 1...  5.5 us
    pallas_call x1, Pallas kernels, prepare(): pl.pallas_call(functools.partial(prep_kernel, zs), grid_spec=pltpu.Prefet...  5.33 us
  transfers between devices with their start and end apart: 25, of which 14 were waited for; matrix products, arithmetic and copies ran while one was open for 4% of the time, Pallas kernels for 9%

profile of v8, /device:TPU:2, one launch (start us, length us, event | category | flops | bytes accessed | tf_op | source)
XLA Modules:
  0.0 179.7 jit_solution(11274901383991181057)
XLA Ops:
  7.2 0.0 copy-start
  7.2 0.0 reduce-scatter.2.cloned.1.call-start
  7.2 0.1 collective-permute-start
  7.3 0.5 collective-permute-start.1
  7.8 0.1 collective-permute-start.2
  7.9 0.7 pad_add_fusion.place_ref
  8.6 5.3 %prepare.1 = (bf16[512,4096]{1,0:T(8,128)(2,1)}, bf16[16,4096]{1,0:T(8,128)(2,1)}, s32[2,128]{1,0:T(2,128)}) custom-call(s32[2]{0:T(128)} %pad_add_fusion.place_ref, bf16[8,2,16,4096]{3,2,1,0:T(8,128)(2,1)} %bitcast.26, f32[1,4096]{1,0:T(1,128)} %bitcast.33, s32[2,256]{1,0:T(2,128)} %bitcast.35), custom_call_target="tpu_custom_call" | custom-call | flops 536870912 | bytes 5242880 | tf_op jit(solution)/shard_map/prepare/pallas_call | solution.py:114
  13.9 0.0 collective-permute-done.g1
  14.0 58.0 %all_to_all.10 = bf16[16,32,4096]{2,1,0:T(8,128)(2,1)} all-to-all(bf16[16,32,4096]{2,1,0:T(8,128)(2,1)} %bitcast.25), channel_id=1, replica_groups=mesh['y'=4,'x'=4,'z'=8,'core'=2] {'y','x'}, dimensions={0} | all-to-all | bytes 8388608 | tf_op jit(solution)/shard_map/all_to_all | solution.py:390
  71.9 0.0 copy-start.4
  72.0 0.0 copy-start.5
  72.0 0.0 copy-start.6
  72.0 9.0 %experts.1 = bf16[512,4096]{1,0:T(8,128)(2,1)} custom-call(bf16[512,4096]{1,0:T(8,128)(2,1)} %bitcast.22, bf16[4096,128]{1,0:T(8,128)(2,1)} %bitcast.28, bf16[4096,128]{1,0:T(8,128)(2,1)} %copy-done.1, bf16[4096,128]{1,0:T(8,128)(2,1)} %bitcast.30, bf16[4096,128]{1,0:T(8,128)(2,1)} %copy-done.2, bf16[128,4096]{1,0:T(8,128)(2,1)} %bitcast.32, ...), custom_call_target="tpu_custom_call" | custom-call | flops 3221225472 | bytes 14680064 | tf_op jit(solution)/shard_map/experts/pallas_call | solution.py:334
  81.0 0.1 collective-permute-start.5
  81.1 0.5 collective-permute-start.6
  81.6 0.1 collective-permute-start.7
  81.7 0.4 collective-permute-start.8
  82.1 0.0 reduce-scatter.2.cloned.1.call-update
  82.2 0.2 collective-permute-start.4
  82.4 0.9 slice.48
  83.3 5.1 %collective-permute-done.4.taps_theirs = f32[3,128]{1,0:T(4,128)S(1)} collective-permute-done((f32[3,128]{1,0:T(4,128)S(1)}, f32[3,128]{1,0:T(4,128)S(1)}, u32[]{:S(2)}, u32[]{:S(2)}) %collective-permute-start.4) | collective-permute-done | bytes 1568 | tf_op jit(solution)/shard_map/ppermute | solution.py:49
  88.4 1.9 %collective-permute-start.3 = (bf16[16,4096]{1,0:T(8,128)(2,1)S(1)}, bf16[16,4096]{1,0:T(8,128)(2,1)S(1)}, u32[]{:S(2)}, u32[]{:S(2)}) collective-permute-start(bf16[16,4096]{1,0:T(8,128)(2,1)S(1)} %slice.48), channel_id=1, source_target_pairs={{0,16},{16,32},{32,48},{48,64},{64,80},{80,96},{96,112},{112,128},... | collective-permute-start | bytes 393224 | tf_op jit(solution)/shard_map/ppermute | solution.py:410
  90.3 5.5 %collective-permute-done.3.before_ref = bf16[16,4096]{1,0:T(8,128)(2,1)S(1)} collective-permute-done((bf16[16,4096]{1,0:T(8,128)(2,1)S(1)}, bf16[16,4096]{1,0:T(8,128)(2,1)S(1)}, u32[]{:S(2)}, u32[]{:S(2)}) %collective-permute-start.3) | collective-permute-done | bytes 131104 | tf_op jit(solution)/shard_map/ppermute | solution.py:410
  95.9 0.6 copy-done.7
  96.5 11.1 %mixer.1 = (bf16[128,2048]{1,0:T(8,128)(2,1)}, bf16[128,2048]{1,0:T(8,128)(2,1)}, bf16[16,2048]{1,0:T(8,128)(2,1)}, bf16[16,2048]{1,0:T(8,128)(2,1)}) custom-call(s32[2]{0:T(128)} %pad_add_fusion.place_ref, bf16[8,2,16,4096]{3,2,1,0:T(8,128)(2,1)} %bitcast.23, bf16[8,2,16,4096]{3,2,1,0:T(8,128)(2,1)} %bitcast.24, bf16[16,4096]{1,0:T(8,128)(2,1)} %copy-done.7, ...), custom_call_target="tpu_custom_call" | custom-call | flops 1577058304 | bytes 11141120 | tf_op jit(solution)/shard_map/mixer/pallas_call | solution.py:267
  107.6 2.1 %collective-permute-start.9 = (bf16[16,2048]{1,0:T(8,128)(2,1)}, bf16[16,2048]{1,0:T(8,128)(2,1)S(1)}, u32[]{:S(2)}, u32[]{:S(2)}) collective-permute-start(bf16[16,2048]{1,0:T(8,128)(2,1)} %get-tuple-element.43), channel_id=1, source_target_pairs={{0,2},{2,4},{4,6},{6,8},{8,10},{10,12},{12,14},{14,0},{1,3},{3,5},... | collective-permute-start | bytes 196616 | tf_op jit(solution)/shard_map/ppermute | solution.py:247
  109.6 4.2 %collective-permute-start.16 = (bf16[16,2048]{1,0:T(8,128)(2,1)}, bf16[16,2048]{1,0:T(8,128)(2,1)S(1)}, u32[]{:S(2)}, u32[]{:S(2)}) collective-permute-start(bf16[16,2048]{1,0:T(8,128)(2,1)} %get-tuple-element.45), channel_id=1, source_target_pairs={{0,14},{2,0},{4,2},{6,4},{8,6},{10,8},{12,10},{14,12},{1,15},{3,1}... | collective-permute-start | bytes 196616 | tf_op jit(solution)/shard_map/ppermute | solution.py:247
  113.9 1.1 broadcast_multiply_fusion.1
  114.9 1.1 broadcast_multiply_fusion
  116.1 0.1 bitcast_add_fusion
  116.2 0.2 fusion.1
  116.4 0.2 fusion.2
  116.5 0.2 select_reduce_fusion.1
  116.7 0.1 select_reduce_fusion
  116.8 0.8 collective-permute-done.16
  117.6 3.7 %collective-permute-start.17 = (bf16[16,2048]{1,0:T(8,128)(2,1)S(1)}, bf16[16,2048]{1,0:T(8,128)(2,1)S(1)}, u32[]{:S(2)}, u32[]{:S(2)}) collective-permute-start(bf16[16,2048]{1,0:T(8,128)(2,1)S(1)} %add_convert_fusion.6), channel_id=1, source_target_pairs={{0,14},{2,0},{4,2},{6,4},{8,6},{10,8},{12,10},{14,12},{1,15},{3,1}... | collective-permute-start | bytes 196616 | tf_op jit(solution)/shard_map/ppermute | solution.py:247
  121.3 0.1 collective-permute-start.10
  121.4 3.1 %collective-permute-done.17 = bf16[16,2048]{1,0:T(8,128)(2,1)S(1)} collective-permute-done((bf16[16,2048]{1,0:T(8,128)(2,1)S(1)}, bf16[16,2048]{1,0:T(8,128)(2,1)S(1)}, u32[]{:S(2)}, u32[]{:S(2)}) %collective-permute-start.17) | collective-permute-done | bytes 65568 | tf_op jit(solution)/shard_map/ppermute | solution.py:247
  124.5 3.8 %collective-permute-start.18 = (bf16[16,2048]{1,0:T(8,128)(2,1)S(1)}, bf16[16,2048]{1,0:T(8,128)(2,1)S(1)}, u32[]{:S(2)}, u32[]{:S(2)}) collective-permute-start(bf16[16,2048]{1,0:T(8,128)(2,1)S(1)} %add_convert_fusion.5), channel_id=1, source_target_pairs={{0,14},{2,0},{4,2},{6,4},{8,6},{10,8},{12,10},{14,12},{1,15},{3,1}... | collective-permute-start | bytes 196616 | tf_op jit(solution)/shard_map/ppermute | solution.py:247
  128.2 0.1 collective-permute-done.10
  128.4 0.1 collective-permute-start.11
  128.5 3.1 %collective-permute-done.18 = bf16[16,2048]{1,0:T(8,128)(2,1)S(1)} collective-permute-done((bf16[16,2048]{1,0:T(8,128)(2,1)S(1)}, bf16[16,2048]{1,0:T(8,128)(2,1)S(1)}, u32[]{:S(2)}, u32[]{:S(2)}) %collective-permute-start.18) | collective-permute-done | bytes 65568 | tf_op jit(solution)/shard_map/ppermute | solution.py:247
  131.6 3.8 %collective-permute-start.19 = (bf16[16,2048]{1,0:T(8,128)(2,1)S(1)}, bf16[16,2048]{1,0:T(8,128)(2,1)S(1)}, u32[]{:S(2)}, u32[]{:S(2)}) collective-permute-start(bf16[16,2048]{1,0:T(8,128)(2,1)S(1)} %add_convert_fusion.4), channel_id=1, source_target_pairs={{0,14},{2,0},{4,2},{6,4},{8,6},{10,8},{12,10},{14,12},{1,15},{3,1}... | collective-permute-start | bytes 196616 | tf_op jit(solution)/shard_map/ppermute | solution.py:247
  135.3 0.1 collective-permute-done.11
  135.5 0.1 collective-permute-start.12
  135.6 2.8 %collective-permute-done.19 = bf16[16,2048]{1,0:T(8,128)(2,1)S(1)} collective-permute-done((bf16[16,2048]{1,0:T(8,128)(2,1)S(1)}, bf16[16,2048]{1,0:T(8,128)(2,1)S(1)}, u32[]{:S(2)}, u32[]{:S(2)}) %collective-permute-start.19) | collective-permute-done | bytes 65568 | tf_op jit(solution)/shard_map/ppermute | solution.py:247
  138.4 3.8 %collective-permute-start.20 = (bf16[16,2048]{1,0:T(8,128)(2,1)S(1)}, bf16[16,2048]{1,0:T(8,128)(2,1)S(1)}, u32[]{:S(2)}, u32[]{:S(2)}) collective-permute-start(bf16[16,2048]{1,0:T(8,128)(2,1)S(1)} %add_convert_fusion.3), channel_id=1, source_target_pairs={{0,14},{2,0},{4,2},{6,4},{8,6},{10,8},{12,10},{14,12},{1,15},{3,1}... | collective-permute-start | bytes 196616 | tf_op jit(solution)/shard_map/ppermute | solution.py:247
  142.2 0.1 collective-permute-start.13
  142.3 2.0 %collective-permute-done.20 = bf16[16,2048]{1,0:T(8,128)(2,1)S(1)} collective-permute-done((bf16[16,2048]{1,0:T(8,128)(2,1)S(1)}, bf16[16,2048]{1,0:T(8,128)(2,1)S(1)}, u32[]{:S(2)}, u32[]{:S(2)}) %collective-permute-start.20) | collective-permute-done | bytes 65568 | tf_op jit(solution)/shard_map/ppermute | solution.py:247
  144.3 3.8 %collective-permute-start.21 = (bf16[16,2048]{1,0:T(8,128)(2,1)S(1)}, bf16[16,2048]{1,0:T(8,128)(2,1)S(1)}, u32[]{:S(2)}, u32[]{:S(2)}) collective-permute-start(bf16[16,2048]{1,0:T(8,128)(2,1)S(1)} %add_convert_fusion.2), channel_id=1, source_target_pairs={{0,14},{2,0},{4,2},{6,4},{8,6},{10,8},{12,10},{14,12},{1,15},{3,1}... | collective-permute-start | bytes 196616 | tf_op jit(solution)/shard_map/ppermute | solution.py:247
  148.0 0.3 collective-permute-done.13
  148.4 0.1 collective-permute-start.14
  148.4 1.5 collective-permute-done.21
  150.0 3.6 %collective-permute-start.22 = (bf16[16,2048]{1,0:T(8,128)(2,1)S(1)}, bf16[16,2048]{1,0:T(8,128)(2,1)S(1)}, u32[]{:S(2)}, u32[]{:S(2)}) collective-permute-start(bf16[16,2048]{1,0:T(8,128)(2,1)S(1)} %add_convert_fusion.1), channel_id=1, source_target_pairs={{0,14},{2,0},{4,2},{6,4},{8,6},{10,8},{12,10},{14,12},{1,15},{3,1}... | collective-permute-start | bytes 196616 | tf_op jit(solution)/shard_map/ppermute | solution.py:247
  153.6 0.3 collective-permute-done.14
  153.9 0.1 collective-permute-start.15
  154.0 1.5 collective-permute-done.22
  155.6 0.0 reduce-scatter.2.cloned.1.call-done
  155.6 2.1 %reshape.76 = bf16[16,128,128]{2,1,0:T(8,128)(2,1)} reshape(bf16[64,4096]{1,0:T(8,128)(2,1)} %reduce-scatter.2.cloned.1.call-done) | data formatting | bytes 1048576 | tf_op jit(solution)/shard_map/reshape | solution.py:423
  157.7 5.2 %all-to-all-start.1 = ((bf16[16,128,128]{2,1,0:T(8,128)(2,1)}), bf16[16,128,128]{2,1,0:T(8,128)(2,1)S(1)}, u32[]{:S(2)}, u32[]{:S(2)}) async-start(bf16[16,128,128]{2,1,0:T(8,128)(2,1)} %reshape.76), calls=%async_computation.2 | async-start | bytes 1048576 | tf_op jit(solution)/shard_map/all_to_all | solution.py:390
  162.9 0.7 pad_maximum_fusion
  163.5 8.1 %all-to-all-done.1 = bf16[16,128,128]{2,1,0:T(8,128)(2,1)S(1)} async-done(((bf16[16,128,128]{2,1,0:T(8,128)(2,1)}), bf16[16,128,128]{2,1,0:T(8,128)(2,1)S(1)}, u32[]{:S(2)}, u32[]{:S(2)}) %all-to-all-start.1) | async-done | bytes 524320 | tf_op jit(solution)/shard_map/all_to_all | solution.py:390
  171.6 0.2 reshape.77
  171.8 1.0 convolution_convert_fusion
  (50 shorter events, 0.4 us)
Async XLA Ops:
  7.2 109.2 %copy-start = (bf16[4096,16]{0,1:T(8,128)(2,1)S(1)}, bf16[4096,16]{0,1:T(8,128)(2,1)}, u32[]{:S(2)}) copy-start(bf16[4096,16]{0,1:T(8,128)(2,1)} %param.25) | copy-start | bytes 393220
  7.2 148.4 %reduce-scatter.2.cloned.1.call-start = ((), (), s32[]{:S(2)}) async-start(), calls=%async_computation.3 | async-start | bytes 4718592 | tf_op jit(solution)/shard_map/reduce_scatter | solution.py:394
  7.2 6.7 %collective-permute-start = (bf16[4096,128]{1,0:T(8,128)(2,1)}, bf16[4096,128]{1,0:T(8,128)(2,1)S(1)}, u32[]{:S(2)}, u32[]{:S(2)}) collective-permute-start(bf16[4096,128]{1,0:T(8,128)(2,1)} %bitcast.27), channel_id=1, source_target_pairs={{0,1},{1,0},{2,3},{3,2},{4,5},{5,4},{6,7},{7,6},{8,9},{9,8},{10,11... | collective-permute-start | bytes 3145736 | tf_op jit(solution)/shard_map/ppermute | solution.py:45
  7.3 6.6 %collective-permute-start.1 = (bf16[4096,128]{1,0:T(8,128)(2,1)}, bf16[4096,128]{1,0:T(8,128)(2,1)S(1)}, u32[]{:S(2)}, u32[]{:S(2)}) collective-permute-start(bf16[4096,128]{1,0:T(8,128)(2,1)} %bitcast.29), channel_id=1, source_target_pairs={{0,1},{1,0},{2,3},{3,2},{4,5},{5,4},{6,7},{7,6},{8,9},{9,8},{10,11... | collective-permute-start | bytes 3145736 | tf_op jit(solution)/shard_map/ppermute | solution.py:45
  7.8 6.1 %collective-permute-start.2 = (bf16[128,4096]{1,0:T(8,128)(2,1)}, bf16[128,4096]{1,0:T(8,128)(2,1)S(1)}, u32[]{:S(2)}, u32[]{:S(2)}) collective-permute-start(bf16[128,4096]{1,0:T(8,128)(2,1)} %bitcast.31), channel_id=1, source_target_pairs={{0,1},{1,0},{2,3},{3,2},{4,5},{5,4},{6,7},{7,6},{8,9},{9,8},{10,11... | collective-permute-start | bytes 3145736 | tf_op jit(solution)/shard_map/ppermute | solution.py:45
  13.9 58.0 %copy-start.1 = (bf16[4096,128]{1,0:T(8,128)(2,1)}, bf16[4096,128]{1,0:T(8,128)(2,1)S(1)}, u32[]{:S(2)}) copy-start(bf16[4096,128]{1,0:T(8,128)(2,1)S(1)} %collective-permute-done.g1) | copy-start | bytes 3145732
  13.9 58.0 %copy-start.2 = (bf16[4096,128]{1,0:T(8,128)(2,1)}, bf16[4096,128]{1,0:T(8,128)(2,1)S(1)}, u32[]{:S(2)}) copy-start(bf16[4096,128]{1,0:T(8,128)(2,1)S(1)} %collective-permute-done.1.u1) | copy-start | bytes 3145732
  14.0 58.0 %copy-start.3 = (bf16[128,4096]{1,0:T(8,128)(2,1)}, bf16[128,4096]{1,0:T(8,128)(2,1)S(1)}, u32[]{:S(2)}) copy-start(bf16[128,4096]{1,0:T(8,128)(2,1)S(1)} %collective-permute-done.2.d1) | copy-start | bytes 3145732
  71.9 9.1 %copy-start.4 = (bf16[4096,128]{1,0:T(8,128)(2,1)S(1)}, bf16[4096,128]{1,0:T(8,128)(2,1)}, u32[]{:S(2)}) copy-start(bf16[4096,128]{1,0:T(8,128)(2,1)} %refs_0_) | copy-start | bytes 3145732
  72.0 9.2 %copy-start.5 = (bf16[4096,128]{1,0:T(8,128)(2,1)S(1)}, bf16[4096,128]{1,0:T(8,128)(2,1)}, u32[]{:S(2)}) copy-start(bf16[4096,128]{1,0:T(8,128)(2,1)} %refs_2_) | copy-start | bytes 3145732
  72.0 9.6 %copy-start.6 = (bf16[4096,128]{1,0:T(8,128)(2,1)S(1)}, bf16[4096,128]{1,0:T(8,128)(2,1)}, u32[]{:S(2)}) copy-start(bf16[4096,128]{1,0:T(8,128)(2,1)} %refs_4_) | copy-start | bytes 3145732
  81.0 1.1 copy-start.10
  81.0 14.8 %collective-permute-start.5 = (bf16[4096,128]{1,0:T(8,128)(2,1)S(1)}, bf16[4096,128]{1,0:T(8,128)(2,1)}, u32[]{:S(2)}, u32[]{:S(2)}) collective-permute-start(bf16[4096,128]{1,0:T(8,128)(2,1)S(1)} %copy-done.4), channel_id=1, source_target_pairs={{0,1},{1,0},{2,3},{3,2},{4,5},{5,4},{6,7},{7,6},{8,9},{9,8},{10,11... | collective-permute-start | bytes 3145736 | tf_op jit(solution)/shard_map/ppermute | solution.py:49
  81.1 14.7 %collective-permute-start.6 = (bf16[4096,128]{1,0:T(8,128)(2,1)S(1)}, bf16[4096,128]{1,0:T(8,128)(2,1)}, u32[]{:S(2)}, u32[]{:S(2)}) collective-permute-start(bf16[4096,128]{1,0:T(8,128)(2,1)S(1)} %copy-done.5), channel_id=1, source_target_pairs={{0,1},{1,0},{2,3},{3,2},{4,5},{5,4},{6,7},{7,6},{8,9},{9,8},{10,11... | collective-permute-start | bytes 3145736 | tf_op jit(solution)/shard_map/ppermute | solution.py:49
  81.6 14.2 %collective-permute-start.7 = (bf16[4096,128]{1,0:T(8,128)(2,1)S(1)}, bf16[4096,128]{1,0:T(8,128)(2,1)}, u32[]{:S(2)}, u32[]{:S(2)}) collective-permute-start(bf16[4096,128]{1,0:T(8,128)(2,1)S(1)} %copy-done.6), channel_id=1, source_target_pairs={{0,1},{1,0},{2,3},{3,2},{4,5},{5,4},{6,7},{7,6},{8,9},{9,8},{10,11... | collective-permute-start | bytes 3145736 | tf_op jit(solution)/shard_map/ppermute | solution.py:49
  81.7 14.1 %collective-permute-start.8 = (bf16[128,4096]{1,0:T(8,128)(2,1)}, bf16[128,4096]{1,0:T(8,128)(2,1)}, u32[]{:S(2)}, u32[]{:S(2)}) collective-permute-start(bf16[128,4096]{1,0:T(8,128)(2,1)} %refs_6_), channel_id=1, source_target_pairs={{0,1},{1,0},{2,3},{3,2},{4,5},{5,4},{6,7},{7,6},{8,9},{9,8},{10,11... | collective-permute-start | bytes 3145736 | tf_op jit(solution)/shard_map/ppermute | solution.py:49
  82.2 6.2 %collective-permute-start.4 = (f32[3,128]{1,0:T(4,128)S(1)}, f32[3,128]{1,0:T(4,128)S(1)}, u32[]{:S(2)}, u32[]{:S(2)}) collective-permute-start(f32[3,128]{1,0:T(4,128)S(1)} %copy-done.10), channel_id=1, source_target_pairs={{0,1},{1,0},{2,3},{3,2},{4,5},{5,4},{6,7},{7,6},{8,9},{9,8},{10,11... | collective-permute-start | bytes 4616 | tf_op jit(solution)/shard_map/ppermute | solution.py:49
  88.4 7.5 %copy-start.11 = (f32[3,128]{1,0:T(4,128)}, f32[3,128]{1,0:T(4,128)S(1)}, u32[]{:S(2)}) copy-start(f32[3,128]{1,0:T(4,128)S(1)} %collective-permute-done.4.taps_theirs) | copy-start | bytes 4612
  88.4 7.4 %collective-permute-start.3 = (bf16[16,4096]{1,0:T(8,128)(2,1)S(1)}, bf16[16,4096]{1,0:T(8,128)(2,1)S(1)}, u32[]{:S(2)}, u32[]{:S(2)}) collective-permute-start(bf16[16,4096]{1,0:T(8,128)(2,1)S(1)} %slice.48), channel_id=1, source_target_pairs={{0,16},{16,32},{32,48},{48,64},{64,80},{80,96},{96,112},{112,128},... | collective-permute-start | bytes 393224 | tf_op jit(solution)/shard_map/ppermute | solution.py:410
  95.8 0.7 copy-start.7
  96.5 19.6 %copy-start.9 = (s32[256,2]{0,1:T(2,128)S(1)}, s32[256,2]{0,1:T(2,128)}, u32[]{:S(2)}) copy-start(s32[256,2]{0,1:T(2,128)} %param.26) | copy-start | bytes 6148
  96.5 19.6 %copy-start.12 = (s32[2,128]{1,0:T(2,128)S(1)}, s32[2,128]{1,0:T(2,128)}, u32[]{:S(2)}) copy-start(s32[2,128]{1,0:T(2,128)} %get-tuple-element.51) | copy-start | bytes 3076
  96.5 19.7 %copy-start.8 = (bf16[16,4096]{1,0:T(8,128)(2,1)S(1)}, bf16[16,4096]{1,0:T(8,128)(2,1)}, u32[]{:S(2)}) copy-start(bf16[16,4096]{1,0:T(8,128)(2,1)} %get-tuple-element.52) | copy-start | bytes 393220
  96.5 19.7 %copy-start.13 = (bf16[4096,4]{0,1:T(4,128)(2,1)S(1)}, bf16[4096,4]{0,1:T(4,128)(2,1)}, u32[]{:S(2)}) copy-start(bf16[4096,4]{0,1:T(4,128)(2,1)} %param.24) | copy-start | bytes 98308
  107.6 13.7 %collective-permute-start.9 = (bf16[16,2048]{1,0:T(8,128)(2,1)}, bf16[16,2048]{1,0:T(8,128)(2,1)S(1)}, u32[]{:S(2)}, u32[]{:S(2)}) collective-permute-start(bf16[16,2048]{1,0:T(8,128)(2,1)} %get-tuple-element.43), channel_id=1, source_target_pairs={{0,2},{2,4},{4,6},{6,8},{8,10},{10,12},{12,14},{14,0},{1,3},{3,5},... | collective-permute-start | bytes 196616 | tf_op jit(solution)/shard_map/ppermute | solution.py:247
  109.6 7.9 %collective-permute-start.16 = (bf16[16,2048]{1,0:T(8,128)(2,1)}, bf16[16,2048]{1,0:T(8,128)(2,1)S(1)}, u32[]{:S(2)}, u32[]{:S(2)}) collective-permute-start(bf16[16,2048]{1,0:T(8,128)(2,1)} %get-tuple-element.45), channel_id=1, source_target_pairs={{0,14},{2,0},{4,2},{6,4},{8,6},{10,8},{12,10},{14,12},{1,15},{3,1}... | collective-permute-start | bytes 196616 | tf_op jit(solution)/shard_map/ppermute | solution.py:247
  117.6 6.9 %collective-permute-start.17 = (bf16[16,2048]{1,0:T(8,128)(2,1)S(1)}, bf16[16,2048]{1,0:T(8,128)(2,1)S(1)}, u32[]{:S(2)}, u32[]{:S(2)}) collective-permute-start(bf16[16,2048]{1,0:T(8,128)(2,1)S(1)} %add_convert_fusion.6), channel_id=1, source_target_pairs={{0,14},{2,0},{4,2},{6,4},{8,6},{10,8},{12,10},{14,12},{1,15},{3,1}... | collective-permute-start | bytes 196616 | tf_op jit(solution)/shard_map/ppermute | solution.py:247
  121.3 7.1 %collective-permute-start.10 = (bf16[16,2048]{1,0:T(8,128)(2,1)S(1)}, bf16[16,2048]{1,0:T(8,128)(2,1)S(1)}, u32[]{:S(2)}, u32[]{:S(2)}) collective-permute-start(bf16[16,2048]{1,0:T(8,128)(2,1)S(1)} %add_convert_fusion.13), channel_id=1, source_target_pairs={{0,2},{2,4},{4,6},{6,8},{8,10},{10,12},{12,14},{14,0},{1,3},{3,5},... | collective-permute-start | bytes 196616 | tf_op jit(solution)/shard_map/ppermute | solution.py:247
  124.5 7.1 %collective-permute-start.18 = (bf16[16,2048]{1,0:T(8,128)(2,1)S(1)}, bf16[16,2048]{1,0:T(8,128)(2,1)S(1)}, u32[]{:S(2)}, u32[]{:S(2)}) collective-permute-start(bf16[16,2048]{1,0:T(8,128)(2,1)S(1)} %add_convert_fusion.5), channel_id=1, source_target_pairs={{0,14},{2,0},{4,2},{6,4},{8,6},{10,8},{12,10},{14,12},{1,15},{3,1}... | collective-permute-start | bytes 196616 | tf_op jit(solution)/shard_map/ppermute | solution.py:247
  128.4 7.1 %collective-permute-start.11 = (bf16[16,2048]{1,0:T(8,128)(2,1)S(1)}, bf16[16,2048]{1,0:T(8,128)(2,1)S(1)}, u32[]{:S(2)}, u32[]{:S(2)}) collective-permute-start(bf16[16,2048]{1,0:T(8,128)(2,1)S(1)} %add_convert_fusion.12), channel_id=1, source_target_pairs={{0,2},{2,4},{4,6},{6,8},{8,10},{10,12},{12,14},{14,0},{1,3},{3,5},... | collective-permute-start | bytes 196616 | tf_op jit(solution)/shard_map/ppermute | solution.py:247
  131.6 6.8 %collective-permute-start.19 = (bf16[16,2048]{1,0:T(8,128)(2,1)S(1)}, bf16[16,2048]{1,0:T(8,128)(2,1)S(1)}, u32[]{:S(2)}, u32[]{:S(2)}) collective-permute-start(bf16[16,2048]{1,0:T(8,128)(2,1)S(1)} %add_convert_fusion.4), channel_id=1, source_target_pairs={{0,14},{2,0},{4,2},{6,4},{8,6},{10,8},{12,10},{14,12},{1,15},{3,1}... | collective-permute-start | bytes 196616 | tf_op jit(solution)/shard_map/ppermute | solution.py:247
  135.5 6.7 %collective-permute-start.12 = (bf16[16,2048]{1,0:T(8,128)(2,1)S(1)}, bf16[16,2048]{1,0:T(8,128)(2,1)S(1)}, u32[]{:S(2)}, u32[]{:S(2)}) collective-permute-start(bf16[16,2048]{1,0:T(8,128)(2,1)S(1)} %add_convert_fusion.11), channel_id=1, source_target_pairs={{0,2},{2,4},{4,6},{6,8},{8,10},{10,12},{12,14},{14,0},{1,3},{3,5},... | collective-permute-start | bytes 196616 | tf_op jit(solution)/shard_map/ppermute | solution.py:247
  138.4 5.9 %collective-permute-start.20 = (bf16[16,2048]{1,0:T(8,128)(2,1)S(1)}, bf16[16,2048]{1,0:T(8,128)(2,1)S(1)}, u32[]{:S(2)}, u32[]{:S(2)}) collective-permute-start(bf16[16,2048]{1,0:T(8,128)(2,1)S(1)} %add_convert_fusion.3), channel_id=1, source_target_pairs={{0,14},{2,0},{4,2},{6,4},{8,6},{10,8},{12,10},{14,12},{1,15},{3,1}... | collective-permute-start | bytes 196616 | tf_op jit(solution)/shard_map/ppermute | solution.py:247
  142.2 6.1 %collective-permute-start.13 = (bf16[16,2048]{1,0:T(8,128)(2,1)S(1)}, bf16[16,2048]{1,0:T(8,128)(2,1)S(1)}, u32[]{:S(2)}, u32[]{:S(2)}) collective-permute-start(bf16[16,2048]{1,0:T(8,128)(2,1)S(1)} %add_convert_fusion.10), channel_id=1, source_target_pairs={{0,2},{2,4},{4,6},{6,8},{8,10},{10,12},{12,14},{14,0},{1,3},{3,5},... | collective-permute-start | bytes 196616 | tf_op jit(solution)/shard_map/ppermute | solution.py:247
  144.3 5.7 %collective-permute-start.21 = (bf16[16,2048]{1,0:T(8,128)(2,1)S(1)}, bf16[16,2048]{1,0:T(8,128)(2,1)S(1)}, u32[]{:S(2)}, u32[]{:S(2)}) collective-permute-start(bf16[16,2048]{1,0:T(8,128)(2,1)S(1)} %add_convert_fusion.2), channel_id=1, source_target_pairs={{0,14},{2,0},{4,2},{6,4},{8,6},{10,8},{12,10},{14,12},{1,15},{3,1}... | collective-permute-start | bytes 196616 | tf_op jit(solution)/shard_map/ppermute | solution.py:247
  148.4 5.6 %collective-permute-start.14 = (bf16[16,2048]{1,0:T(8,128)(2,1)S(1)}, bf16[16,2048]{1,0:T(8,128)(2,1)S(1)}, u32[]{:S(2)}, u32[]{:S(2)}) collective-permute-start(bf16[16,2048]{1,0:T(8,128)(2,1)S(1)} %add_convert_fusion.9), channel_id=1, source_target_pairs={{0,2},{2,4},{4,6},{6,8},{8,10},{10,12},{12,14},{14,0},{1,3},{3,5},... | collective-permute-start | bytes 196616 | tf_op jit(solution)/shard_map/ppermute | solution.py:247
  150.0 5.6 %collective-permute-start.22 = (bf16[16,2048]{1,0:T(8,128)(2,1)S(1)}, bf16[16,2048]{1,0:T(8,128)(2,1)S(1)}, u32[]{:S(2)}, u32[]{:S(2)}) collective-permute-start(bf16[16,2048]{1,0:T(8,128)(2,1)S(1)} %add_convert_fusion.1), channel_id=1, source_target_pairs={{0,14},{2,0},{4,2},{6,4},{8,6},{10,8},{12,10},{14,12},{1,15},{3,1}... | collective-permute-start | bytes 196616 | tf_op jit(solution)/shard_map/ppermute | solution.py:247
  153.9 8.9 %collective-permute-start.15 = (bf16[16,2048]{1,0:T(8,128)(2,1)S(1)}, bf16[16,2048]{1,0:T(8,128)(2,1)S(1)}, u32[]{:S(2)}, u32[]{:S(2)}) collective-permute-start(bf16[16,2048]{1,0:T(8,128)(2,1)S(1)} %add_convert_fusion.8), channel_id=1, source_target_pairs={{0,2},{2,4},{4,6},{6,8},{8,10},{10,12},{12,14},{14,0},{1,3},{3,5},... | collective-permute-start | bytes 196616 | tf_op jit(solution)/shard_map/ppermute | solution.py:247
  157.7 13.9 %all-to-all-start.1 = ((bf16[16,128,128]{2,1,0:T(8,128)(2,1)}), bf16[16,128,128]{2,1,0:T(8,128)(2,1)S(1)}, u32[]{:S(2)}, u32[]{:S(2)}) async-start(bf16[16,128,128]{2,1,0:T(8,128)(2,1)} %reshape.76), calls=%async_computation.2 | async-start | bytes 1048576 | tf_op jit(solution)/shard_map/all_to_all | solution.py:390
Sparse Core Ops, SparseCore 0:
  82.3 60.3 reduce-scatter.1

commit v9 on v8

--- a/solution.py
+++ b/solution.py
@@ -79,10 +79,10 @@
     @pl.when(step == 0)
     def _():
         normed_ref[...] = scaled_rows(tokens_ref[...].reshape(rows, width), gain_ref[...])
-        own_ref[...] = normed_ref[pl.ds(pl.multiple_of(place_ref[1] * share, share), share), :]
+        own_ref[...] = normed_ref[pl.ds(pl.multiple_of((place_ref[0] >> 1) * share, share), share), :]
         token = iota((1, rows), 1)
         block = token // share
-        source = block * (2 * share) + place_ref[0] * share + token % share
+        source = block * (2 * share) + (place_ref[0] & 1) * share + token % share
         pick = select_matrix(iota((2 * rows, 1), 0) == source)
         routes = routes_ref[...].astype(jnp.float32).astype(jnp.bfloat16)
         routes = product(routes, pick).astype(jnp.int32)
@@ -117,7 +117,7 @@
             num_scalar_prefetch=1,
             grid=(width // depth,),
             in_specs=[
-                pl.BlockSpec((zs, 1, MOE_SHARE, width), lambda i, p: (0, p[0], 0, 0)),
+                pl.BlockSpec((zs, 1, MOE_SHARE, width), lambda i, p: (0, (p[0] & 1), 0, 0)),
                 pl.BlockSpec((1, width), fixed),
                 pl.BlockSpec((TOPK, rows), fixed),
             ],
@@ -186,7 +186,7 @@
         gated = (pair(1) * pair(0)).astype(jnp.bfloat16)
         row, source = iota((rows, 1), 0), iota((1, total), 1)
         place = row % MOE_SHARE
-        ahead = row // MOE_SHARE + place_ref[0]
+        ahead = row // MOE_SHARE + (place_ref[0] & 1)
         tail = jnp.where(ahead == 0, total, rows + ahead * tail_rows)
         taps = jnp.concatenate([taps_mine[...], taps_theirs[...]], axis=1)
         mixed = None
@@ -198,7 +198,7 @@
             mixed = term if mixed is None else mixed + term
         channels = (pair(2)[0:rows] * mixed).astype(jnp.bfloat16)
         target, source = iota((rows, 1), 0), iota((1, rows), 1)
-        turned = (source // MOE_SHARE - place_ref[1] + blocks) % blocks
+        turned = (source // MOE_SHARE - (place_ref[0] >> 1) + blocks) % blocks
         order = select_matrix(target == turned * MOE_SHARE + source % MOE_SHARE)
         channels_ref[...] = product(order, channels).astype(jnp.bfloat16)
 
@@ -270,8 +270,8 @@
             num_scalar_prefetch=1,
             grid=(2 * steps,),
             in_specs=[
-                pl.BlockSpec((zs, 1, MOE_SHARE, width), lambda i, c: (0, c[0], 0, 0)),
-                pl.BlockSpec((zs, 1, tail_rows, width), lambda i, c: (0, 1 - c[0], 1, 0)),
+                pl.BlockSpec((zs, 1, MOE_SHARE, width), lambda i, c: (0, (c[0] & 1), 0, 0)),
+                pl.BlockSpec((zs, 1, tail_rows, width), lambda i, c: (0, 1 - (c[0] & 1), 1, 0)),
                 pl.BlockSpec(before.shape, fixed),
                 pl.BlockSpec((1, width), fixed),
                 pl.BlockSpec((TAPS, channels), fixed),
@@ -374,7 +374,7 @@
     zs = lax.axis_size("z")
     eps = lax.axis_size(EP)
     width = moe_tokens.shape[1]
-    core_ref = jnp.stack([core, z_index]).astype(jnp.int32)
+    core_ref = (2 * z_index + core).reshape(1).astype(jnp.int32)
 
     gate, up, down = gate_weight[0], up_weight[0], down_weight[0]
     theirs = [swap_cores(array) for array in (gate, up, down)]

time: 183 us -> 181 us (0.989); the launches traced: 180 us -> 180 us
  waiting for transfers between devices: 34.3 us -> 37.3 us
    ppermute x14, waiting for transfers between devices: 15.5 us -> 18.1 us  [ring_sum(): lax.ppermute(sums[chain], 'z', [(i, (i + way) % zs) for i in range(zs)])]
  transfers between devices with their start and end apart: 25 -> 25, of which waited for: 14 -> 14; matrix products, arithmetic and copies ran while one was open for 4% -> 4% of each run, Pallas kernels for 9% -> 8%
where the time goes in v9:
time: 181 us; the launch traced here: 180 us
  blocking collectives  57.4 us (32%)
  starting transfers between devices  38.3 us (21%)
  waiting for transfers between devices  37.3 us (21%)
  Pallas kernels  24 us (13%)
  between operations  14.4 us (8%)
  local copies, waits for them, and re-layouts  3.91 us (2%)
  other arithmetic  3.47 us (2%)
    all_to_all x1, blocking collectives, exchange(): return lax.all_to_all(array, EP, split_axis=0, concat_axis=0, tiled=True)  57.4 us
    ppermute x14, starting transfers between devices, ring_sum(): lax.ppermute(sums[chain], 'z', [(i, (i + way) % zs) for i in range(zs)])  27.8 us
    ppermute x14, waiting for transfers between devices, ring_sum(): lax.ppermute(sums[chain], 'z', [(i, (i + way) % zs) for i in range(zs)])  18.1 us
    pallas_call x1, Pallas kernels, mixer_partial(): pl.pallas_call(functools.partial(mixer_kernel, steps), grid_spec=pltpu.Pr...  10.4 us
    pallas_call x1, Pallas kernels, expert_partial(): pl.pallas_call(functools.partial(expert_kernel, zs, steps), grid=(2 * ste...  9.02 us
    all_to_all x1, waiting for transfers between devices, exchange(): return lax.all_to_all(array, EP, split_axis=0, concat_axis=0, tiled=True)  8.08 us
    all_to_all x1, starting transfers between devices, exchange(): return lax.all_to_all(array, EP, split_axis=0, concat_axis=0, tiled=True)  6.32 us
    ppermute x1, waiting for transfers between devices, layer(): lax.ppermute(mix_tokens[mix_tokens.shape[0] - MOE_SHARE:], EP, [(i, i + 1...  5.31 us
  transfers between devices with their start and end apart: 25, of which 14 were waited for; matrix products, arithmetic and copies ran while one was open for 4% of the time, Pallas kernels for 8%

profile of v9, /device:TPU:2, one launch (start us, length us, event | category | flops | bytes accessed | tf_op | source)
XLA Modules:
  0.0 180.0 jit_solution(11046666598576666553)
XLA Ops:
  7.2 0.0 copy-start
  7.2 0.0 reduce-scatter.2.cloned.1.call-start
  7.2 0.1 collective-permute-start
  7.3 0.5 collective-permute-start.1
  7.8 0.1 collective-permute-start.2
  7.9 4.6 %prepare.1 = (bf16[512,4096]{1,0:T(8,128)(2,1)}, bf16[16,4096]{1,0:T(8,128)(2,1)}, s32[2,128]{1,0:T(2,128)}) custom-call(s32[1]{0:T(128)} %bitcast.place_ref, bf16[8,2,16,4096]{3,2,1,0:T(8,128)(2,1)} %bitcast.25, f32[1,4096]{1,0:T(1,128)} %bitcast.32, s32[2,256]{1,0:T(2,128)} %bitcast.34), custom_call_target="tpu_custom_call" | custom-call | flops 536870912 | bytes 5242880 | tf_op jit(solution)/shard_map/prepare/pallas_call | solution.py:114
  12.6 0.6 collective-permute-done.2.d1
  13.2 57.4 %all_to_all.10 = bf16[16,32,4096]{2,1,0:T(8,128)(2,1)} all-to-all(bf16[16,32,4096]{2,1,0:T(8,128)(2,1)} %bitcast.24), channel_id=1, replica_groups=mesh['y'=4,'x'=4,'z'=8,'core'=2] {'y','x'}, dimensions={0} | all-to-all | bytes 8388608 | tf_op jit(solution)/shard_map/all_to_all | solution.py:390
  70.6 0.0 copy-start.4
  70.6 0.0 copy-start.5
  70.6 0.0 copy-start.6
  70.6 9.0 %experts.1 = bf16[512,4096]{1,0:T(8,128)(2,1)} custom-call(bf16[512,4096]{1,0:T(8,128)(2,1)} %bitcast.21, bf16[4096,128]{1,0:T(8,128)(2,1)} %bitcast.27, bf16[4096,128]{1,0:T(8,128)(2,1)} %copy-done.1, bf16[4096,128]{1,0:T(8,128)(2,1)} %bitcast.29, bf16[4096,128]{1,0:T(8,128)(2,1)} %copy-done.2, bf16[128,4096]{1,0:T(8,128)(2,1)} %bitcast.31, ...), custom_call_target="tpu_custom_call" | custom-call | flops 3221225472 | bytes 14680064 | tf_op jit(solution)/shard_map/experts/pallas_call | solution.py:334
  79.6 0.1 collective-permute-start.5
  79.7 0.5 collective-permute-start.6
  80.2 0.1 collective-permute-start.7
  80.3 0.4 collective-permute-start.8
  80.8 0.0 reduce-scatter.2.cloned.1.call-update
  80.8 0.2 collective-permute-start.4
  81.0 0.9 slice.48
  81.9 5.1 %collective-permute-done.4.taps_theirs = f32[3,128]{1,0:T(4,128)S(1)} collective-permute-done((f32[3,128]{1,0:T(4,128)S(1)}, f32[3,128]{1,0:T(4,128)S(1)}, u32[]{:S(2)}, u32[]{:S(2)}) %collective-permute-start.4) | collective-permute-done | bytes 1568 | tf_op jit(solution)/shard_map/ppermute | solution.py:49
  87.0 2.1 %collective-permute-start.3 = (bf16[16,4096]{1,0:T(8,128)(2,1)S(1)}, bf16[16,4096]{1,0:T(8,128)(2,1)S(1)}, u32[]{:S(2)}, u32[]{:S(2)}) collective-permute-start(bf16[16,4096]{1,0:T(8,128)(2,1)S(1)} %slice.48), channel_id=1, source_target_pairs={{0,16},{16,32},{32,48},{48,64},{64,80},{80,96},{96,112},{112,128},... | collective-permute-start | bytes 393224 | tf_op jit(solution)/shard_map/ppermute | solution.py:410
  89.1 5.3 %collective-permute-done.3.before_ref = bf16[16,4096]{1,0:T(8,128)(2,1)S(1)} collective-permute-done((bf16[16,4096]{1,0:T(8,128)(2,1)S(1)}, bf16[16,4096]{1,0:T(8,128)(2,1)S(1)}, u32[]{:S(2)}, u32[]{:S(2)}) %collective-permute-start.3) | collective-permute-done | bytes 131104 | tf_op jit(solution)/shard_map/ppermute | solution.py:410
  94.4 0.0 collective-permute-done.5.refs_1_
  94.4 0.0 collective-permute-done.6.refs_3_
  94.5 0.6 copy-done.7
  95.1 10.4 %mixer.1 = (bf16[128,2048]{1,0:T(8,128)(2,1)}, bf16[128,2048]{1,0:T(8,128)(2,1)}, bf16[16,2048]{1,0:T(8,128)(2,1)}, bf16[16,2048]{1,0:T(8,128)(2,1)}) custom-call(s32[1]{0:T(128)} %bitcast.place_ref, bf16[8,2,16,4096]{3,2,1,0:T(8,128)(2,1)} %bitcast.22, bf16[8,2,16,4096]{3,2,1,0:T(8,128)(2,1)} %bitcast.23, bf16[16,4096]{1,0:T(8,128)(2,1)} %copy-done.7, ...), custom_call_target="tpu_custom_call" | custom-call | flops 1577058304 | bytes 11141120 | tf_op jit(solution)/shard_map/mixer/pallas_call | solution.py:267
  105.5 1.1 broadcast_multiply_fusion.1
  106.6 2.0 %collective-permute-start.9 = (bf16[16,2048]{1,0:T(8,128)(2,1)}, bf16[16,2048]{1,0:T(8,128)(2,1)S(1)}, u32[]{:S(2)}, u32[]{:S(2)}) collective-permute-start(bf16[16,2048]{1,0:T(8,128)(2,1)} %get-tuple-element.43), channel_id=1, source_target_pairs={{0,2},{2,4},{4,6},{6,8},{8,10},{10,12},{12,14},{14,0},{1,3},{3,5},... | collective-permute-start | bytes 196616 | tf_op jit(solution)/shard_map/ppermute | solution.py:247
  108.6 1.1 broadcast_multiply_fusion
  109.7 4.2 %collective-permute-start.16 = (bf16[16,2048]{1,0:T(8,128)(2,1)}, bf16[16,2048]{1,0:T(8,128)(2,1)S(1)}, u32[]{:S(2)}, u32[]{:S(2)}) collective-permute-start(bf16[16,2048]{1,0:T(8,128)(2,1)} %get-tuple-element.45), channel_id=1, source_target_pairs={{0,14},{2,0},{4,2},{6,4},{8,6},{10,8},{12,10},{14,12},{1,15},{3,1}... | collective-permute-start | bytes 196616 | tf_op jit(solution)/shard_map/ppermute | solution.py:247
  113.9 0.1 bitcast_add_fusion
  114.0 0.2 fusion.1
  114.2 0.2 fusion.2
  114.4 0.2 select_reduce_fusion.1
  114.6 0.1 select_reduce_fusion
  114.7 2.0 %collective-permute-done.9 = bf16[16,2048]{1,0:T(8,128)(2,1)S(1)} collective-permute-done((bf16[16,2048]{1,0:T(8,128)(2,1)}, bf16[16,2048]{1,0:T(8,128)(2,1)S(1)}, u32[]{:S(2)}, u32[]{:S(2)}) %collective-permute-start.9) | collective-permute-done | bytes 65568 | tf_op jit(solution)/shard_map/ppermute | solution.py:247
  116.7 0.1 collective-permute-start.10
  116.8 0.8 collective-permute-done.16
  117.7 3.7 %collective-permute-start.17 = (bf16[16,2048]{1,0:T(8,128)(2,1)S(1)}, bf16[16,2048]{1,0:T(8,128)(2,1)S(1)}, u32[]{:S(2)}, u32[]{:S(2)}) collective-permute-start(bf16[16,2048]{1,0:T(8,128)(2,1)S(1)} %add_convert_fusion.6), channel_id=1, source_target_pairs={{0,14},{2,0},{4,2},{6,4},{8,6},{10,8},{12,10},{14,12},{1,15},{3,1}... | collective-permute-start | bytes 196616 | tf_op jit(solution)/shard_map/ppermute | solution.py:247
  121.3 2.5 %collective-permute-done.10 = bf16[16,2048]{1,0:T(8,128)(2,1)S(1)} collective-permute-done((bf16[16,2048]{1,0:T(8,128)(2,1)S(1)}, bf16[16,2048]{1,0:T(8,128)(2,1)S(1)}, u32[]{:S(2)}, u32[]{:S(2)}) %collective-permute-start.10) | collective-permute-done | bytes 65568 | tf_op jit(solution)/shard_map/ppermute | solution.py:247
  123.8 0.1 collective-permute-start.11
  123.9 0.6 collective-permute-done.17
  124.5 3.8 %collective-permute-start.18 = (bf16[16,2048]{1,0:T(8,128)(2,1)S(1)}, bf16[16,2048]{1,0:T(8,128)(2,1)S(1)}, u32[]{:S(2)}, u32[]{:S(2)}) collective-permute-start(bf16[16,2048]{1,0:T(8,128)(2,1)S(1)} %add_convert_fusion.5), channel_id=1, source_target_pairs={{0,14},{2,0},{4,2},{6,4},{8,6},{10,8},{12,10},{14,12},{1,15},{3,1}... | collective-permute-start | bytes 196616 | tf_op jit(solution)/shard_map/ppermute | solution.py:247
  128.3 2.6 %collective-permute-done.11 = bf16[16,2048]{1,0:T(8,128)(2,1)S(1)} collective-permute-done((bf16[16,2048]{1,0:T(8,128)(2,1)S(1)}, bf16[16,2048]{1,0:T(8,128)(2,1)S(1)}, u32[]{:S(2)}, u32[]{:S(2)}) %collective-permute-start.11) | collective-permute-done | bytes 65568 | tf_op jit(solution)/shard_map/ppermute | solution.py:247
  130.9 0.1 collective-permute-start.12
  131.0 0.6 collective-permute-done.18
  131.6 3.8 %collective-permute-start.19 = (bf16[16,2048]{1,0:T(8,128)(2,1)S(1)}, bf16[16,2048]{1,0:T(8,128)(2,1)S(1)}, u32[]{:S(2)}, u32[]{:S(2)}) collective-permute-start(bf16[16,2048]{1,0:T(8,128)(2,1)S(1)} %add_convert_fusion.4), channel_id=1, source_target_pairs={{0,14},{2,0},{4,2},{6,4},{8,6},{10,8},{12,10},{14,12},{1,15},{3,1}... | collective-permute-start | bytes 196616 | tf_op jit(solution)/shard_map/ppermute | solution.py:247
  135.4 2.6 %collective-permute-done.12 = bf16[16,2048]{1,0:T(8,128)(2,1)S(1)} collective-permute-done((bf16[16,2048]{1,0:T(8,128)(2,1)S(1)}, bf16[16,2048]{1,0:T(8,128)(2,1)S(1)}, u32[]{:S(2)}, u32[]{:S(2)}) %collective-permute-start.12) | collective-permute-done | bytes 65568 | tf_op jit(solution)/shard_map/ppermute | solution.py:247
  138.0 0.1 collective-permute-start.13
  138.2 3.3 %collective-permute-start.20 = (bf16[16,2048]{1,0:T(8,128)(2,1)S(1)}, bf16[16,2048]{1,0:T(8,128)(2,1)S(1)}, u32[]{:S(2)}, u32[]{:S(2)}) collective-permute-start(bf16[16,2048]{1,0:T(8,128)(2,1)S(1)} %add_convert_fusion.3), channel_id=1, source_target_pairs={{0,14},{2,0},{4,2},{6,4},{8,6},{10,8},{12,10},{14,12},{1,15},{3,1}... | collective-permute-start | bytes 196616 | tf_op jit(solution)/shard_map/ppermute | solution.py:247
  141.5 2.1 %collective-permute-done.13 = bf16[16,2048]{1,0:T(8,128)(2,1)S(1)} collective-permute-done((bf16[16,2048]{1,0:T(8,128)(2,1)S(1)}, bf16[16,2048]{1,0:T(8,128)(2,1)S(1)}, u32[]{:S(2)}, u32[]{:S(2)}) %collective-permute-start.13) | collective-permute-done | bytes 65568 | tf_op jit(solution)/shard_map/ppermute | solution.py:247
  143.6 0.1 collective-permute-start.14
  143.7 3.3 %collective-permute-start.21 = (bf16[16,2048]{1,0:T(8,128)(2,1)S(1)}, bf16[16,2048]{1,0:T(8,128)(2,1)S(1)}, u32[]{:S(2)}, u32[]{:S(2)}) collective-permute-start(bf16[16,2048]{1,0:T(8,128)(2,1)S(1)} %add_convert_fusion.2), channel_id=1, source_target_pairs={{0,14},{2,0},{4,2},{6,4},{8,6},{10,8},{12,10},{14,12},{1,15},{3,1}... | collective-permute-start | bytes 196616 | tf_op jit(solution)/shard_map/ppermute | solution.py:247
  147.0 2.1 %collective-permute-done.14 = bf16[16,2048]{1,0:T(8,128)(2,1)S(1)} collective-permute-done((bf16[16,2048]{1,0:T(8,128)(2,1)S(1)}, bf16[16,2048]{1,0:T(8,128)(2,1)S(1)}, u32[]{:S(2)}, u32[]{:S(2)}) %collective-permute-start.14) | collective-permute-done | bytes 65568 | tf_op jit(solution)/shard_map/ppermute | solution.py:247
  149.2 0.1 collective-permute-start.15
  149.3 3.3 %collective-permute-start.22 = (bf16[16,2048]{1,0:T(8,128)(2,1)S(1)}, bf16[16,2048]{1,0:T(8,128)(2,1)S(1)}, u32[]{:S(2)}, u32[]{:S(2)}) collective-permute-start(bf16[16,2048]{1,0:T(8,128)(2,1)S(1)} %add_convert_fusion.1), channel_id=1, source_target_pairs={{0,14},{2,0},{4,2},{6,4},{8,6},{10,8},{12,10},{14,12},{1,15},{3,1}... | collective-permute-start | bytes 196616 | tf_op jit(solution)/shard_map/ppermute | solution.py:247
  152.6 2.1 %collective-permute-done.15 = bf16[16,2048]{1,0:T(8,128)(2,1)S(1)} collective-permute-done((bf16[16,2048]{1,0:T(8,128)(2,1)S(1)}, bf16[16,2048]{1,0:T(8,128)(2,1)S(1)}, u32[]{:S(2)}, u32[]{:S(2)}) %collective-permute-start.15) | collective-permute-done | bytes 65568 | tf_op jit(solution)/shard_map/ppermute | solution.py:247
  154.8 0.0 reduce-scatter.2.cloned.1.call-done
  154.8 2.1 %reshape.80 = bf16[16,128,128]{2,1,0:T(8,128)(2,1)} reshape(bf16[64,4096]{1,0:T(8,128)(2,1)} %reduce-scatter.2.cloned.1.call-done) | data formatting | bytes 1048576 | tf_op jit(solution)/shard_map/reshape | solution.py:423
  156.9 6.3 %all-to-all-start.1 = ((bf16[16,128,128]{2,1,0:T(8,128)(2,1)}), bf16[16,128,128]{2,1,0:T(8,128)(2,1)S(1)}, u32[]{:S(2)}, u32[]{:S(2)}) async-start(bf16[16,128,128]{2,1,0:T(8,128)(2,1)} %reshape.80), calls=%async_computation.2 | async-start | bytes 1048576 | tf_op jit(solution)/shard_map/all_to_all | solution.py:390
  163.2 0.7 pad_maximum_fusion
  163.9 8.1 %all-to-all-done.1 = bf16[16,128,128]{2,1,0:T(8,128)(2,1)S(1)} async-done(((bf16[16,128,128]{2,1,0:T(8,128)(2,1)}), bf16[16,128,128]{2,1,0:T(8,128)(2,1)S(1)}, u32[]{:S(2)}, u32[]{:S(2)}) %all-to-all-start.1) | async-done | bytes 524320 | tf_op jit(solution)/shard_map/all_to_all | solution.py:390
  172.0 0.2 reshape.81
  172.2 1.0 convolution_convert_fusion
  (49 shorter events, 0.4 us)
Async XLA Ops:
  7.2 107.1 %copy-start = (bf16[4096,16]{0,1:T(8,128)(2,1)S(1)}, bf16[4096,16]{0,1:T(8,128)(2,1)}, u32[]{:S(2)}) copy-start(bf16[4096,16]{0,1:T(8,128)(2,1)} %param.25) | copy-start | bytes 393220
  7.2 147.6 %reduce-scatter.2.cloned.1.call-start = ((), (), s32[]{:S(2)}) async-start(), calls=%async_computation.3 | async-start | bytes 4718592 | tf_op jit(solution)/shard_map/reduce_scatter | solution.py:394
  7.2 5.3 %collective-permute-start = (bf16[4096,128]{1,0:T(8,128)(2,1)}, bf16[4096,128]{1,0:T(8,128)(2,1)S(1)}, u32[]{:S(2)}, u32[]{:S(2)}) collective-permute-start(bf16[4096,128]{1,0:T(8,128)(2,1)} %bitcast.26), channel_id=1, source_target_pairs={{0,1},{1,0},{2,3},{3,2},{4,5},{5,4},{6,7},{7,6},{8,9},{9,8},{10,11... | collective-permute-start | bytes 3145736 | tf_op jit(solution)/shard_map/ppermute | solution.py:45
  7.3 5.2 %collective-permute-start.1 = (bf16[4096,128]{1,0:T(8,128)(2,1)}, bf16[4096,128]{1,0:T(8,128)(2,1)S(1)}, u32[]{:S(2)}, u32[]{:S(2)}) collective-permute-start(bf16[4096,128]{1,0:T(8,128)(2,1)} %bitcast.28), channel_id=1, source_target_pairs={{0,1},{1,0},{2,3},{3,2},{4,5},{5,4},{6,7},{7,6},{8,9},{9,8},{10,11... | collective-permute-start | bytes 3145736 | tf_op jit(solution)/shard_map/ppermute | solution.py:45
  7.8 5.4 %collective-permute-start.2 = (bf16[128,4096]{1,0:T(8,128)(2,1)}, bf16[128,4096]{1,0:T(8,128)(2,1)S(1)}, u32[]{:S(2)}, u32[]{:S(2)}) collective-permute-start(bf16[128,4096]{1,0:T(8,128)(2,1)} %bitcast.30), channel_id=1, source_target_pairs={{0,1},{1,0},{2,3},{3,2},{4,5},{5,4},{6,7},{7,6},{8,9},{9,8},{10,11... | collective-permute-start | bytes 3145736 | tf_op jit(solution)/shard_map/ppermute | solution.py:45
  12.6 58.0 %copy-start.1 = (bf16[4096,128]{1,0:T(8,128)(2,1)}, bf16[4096,128]{1,0:T(8,128)(2,1)S(1)}, u32[]{:S(2)}) copy-start(bf16[4096,128]{1,0:T(8,128)(2,1)S(1)} %collective-permute-done.g1) | copy-start | bytes 3145732
  12.6 58.0 %copy-start.2 = (bf16[4096,128]{1,0:T(8,128)(2,1)}, bf16[4096,128]{1,0:T(8,128)(2,1)S(1)}, u32[]{:S(2)}) copy-start(bf16[4096,128]{1,0:T(8,128)(2,1)S(1)} %collective-permute-done.1.u1) | copy-start | bytes 3145732
  13.2 57.4 %copy-start.3 = (bf16[128,4096]{1,0:T(8,128)(2,1)}, bf16[128,4096]{1,0:T(8,128)(2,1)S(1)}, u32[]{:S(2)}) copy-start(bf16[128,4096]{1,0:T(8,128)(2,1)S(1)} %collective-permute-done.2.d1) | copy-start | bytes 3145732
  70.6 9.1 %copy-start.4 = (bf16[4096,128]{1,0:T(8,128)(2,1)S(1)}, bf16[4096,128]{1,0:T(8,128)(2,1)}, u32[]{:S(2)}) copy-start(bf16[4096,128]{1,0:T(8,128)(2,1)} %refs_0_) | copy-start | bytes 3145732
  70.6 9.2 %copy-start.5 = (bf16[4096,128]{1,0:T(8,128)(2,1)S(1)}, bf16[4096,128]{1,0:T(8,128)(2,1)}, u32[]{:S(2)}) copy-start(bf16[4096,128]{1,0:T(8,128)(2,1)} %refs_2_) | copy-start | bytes 3145732
  70.6 9.6 %copy-start.6 = (bf16[4096,128]{1,0:T(8,128)(2,1)S(1)}, bf16[4096,128]{1,0:T(8,128)(2,1)}, u32[]{:S(2)}) copy-start(bf16[4096,128]{1,0:T(8,128)(2,1)} %refs_4_) | copy-start | bytes 3145732
  79.6 1.1 copy-start.10
  79.6 14.8 %collective-permute-start.5 = (bf16[4096,128]{1,0:T(8,128)(2,1)S(1)}, bf16[4096,128]{1,0:T(8,128)(2,1)}, u32[]{:S(2)}, u32[]{:S(2)}) collective-permute-start(bf16[4096,128]{1,0:T(8,128)(2,1)S(1)} %copy-done.4), channel_id=1, source_target_pairs={{0,1},{1,0},{2,3},{3,2},{4,5},{5,4},{6,7},{7,6},{8,9},{9,8},{10,11... | collective-permute-start | bytes 3145736 | tf_op jit(solution)/shard_map/ppermute | solution.py:49
  79.7 14.7 %collective-permute-start.6 = (bf16[4096,128]{1,0:T(8,128)(2,1)S(1)}, bf16[4096,128]{1,0:T(8,128)(2,1)}, u32[]{:S(2)}, u32[]{:S(2)}) collective-permute-start(bf16[4096,128]{1,0:T(8,128)(2,1)S(1)} %copy-done.5), channel_id=1, source_target_pairs={{0,1},{1,0},{2,3},{3,2},{4,5},{5,4},{6,7},{7,6},{8,9},{9,8},{10,11... | collective-permute-start | bytes 3145736 | tf_op jit(solution)/shard_map/ppermute | solution.py:49
  80.2 14.2 %collective-permute-start.7 = (bf16[4096,128]{1,0:T(8,128)(2,1)S(1)}, bf16[4096,128]{1,0:T(8,128)(2,1)}, u32[]{:S(2)}, u32[]{:S(2)}) collective-permute-start(bf16[4096,128]{1,0:T(8,128)(2,1)S(1)} %copy-done.6), channel_id=1, source_target_pairs={{0,1},{1,0},{2,3},{3,2},{4,5},{5,4},{6,7},{7,6},{8,9},{9,8},{10,11... | collective-permute-start | bytes 3145736 | tf_op jit(solution)/shard_map/ppermute | solution.py:49
  80.3 14.1 %collective-permute-start.8 = (bf16[128,4096]{1,0:T(8,128)(2,1)}, bf16[128,4096]{1,0:T(8,128)(2,1)}, u32[]{:S(2)}, u32[]{:S(2)}) collective-permute-start(bf16[128,4096]{1,0:T(8,128)(2,1)} %refs_6_), channel_id=1, source_target_pairs={{0,1},{1,0},{2,3},{3,2},{4,5},{5,4},{6,7},{7,6},{8,9},{9,8},{10,11... | collective-permute-start | bytes 3145736 | tf_op jit(solution)/shard_map/ppermute | solution.py:49
  80.8 6.2 %collective-permute-start.4 = (f32[3,128]{1,0:T(4,128)S(1)}, f32[3,128]{1,0:T(4,128)S(1)}, u32[]{:S(2)}, u32[]{:S(2)}) collective-permute-start(f32[3,128]{1,0:T(4,128)S(1)} %copy-done.10), channel_id=1, source_target_pairs={{0,1},{1,0},{2,3},{3,2},{4,5},{5,4},{6,7},{7,6},{8,9},{9,8},{10,11... | collective-permute-start | bytes 4616 | tf_op jit(solution)/shard_map/ppermute | solution.py:49
  87.0 7.5 %copy-start.11 = (f32[3,128]{1,0:T(4,128)}, f32[3,128]{1,0:T(4,128)S(1)}, u32[]{:S(2)}) copy-start(f32[3,128]{1,0:T(4,128)S(1)} %collective-permute-done.4.taps_theirs) | copy-start | bytes 4612
  87.0 7.4 %collective-permute-start.3 = (bf16[16,4096]{1,0:T(8,128)(2,1)S(1)}, bf16[16,4096]{1,0:T(8,128)(2,1)S(1)}, u32[]{:S(2)}, u32[]{:S(2)}) collective-permute-start(bf16[16,4096]{1,0:T(8,128)(2,1)S(1)} %slice.48), channel_id=1, source_target_pairs={{0,16},{16,32},{32,48},{48,64},{64,80},{80,96},{96,112},{112,128},... | collective-permute-start | bytes 393224 | tf_op jit(solution)/shard_map/ppermute | solution.py:410
  94.4 0.7 copy-start.7
  95.1 18.8 %copy-start.9 = (s32[256,2]{0,1:T(2,128)S(1)}, s32[256,2]{0,1:T(2,128)}, u32[]{:S(2)}) copy-start(s32[256,2]{0,1:T(2,128)} %param.26) | copy-start | bytes 6148
  95.1 18.8 %copy-start.12 = (s32[2,128]{1,0:T(2,128)S(1)}, s32[2,128]{1,0:T(2,128)}, u32[]{:S(2)}) copy-start(s32[2,128]{1,0:T(2,128)} %get-tuple-element.51) | copy-start | bytes 3076
  95.1 18.9 %copy-start.8 = (bf16[16,4096]{1,0:T(8,128)(2,1)S(1)}, bf16[16,4096]{1,0:T(8,128)(2,1)}, u32[]{:S(2)}) copy-start(bf16[16,4096]{1,0:T(8,128)(2,1)} %get-tuple-element.52) | copy-start | bytes 393220
  95.1 18.9 %copy-start.13 = (bf16[4096,4]{0,1:T(4,128)(2,1)S(1)}, bf16[4096,4]{0,1:T(4,128)(2,1)}, u32[]{:S(2)}) copy-start(bf16[4096,4]{0,1:T(4,128)(2,1)} %param.24) | copy-start | bytes 98308
  106.6 10.2 %collective-permute-start.9 = (bf16[16,2048]{1,0:T(8,128)(2,1)}, bf16[16,2048]{1,0:T(8,128)(2,1)S(1)}, u32[]{:S(2)}, u32[]{:S(2)}) collective-permute-start(bf16[16,2048]{1,0:T(8,128)(2,1)} %get-tuple-element.43), channel_id=1, source_target_pairs={{0,2},{2,4},{4,6},{6,8},{8,10},{10,12},{12,14},{14,0},{1,3},{3,5},... | collective-permute-start | bytes 196616 | tf_op jit(solution)/shard_map/ppermute | solution.py:247
  109.7 8.0 %collective-permute-start.16 = (bf16[16,2048]{1,0:T(8,128)(2,1)}, bf16[16,2048]{1,0:T(8,128)(2,1)S(1)}, u32[]{:S(2)}, u32[]{:S(2)}) collective-permute-start(bf16[16,2048]{1,0:T(8,128)(2,1)} %get-tuple-element.45), channel_id=1, source_target_pairs={{0,14},{2,0},{4,2},{6,4},{8,6},{10,8},{12,10},{14,12},{1,15},{3,1}... | collective-permute-start | bytes 196616 | tf_op jit(solution)/shard_map/ppermute | solution.py:247
  116.7 7.1 %collective-permute-start.10 = (bf16[16,2048]{1,0:T(8,128)(2,1)S(1)}, bf16[16,2048]{1,0:T(8,128)(2,1)S(1)}, u32[]{:S(2)}, u32[]{:S(2)}) collective-permute-start(bf16[16,2048]{1,0:T(8,128)(2,1)S(1)} %add_convert_fusion.13), channel_id=1, source_target_pairs={{0,2},{2,4},{4,6},{6,8},{8,10},{10,12},{12,14},{14,0},{1,3},{3,5},... | collective-permute-start | bytes 196616 | tf_op jit(solution)/shard_map/ppermute | solution.py:247
  117.7 6.9 %collective-permute-start.17 = (bf16[16,2048]{1,0:T(8,128)(2,1)S(1)}, bf16[16,2048]{1,0:T(8,128)(2,1)S(1)}, u32[]{:S(2)}, u32[]{:S(2)}) collective-permute-start(bf16[16,2048]{1,0:T(8,128)(2,1)S(1)} %add_convert_fusion.6), channel_id=1, source_target_pairs={{0,14},{2,0},{4,2},{6,4},{8,6},{10,8},{12,10},{14,12},{1,15},{3,1}... | collective-permute-start | bytes 196616 | tf_op jit(solution)/shard_map/ppermute | solution.py:247
  123.8 7.1 %collective-permute-start.11 = (bf16[16,2048]{1,0:T(8,128)(2,1)S(1)}, bf16[16,2048]{1,0:T(8,128)(2,1)S(1)}, u32[]{:S(2)}, u32[]{:S(2)}) collective-permute-start(bf16[16,2048]{1,0:T(8,128)(2,1)S(1)} %add_convert_fusion.12), channel_id=1, source_target_pairs={{0,2},{2,4},{4,6},{6,8},{8,10},{10,12},{12,14},{14,0},{1,3},{3,5},... | collective-permute-start | bytes 196616 | tf_op jit(solution)/shard_map/ppermute | solution.py:247
  124.5 7.1 %collective-permute-start.18 = (bf16[16,2048]{1,0:T(8,128)(2,1)S(1)}, bf16[16,2048]{1,0:T(8,128)(2,1)S(1)}, u32[]{:S(2)}, u32[]{:S(2)}) collective-permute-start(bf16[16,2048]{1,0:T(8,128)(2,1)S(1)} %add_convert_fusion.5), channel_id=1, source_target_pairs={{0,14},{2,0},{4,2},{6,4},{8,6},{10,8},{12,10},{14,12},{1,15},{3,1}... | collective-permute-start | bytes 196616 | tf_op jit(solution)/shard_map/ppermute | solution.py:247
  130.9 7.1 %collective-permute-start.12 = (bf16[16,2048]{1,0:T(8,128)(2,1)S(1)}, bf16[16,2048]{1,0:T(8,128)(2,1)S(1)}, u32[]{:S(2)}, u32[]{:S(2)}) collective-permute-start(bf16[16,2048]{1,0:T(8,128)(2,1)S(1)} %add_convert_fusion.11), channel_id=1, source_target_pairs={{0,2},{2,4},{4,6},{6,8},{8,10},{10,12},{12,14},{14,0},{1,3},{3,5},... | collective-permute-start | bytes 196616 | tf_op jit(solution)/shard_map/ppermute | solution.py:247
  131.6 6.5 %collective-permute-start.19 = (bf16[16,2048]{1,0:T(8,128)(2,1)S(1)}, bf16[16,2048]{1,0:T(8,128)(2,1)S(1)}, u32[]{:S(2)}, u32[]{:S(2)}) collective-permute-start(bf16[16,2048]{1,0:T(8,128)(2,1)S(1)} %add_convert_fusion.4), channel_id=1, source_target_pairs={{0,14},{2,0},{4,2},{6,4},{8,6},{10,8},{12,10},{14,12},{1,15},{3,1}... | collective-permute-start | bytes 196616 | tf_op jit(solution)/shard_map/ppermute | solution.py:247
  138.0 5.6 %collective-permute-start.13 = (bf16[16,2048]{1,0:T(8,128)(2,1)S(1)}, bf16[16,2048]{1,0:T(8,128)(2,1)S(1)}, u32[]{:S(2)}, u32[]{:S(2)}) collective-permute-start(bf16[16,2048]{1,0:T(8,128)(2,1)S(1)} %add_convert_fusion.10), channel_id=1, source_target_pairs={{0,2},{2,4},{4,6},{6,8},{8,10},{10,12},{12,14},{14,0},{1,3},{3,5},... | collective-permute-start | bytes 196616 | tf_op jit(solution)/shard_map/ppermute | solution.py:247
  138.2 5.5 %collective-permute-start.20 = (bf16[16,2048]{1,0:T(8,128)(2,1)S(1)}, bf16[16,2048]{1,0:T(8,128)(2,1)S(1)}, u32[]{:S(2)}, u32[]{:S(2)}) collective-permute-start(bf16[16,2048]{1,0:T(8,128)(2,1)S(1)} %add_convert_fusion.3), channel_id=1, source_target_pairs={{0,14},{2,0},{4,2},{6,4},{8,6},{10,8},{12,10},{14,12},{1,15},{3,1}... | collective-permute-start | bytes 196616 | tf_op jit(solution)/shard_map/ppermute | solution.py:247
  143.6 5.6 %collective-permute-start.14 = (bf16[16,2048]{1,0:T(8,128)(2,1)S(1)}, bf16[16,2048]{1,0:T(8,128)(2,1)S(1)}, u32[]{:S(2)}, u32[]{:S(2)}) collective-permute-start(bf16[16,2048]{1,0:T(8,128)(2,1)S(1)} %add_convert_fusion.9), channel_id=1, source_target_pairs={{0,2},{2,4},{4,6},{6,8},{8,10},{10,12},{12,14},{14,0},{1,3},{3,5},... | collective-permute-start | bytes 196616 | tf_op jit(solution)/shard_map/ppermute | solution.py:247
  143.7 5.5 %collective-permute-start.21 = (bf16[16,2048]{1,0:T(8,128)(2,1)S(1)}, bf16[16,2048]{1,0:T(8,128)(2,1)S(1)}, u32[]{:S(2)}, u32[]{:S(2)}) collective-permute-start(bf16[16,2048]{1,0:T(8,128)(2,1)S(1)} %add_convert_fusion.2), channel_id=1, source_target_pairs={{0,14},{2,0},{4,2},{6,4},{8,6},{10,8},{12,10},{14,12},{1,15},{3,1}... | collective-permute-start | bytes 196616 | tf_op jit(solution)/shard_map/ppermute | solution.py:247
  149.2 5.6 %collective-permute-start.15 = (bf16[16,2048]{1,0:T(8,128)(2,1)S(1)}, bf16[16,2048]{1,0:T(8,128)(2,1)S(1)}, u32[]{:S(2)}, u32[]{:S(2)}) collective-permute-start(bf16[16,2048]{1,0:T(8,128)(2,1)S(1)} %add_convert_fusion.8), channel_id=1, source_target_pairs={{0,2},{2,4},{4,6},{6,8},{8,10},{10,12},{12,14},{14,0},{1,3},{3,5},... | collective-permute-start | bytes 196616 | tf_op jit(solution)/shard_map/ppermute | solution.py:247
  149.3 13.9 %collective-permute-start.22 = (bf16[16,2048]{1,0:T(8,128)(2,1)S(1)}, bf16[16,2048]{1,0:T(8,128)(2,1)S(1)}, u32[]{:S(2)}, u32[]{:S(2)}) collective-permute-start(bf16[16,2048]{1,0:T(8,128)(2,1)S(1)} %add_convert_fusion.1), channel_id=1, source_target_pairs={{0,14},{2,0},{4,2},{6,4},{8,6},{10,8},{12,10},{14,12},{1,15},{3,1}... | collective-permute-start | bytes 196616 | tf_op jit(solution)/shard_map/ppermute | solution.py:247
  156.9 15.1 %all-to-all-start.1 = ((bf16[16,128,128]{2,1,0:T(8,128)(2,1)}), bf16[16,128,128]{2,1,0:T(8,128)(2,1)S(1)}, u32[]{:S(2)}, u32[]{:S(2)}) async-start(bf16[16,128,128]{2,1,0:T(8,128)(2,1)} %reshape.80), calls=%async_computation.2 | async-start | bytes 1048576 | tf_op jit(solution)/shard_map/all_to_all | solution.py:390
Sparse Core Ops, SparseCore 0:
  80.9 61.6 reduce-scatter.1
